TPU v7x, 256 devices: a 4x2x16 block of a 4x16x16 slice. The times are simulated.
256 devices in a mesh: grp: 2 (over y), sp: 32 (over z, core), tp: 4 (over x).
Axes of the slice: x: 4, y: 2, z: 16, core: 2. Of those that a mesh axis runs over, the one named last changes fastest.
The devices are a block of a 4x16x16 slice.
Arguments:
- query_plain: bfloat16 [10240, 1024], P(('grp', 'sp'), 'tp'), parts along dimension 0, may hold values from -6 to 6
- query_turn: bfloat16 [10240, 512], P(('grp', 'sp'), 'tp'), parts along dimension 0, may hold values from -40 to 40, as said below
- latent: bfloat16 [10240, 512], P(('grp', 'sp')), parts along dimension 0, may hold values from -6 to 6
- key_turn: bfloat16 [10240, 64], P(('grp', 'sp')), parts along dimension 0, may hold values from -40 to 40, as said below
- latent_norm_scale: bfloat16 [512], replicated, may hold values from 0.099609375 to 1.8984375
- plain_key_matrix: bfloat16 [512, 1024], P(None, 'tp'), may hold values from -0.25 to 0.25
- value_matrix: bfloat16 [512, 1024], P(None, 'tp'), may hold values from -0.25 to 0.25
- residual: bfloat16 [10240, 2048], P(('grp', 'sp', 'tp')), parts along dimension 0, may hold values from -6 to 6
- out_weight: bfloat16 [1024, 2048], replicated, may hold values from -6 to 6
- ffn_gain: bfloat16 [2048], replicated, may hold values from 0.099609375 to 1.8984375
- gate_weight: bfloat16 [32, 2048, 1024], P('sp', None, 'tp'), may hold values from -1 to 1
- up_weight: bfloat16 [32, 2048, 1024], P('sp', None, 'tp'), may hold values from -1 to 1
- down_weight: bfloat16 [32, 1024, 2048], P('sp', 'tp'), may hold values from -0.0625 to 0.0625
- routes: int32 [10240, 4], P(('grp', 'sp', 'tp')), parts along dimension 0, may hold values from 0 to 31, all different within a row; in each aligned block of 40 rows (0 to 39, 40 to 79, ...) at most 7 rows name the same one
- route_weights: float32 [10240, 4], P(('grp', 'sp', 'tp')), parts along dimension 0, may hold values from 0.1 to 0.6
Outputs:
- mixed: bfloat16 [10240, 2048], P(('grp', 'sp', 'tp')), parts along dimension 0
There are 2 independent parts, one for each index of `grp`. A program takes and returns all parts, laid end to end along the dimension named above; an argument that names none is the same for every part. Nothing has to cross between parts.
Inputs may be any that keep to these rules, and one draw needn't show every extreme that they name: `query_turn`: in the hidden draw some rows are large. `key_turn`: in the hidden draw some rows are large. `routes`: each row names 4 different experts. In each aligned block of 40 rows (the rows of one device) no expert is named more than 7 times, a bound that some block reaches.
All inputs are finite; a program needn't handle non-finite values.
Results may differ from a plain program's by a relative error of at most 0.015.
Values may be sent and summed in bfloat16 or wider, within the bound.
No kernel may reach another device: no remote copies, remote signals or barrier semaphores. Data moves between devices by JAX's collectives and lax.ppermute only.
A program may use at most 128 MiB of HBM per device.

v0:
```python
import jax
import jax.numpy as jnp
from jax import lax
from jax.sharding import Mesh
from jax.sharding import PartitionSpec as P

PLAIN_HEAD_WIDTH = 128
QK_ROPE = 64
VALUE_WIDTH = 128
GRID_W = 64
SP = ("sp_0", "sp_1")
GRP_SP = ("grp", "sp_0", "sp_1")
GRP_SP_TP = ("grp", "sp_0", "sp_1", "tp")


theta = 10000.0
eps = 1e-06
limit = 7.0
slope = 1.702


def sent_together(arrays, axis, dim, along):
    both = jnp.concatenate(arrays, axis=along)
    result, at, finished = (lax.all_gather(both, axis, axis=dim, tiled=True), 0, [])
    for a in arrays:
        finished.append(lax.slice_in_dim(result, at, at + a.shape[along], axis=along))
        at += a.shape[along]
    return tuple(finished)


def turned_gather(arrays, axis, dims):
    turned = [jnp.moveaxis(a, dim, 0) for a, dim in zip(arrays, dims)]
    both = jnp.concatenate([t.reshape(len(t), -1) for t in turned], axis=1)
    result, at, finished = (lax.all_gather(both, axis, axis=0, tiled=True), 0, [])
    for t, dim in zip(turned, dims):
        share = result[:, at : at + t[0].size].reshape(-1, *t.shape[1:])
        finished.append(jnp.moveaxis(share, 0, dim))
        at += t[0].size
    return tuple(finished)


def cut_along(array, dim, count):
    lengths = array.shape
    blocks = array.reshape(*lengths[:dim], count, lengths[dim] // count, *lengths[dim + 1 :])
    return jnp.moveaxis(blocks, dim, 0)


def laid_out(blocks, dim):
    lengths = list(blocks.shape[1:])
    lengths[dim] *= blocks.shape[0]
    return jnp.moveaxis(blocks, 0, dim).reshape(lengths)


def moved_by_axis(blocks, axes, order):
    inside = blocks.shape[1:]
    result = blocks.reshape(*(lax.axis_size(a) for a in axes), *inside)
    for k in order:
        result = lax.all_to_all(result, axes[k], k, k, tiled=True)
    return result.reshape(-1, *inside)


def exchange_by_chip(array, groups, order, split_dim, concat_dim):
    count = lax.axis_size(groups[0]) * lax.axis_size(groups[1])
    blocks = cut_along(array, split_dim, count)
    return laid_out(moved_by_axis(blocks, groups, order), concat_dim)


def turn(vector, row_shift, col_shift):
    width = vector.shape[-1]
    count = width // 4
    half = width // 2
    freqs = theta ** (-jnp.arange(count, dtype=jnp.float32) / count)
    extra = (1,) * (vector.ndim - 2)
    pieces = []
    for portion, shift in ((vector[..., :half], row_shift), (vector[..., half:], col_shift)):
        angle = (shift.astype(jnp.float32)[:, None] * freqs[None, :]).reshape(
            (shift.shape[0],) + extra + (count,)
        )
        lower = portion[..., :count]
        upper = portion[..., count:]
        pieces.append(
            jnp.concatenate(
                [
                    lower * jnp.cos(angle) - upper * jnp.sin(angle),
                    lower * jnp.sin(angle) + upper * jnp.cos(angle),
                ],
                axis=-1,
            )
        )
    return jnp.concatenate(pieces, axis=-1)


def norm_scale(values, gain):
    wide = values.astype(jnp.float32)
    return (
        wide
        * lax.rsqrt(jnp.mean(wide * wide, axis=-1, keepdims=True) + eps)
        * gain.astype(jnp.float32)
    )


def expert_active(rows, gate_w, up_w):
    gate_pre = jnp.minimum(jnp.dot(rows, gate_w, preferred_element_type=jnp.float32), limit)
    up_pre = jnp.clip(jnp.dot(rows, up_w, preferred_element_type=jnp.float32), -limit, limit)
    return ((up_pre + 1.0) * gate_pre * jax.nn.sigmoid(slope * gate_pre)).astype(jnp.bfloat16)


def expert_whole(rows, gate_w, up_w, down_w, groups):
    active = expert_active(rows, gate_w, up_w)
    piece = down_w.shape[0] // groups
    total = jnp.zeros((rows.shape[0], down_w.shape[1]), jnp.float32)
    for index in range(groups):
        product = jnp.dot(
            active[:, index * piece : (index + 1) * piece],
            down_w[index * piece : (index + 1) * piece],
            preferred_element_type=jnp.float32,
        )
        total = total + product.astype(jnp.bfloat16).astype(jnp.float32)
    return total.astype(jnp.bfloat16)


def on_device(
    query_plain,
    query_turn,
    latent,
    key_turn,
    latent_norm_scale,
    plain_key_matrix,
    value_matrix,
    residual,
    out_weight,
    ffn_gain,
    gate_weight,
    up_weight,
    down_weight,
    routes,
    route_weights,
):
    tok_dev = latent.shape[0]
    heads_dev = query_plain.shape[1] // PLAIN_HEAD_WIDTH
    model_width = residual.shape[1]
    place = lax.axis_index(SP) * tok_dev + jnp.arange(tok_dev, dtype=jnp.int32)
    grid_row = place // GRID_W
    grid_col = place % GRID_W
    normed_latent = norm_scale(latent, latent_norm_scale).astype(jnp.bfloat16)
    key_plain = jnp.dot(normed_latent, plain_key_matrix, preferred_element_type=jnp.float32).astype(
        jnp.bfloat16
    )
    values = jnp.dot(normed_latent, value_matrix, preferred_element_type=jnp.float32).astype(
        jnp.bfloat16
    )
    key_rot = turn(key_turn.astype(jnp.float32), grid_row, grid_col).astype(jnp.bfloat16)
    key_pairs = key_rot.reshape(tok_dev // 2, 2 * QK_ROPE)
    query_rot = turn(
        query_turn.astype(jnp.float32).reshape(tok_dev, heads_dev, QK_ROPE), grid_row, grid_col
    ).astype(jnp.bfloat16)
    plain_query = query_plain.reshape(tok_dev, heads_dev, PLAIN_HEAD_WIDTH)
    scale = (PLAIN_HEAD_WIDTH + QK_ROPE) ** (-0.5)
    most = jnp.full((heads_dev, tok_dev), -jnp.inf, jnp.float32)
    total = jnp.zeros((heads_dev, tok_dev), jnp.float32)
    summed = jnp.zeros((heads_dev, tok_dev, VALUE_WIDTH), jnp.float32)
    piece_keys, piece_values, piece_pairs = (
        *sent_together((key_plain, values), SP, 0, 1),
        lax.all_gather(key_pairs, SP, axis=0, tiled=True),
    )
    count = piece_keys.shape[0]
    piece_rot = piece_pairs.reshape(count, QK_ROPE)
    new_most = []
    new_total = []
    new_summed = []
    for head in range(heads_dev):
        head_keys = piece_keys[:, head * PLAIN_HEAD_WIDTH : (head + 1) * PLAIN_HEAD_WIDTH]
        head_values = piece_values[:, head * VALUE_WIDTH : (head + 1) * VALUE_WIDTH]
        scores = (
            jnp.einsum(
                "qd,kd->qk", plain_query[:, head], head_keys, preferred_element_type=jnp.float32
            )
            + jnp.einsum(
                "qd,kd->qk", query_rot[:, head], piece_rot, preferred_element_type=jnp.float32
            )
        ) * scale
        peak = jnp.max(scores, axis=1)
        factor = jnp.exp(most[head] - peak)
        weights = jnp.exp(scores - peak[:, None])
        new_total.append(total[head] * factor + jnp.sum(weights, axis=1))
        new_summed.append(
            summed[head] * factor[:, None]
            + jnp.dot(weights.astype(jnp.bfloat16), head_values, preferred_element_type=jnp.float32)
        )
        new_most.append(peak)
    total = jnp.stack(new_total)
    summed = jnp.stack(new_summed)
    attended = jnp.transpose((summed / total[..., None]).astype(jnp.bfloat16), (1, 0, 2)).reshape(
        tok_dev, heads_dev * VALUE_WIDTH
    )
    rows_dev = residual.shape[0]
    token_heads = lax.all_to_all(attended, "tp", split_axis=0, concat_axis=1, tiled=True)
    projected = jnp.dot(token_heads, out_weight, preferred_element_type=jnp.float32)
    hidden = (residual.astype(jnp.float32) + projected).astype(jnp.bfloat16)
    normed = norm_scale(hidden, ffn_gain).astype(jnp.bfloat16)
    top_count = routes.shape[1]
    experts_all = lax.axis_size(SP) * gate_weight.shape[0]
    capacity = min(rows_dev, max(2, rows_dev * top_count * 3 // (2 * experts_all)))
    flat_routes = routes.reshape(rows_dev * top_count)
    marks = (flat_routes[:, None] == jnp.arange(experts_all, dtype=jnp.int32)[None, :]).astype(
        jnp.int32
    )
    earlier = jnp.cumsum(marks, axis=0, dtype=jnp.int32) - marks
    slots = jnp.sum(earlier * marks, axis=1, dtype=jnp.int32)
    target = flat_routes * capacity + slots
    chosen = (
        target.reshape(rows_dev, top_count)[None, :, :]
        == jnp.arange(experts_all * capacity, dtype=jnp.int32)[:, None, None]
    )
    dispatch_table = jnp.sum(chosen.astype(jnp.bfloat16), axis=2)
    outgoing = jnp.dot(dispatch_table, normed, preferred_element_type=jnp.float32).astype(
        jnp.bfloat16
    )
    outgoing = outgoing.reshape(experts_all, capacity, model_width)
    gate_w = gate_weight[0]
    up_w = up_weight[0]
    down_w = down_weight[0]
    group = lax.axis_size("tp")
    gate_full, up_full, down_full = turned_gather((gate_w, up_w, down_w), "tp", (1, 1, 0))
    arrived = lax.all_to_all(outgoing, SP, split_axis=0, concat_axis=0, tiled=True)
    result_rows = expert_whole(
        arrived.reshape(experts_all * capacity, model_width), gate_full, up_full, down_full, group
    )
    returned = exchange_by_chip(
        result_rows.reshape(experts_all, capacity, model_width), ("sp_0", "sp_1"), (1, 0), 0, 0
    )
    picked = returned.reshape(experts_all * capacity, model_width)[target]
    picked = picked.reshape(rows_dev, top_count, model_width).astype(jnp.float32)
    return (hidden.astype(jnp.float32) + jnp.sum(route_weights[..., None] * picked, axis=1)).astype(
        jnp.bfloat16
    )


def solution(mesh):
    torus = Mesh(
        mesh.devices.reshape(mesh.shape["grp"], 16, 2, mesh.shape["tp"]),
        ("grp", "sp_0", "sp_1", "tp"),
    )
    placed = (
        P(GRP_SP, "tp"),
        P(GRP_SP, "tp"),
        P(GRP_SP, None),
        P(GRP_SP, None),
        P(),
        P(None, "tp"),
        P(None, "tp"),
        P(GRP_SP_TP, None),
        P(),
        P(),
        P(SP, None, "tp"),
        P(SP, None, "tp"),
        P(SP, "tp", None),
        P(GRP_SP_TP, None),
        P(GRP_SP_TP, None),
    )
    return jax.shard_map(
        on_device, mesh=torus, in_specs=placed, out_specs=P(GRP_SP_TP, None), check_vma=False
    )
```

profile of v0, /device:TPU:34, one launch (start us, length us, event | category | flops | bytes accessed | tf_op | source)
XLA Modules:
  0.0 310.7 jit_solution(7776849853484320127)
XLA Ops:
  8.4 1.2 convolution_convert_fusion.5
  9.6 1.3 convolution_convert_fusion.6
  11.7 1.5 copy.71
  13.8 2.8 pad_maximum_fusion
  17.3 52.1 %all_gather.10 = bf16[2560,128]{1,0:T(8,128)(2,1)S(1)} all-gather(bf16[80,128]{1,0:T(8,128)(2,1)S(1)} %convert_element_type.126), channel_id=1, replica_groups=mesh['grp'=2,'sp_0'=16,'sp_1'=2,'tp'=4] {'sp_0','sp_1'}, dimensions={0}, use_global_device_ids=true | all-gather | bytes 675840 | tf_op jit(solution)/shard_map/all_gather | solution.py:164
  72.8 2.3 fusion.95
  75.1 2.0 fusion.96
  77.1 22.1 %all-gather.3.cloned.1.call-done = bf16[5120,512]{1,0:T(8,128)(2,1)} async-done(((bf16[160,512]{1,0:T(8,128)(2,1)}), bf16[5120,512]{1,0:T(8,128)(2,1)}) %all-gather.3.cloned.1.call-update) | async-done | bytes 5242896 | tf_op jit(solution)/shard_map/all_gather | solution.py:24
  99.2 3.2 %fusion.104 = (f32[160]{0:T(256)S(1)}, f32[160,5120]{1,0:T(8,128)S(1)}) fusion(f32[160,5120]{1,0:T(8,128)} %fusion.95, bf16[160,1,128]{2,1,0:T(2,128)(2,1)S(1)} %copy-done.4, bf16[5120,512]{1,0:T(8,128)(2,1)} %all-gather.3.cloned.1.call-done), kind=kOutput, calls=%fused_computation.135 | convolution fusion | flops 212172640 | bytes 7905920 | tf_op jit(solution)/shard_map/qd,kd->qk/dot_general | solution.py:175
  106.8 4.8 %all-to-all-start = ((bf16[4,40,256]{2,1,0:T(8,128)(2,1)}), bf16[4,40,256]{2,1,0:T(8,128)(2,1)S(1)}, u32[]{:S(2)}, u32[]{:S(2)}) async-start(bf16[4,40,256]{2,1,0:T(8,128)(2,1)} %all_to_all.23), calls=%async_computation | async-start | bytes 163840 | tf_op jit(solution)/shard_map/all_to_all | solution.py:197
  111.6 4.2 %all-to-all-done = bf16[4,40,256]{2,1,0:T(8,128)(2,1)S(1)} async-done(((bf16[4,40,256]{2,1,0:T(8,128)(2,1)}), bf16[4,40,256]{2,1,0:T(8,128)(2,1)S(1)}, u32[]{:S(2)}, u32[]{:S(2)}) %all-to-all-start) | async-done | bytes 81952 | tf_op jit(solution)/shard_map/all_to_all | solution.py:197
  115.8 3.6 %multiply_reduce_fusion.1 = (f32[40]{0:T(128)S(1)}, f32[40,2048]{1,0:T(8,128)S(1)}) fusion(bf16[40,1024]{1,0:T(8,128)(2,1)S(1)} %bitcast.79, bf16[1024,2048]{1,0:T(8,128)(2,1)} %param.23, bf16[40,2048]{1,0:T(8,128)(2,1)S(1)} %copy-done.5), kind=kOutput, calls=%fused_computation.66 | convolution fusion | flops 168263648 | bytes 4767904 | tf_op jit(solution)/shard_map/dot_general | solution.py:198
  120.2 63.2 %all_to_all.34 = bf16[32,7,2048]{2,1,0:T(8,128)(2,1)S(1)} all-to-all(bf16[32,7,2048]{2,1,0:T(8,128)(2,1)S(1)} %reshape.304), channel_id=1, replica_groups=mesh['grp'=2,'sp_0'=16,'sp_1'=2,'tp'=4] {'sp_0','sp_1'}, dimensions={0} | all-to-all | bytes 1835008 | tf_op jit(solution)/shard_map/all_to_all | solution.py:225
  183.7 38.2 %all-gather.5.cloned.1.call-done = bf16[1024,6144]{1,0:T(8,128)(2,1)} async-done(((bf16[256,6144]{1,0:T(8,128)(2,1)}), bf16[1024,6144]{1,0:T(8,128)(2,1)}) %all-gather.5.cloned.1.call-update) | async-done | bytes 12582928 | tf_op jit(solution)/shard_map/all_gather | solution.py:34
  221.9 3.6 %fusion.44 = f32[224,1024]{1,0:T(8,128)S(1)} fusion(bf16[224,2048]{1,0:T(8,128)(2,1)S(1)} %reshape.305, bf16[1024,6144]{1,0:T(8,128)(2,1)} %all-gather.5.cloned.1.call-done), kind=kOutput, calls=%fused_computation.47 | convolution fusion | flops 939753472 | bytes 6029312 | tf_op jit(solution)/shard_map/dot_general | solution.py:103
  225.5 3.7 %fusion.47 = bf16[224,1024]{1,0:T(8,128)(2,1)S(1)} fusion(f32[224,1024]{1,0:T(8,128)S(1)} %fusion.44, bf16[224,2048]{1,0:T(8,128)(2,1)S(1)} %reshape.305, bf16[1024,6144]{1,0:T(8,128)(2,1)} %all-gather.5.cloned.1.call-done), kind=kOutput, calls=%fused_computation.48 | convolution fusion | flops 941588480 | bytes 6488064 | tf_op jit(solution)/shard_map/dot_general | solution.py:104
  229.2 1.6 fusion.19
  230.9 1.6 fusion.18
  232.5 1.6 fusion.16
  234.1 1.6 fusion.14
  236.7 4.5 %all_to_all.35 = bf16[16,2,1,7,2048]{4,0,3,2,1:T(8,128)(2,1)S(1)} all-to-all(bf16[16,2,1,7,2048]{4,0,3,2,1:T(8,128)(2,1)S(1)} %copy.72), channel_id=1, replica_groups=mesh['grp'=2,'sp_0'=16,'sp_1'=2,'tp'=4] {'sp_1'}, dimensions={1} | all-to-all | bytes 1835008 | tf_op jit(solution)/shard_map/all_to_all | solution.py:58
  241.2 1.9 copy.73
  243.1 12.4 %all-to-all-start.3 = ((bf16[16,2,1,7,2048]{4,1,3,2,0:T(2,128)(2,1)}), bf16[16,2,1,7,2048]{4,1,3,2,0:T(2,128)(2,1)S(1)}, u32[]{:S(2)}, u32[]{:S(2)}) async-start(bf16[16,2,1,7,2048]{4,1,3,2,0:T(2,128)(2,1)} %copy.73), calls=%async_computation.3 | async-start | bytes 1835008 | tf_op jit(solution)/shard_map/all_to_all | solution.py:58
  255.7 44.4 %all-to-all-done.3 = bf16[16,2,1,7,2048]{4,1,3,2,0:T(2,128)(2,1)S(1)} async-done(((bf16[16,2,1,7,2048]{4,1,3,2,0:T(2,128)(2,1)}), bf16[16,2,1,7,2048]{4,1,3,2,0:T(2,128)(2,1)S(1)}, u32[]{:S(2)}, u32[]{:S(2)}) %all-to-all-start.3) | async-done | bytes 917536 | tf_op jit(solution)/shard_map/all_to_all | solution.py:58
  (97 shorter events, 17.5 us)
Async XLA Ops:
  6.5 1.8 copy-start
  6.6 6.6 %copy-start.3 = (bf16[1,2048,256]{2,1,0:T(8,128)(2,1)S(1)}, bf16[1,2048,256]{2,1,0:T(8,128)(2,1)}, u32[]{:S(2)}) copy-start(bf16[1,2048,256]{2,1,0:T(8,128)(2,1)} %param.25) | copy-start | bytes 3145732
  6.6 92.6 %all-gather.3.cloned.1.call-start = ((), (), s32[]{:S(2)}) async-start(), calls=%async_computation.4 | async-start | bytes 5406720 | tf_op jit(solution)/shard_map/all_gather | solution.py:24
  11.6 210.3 %all-gather.5.cloned.1.call-start = ((), (), s32[]{:S(2)}) async-start(), calls=%async_computation.5 | async-start | bytes 15728640 | tf_op jit(solution)/shard_map/all_gather | solution.py:34
  13.8 2.9 copy-start.9
  16.7 53.2 %copy-start.8 = (bf16[160,128]{1,0:T(8,128)(2,1)S(1)}, bf16[160,128]{1,0:T(8,128)(2,1)}, u32[]{:S(2)}) copy-start(bf16[160,128]{1,0:T(8,128)(2,1)} %param.16) | copy-start | bytes 122884
  16.7 53.3 %copy-start.7 = (bf16[160,256]{1,0:T(8,128)(2,1)S(1)}, bf16[160,256]{1,0:T(8,128)(2,1)}, u32[]{:S(2)}) copy-start(bf16[160,256]{1,0:T(8,128)(2,1)} %param.15) | copy-start | bytes 245764
  16.7 53.4 %copy-start.11 = (s32[40,4]{0,1:T(4,128)S(1)}, s32[40,4]{0,1:T(4,128)}, u32[]{:S(2)}) copy-start(s32[40,4]{0,1:T(4,128)} %param.28) | copy-start | bytes 1924
  16.7 55.3 %copy-start.10 = (bf16[2048]{0:T(1024)(128)(2,1)S(1)}, bf16[2048]{0:T(1024)(128)(2,1)}, u32[]{:S(2)}) copy-start(bf16[2048]{0:T(1024)(128)(2,1)} %param.24) | copy-start | bytes 12292
  69.8 3.0 copy-start.2
  75.1 24.1 %copy-start.4 = (bf16[160,1,128]{2,1,0:T(2,128)(2,1)S(1)}, bf16[160,1,128]{2,1,0:T(2,128)(2,1)}, u32[]{:S(2)}) copy-start(bf16[160,1,128]{2,1,0:T(2,128)(2,1)} %get-tuple-element.12) | copy-start | bytes 122884
  99.2 3.8 %slice-start = ((s8[5242880]{0:T(1024)(128)(4,1)}), s8[4194304]{0:T(1024)(128)(4,1)S(1)}, s32[]{:S(2)}) async-start(s8[5242880]{0:T(1024)(128)(4,1)} %bitcast.73), calls=%async_computation.6 | async-start | bytes 8388608
  99.2 3.9 %slice-start.1 = ((s8[5242880]{0:T(1024)(128)(4,1)}), s8[1048576]{0:T(1024)(128)(4,1)S(1)}, s32[]{:S(2)}) async-start(s8[5242880]{0:T(1024)(128)(4,1)} %bitcast.73), calls=%async_computation.7 | async-start | bytes 2097152
  105.1 10.7 %copy-start.5 = (bf16[40,2048]{1,0:T(8,128)(2,1)S(1)}, bf16[40,2048]{1,0:T(8,128)(2,1)}, u32[]{:S(2)}) copy-start(bf16[40,2048]{1,0:T(8,128)(2,1)} %param.22) | copy-start | bytes 491524
  106.8 9.0 %all-to-all-start = ((bf16[4,40,256]{2,1,0:T(8,128)(2,1)}), bf16[4,40,256]{2,1,0:T(8,128)(2,1)S(1)}, u32[]{:S(2)}, u32[]{:S(2)}) async-start(bf16[4,40,256]{2,1,0:T(8,128)(2,1)} %all_to_all.23), calls=%async_computation | async-start | bytes 163840 | tf_op jit(solution)/shard_map/all_to_all | solution.py:197
  236.1 19.3 %copy-start.6 = (s32[40,4]{1,0:T(8,128)S(1)}, s32[40,4]{1,0:T(8,128)}, u32[]{:S(2)}) copy-start(s32[40,4]{1,0:T(8,128)} %get-tuple-element.19) | copy-start | bytes 1924
  236.1 19.4 %copy-start.12 = (f32[40,4]{0,1:T(4,128)S(1)}, f32[40,4]{0,1:T(4,128)}, u32[]{:S(2)}) copy-start(f32[40,4]{0,1:T(4,128)} %param.29) | copy-start | bytes 1924
  243.1 57.0 %all-to-all-start.3 = ((bf16[16,2,1,7,2048]{4,1,3,2,0:T(2,128)(2,1)}), bf16[16,2,1,7,2048]{4,1,3,2,0:T(2,128)(2,1)S(1)}, u32[]{:S(2)}, u32[]{:S(2)}) async-start(bf16[16,2,1,7,2048]{4,1,3,2,0:T(2,128)(2,1)} %copy.73), calls=%async_computation.3 | async-start | bytes 1835008 | tf_op jit(solution)/shard_map/all_to_all | solution.py:58
  300.8 3.1 %copy-start.1 = (bf16[512,256]{1,0:T(8,128)(2,1)S(1)}, bf16[512,256]{1,0:T(8,128)(2,1)}, u32[]{:S(2)}) copy-start(bf16[512,256]{1,0:T(8,128)(2,1)} %param.21) | copy-start | bytes 786436
Sparse Core Ops, SparseCore 0:
  11.7 87.4 all-gather.2
  101.0 120.8 all-gather.4
where the time goes:
time: 312 us; the launch traced here: 311 us
  blocking collectives  120 us (38%)
  waiting for transfers between devices  109 us (35%)
  matrix products  29.9 us (10%)
  starting transfers between devices  17.2 us (6%)
  between operations  13.9 us (4%)
  local copies, waits for them, and re-layouts  10.8 us (3%)
  other arithmetic  10.1 us (3%)
    all_to_all x1, blocking collectives, on_device(): lax.all_to_all(outgoing, SP, split_axis=0, concat_axis=0, tiled=True)  63.2 us
    all_gather x1, blocking collectives, on_device(): lax.all_gather(key_pairs, SP, axis=0, tiled=True)  52.1 us
    all_to_all x1, waiting for transfers between devices, moved_by_axis(): result = lax.all_to_all(result, axes[k], k, k, tiled=True)  44.4 us
    all_gather x1, waiting for transfers between devices, turned_gather(): lax.all_gather(both, axis, axis=0, tiled=True)  38.2 us
    all_gather x1, waiting for transfers between devices, sent_together(): lax.all_gather(both, axis, axis=dim, tiled=True)  22.1 us
    all_to_all x1, starting transfers between devices, moved_by_axis(): result = lax.all_to_all(result, axes[k], k, k, tiled=True)  12.4 us
    dot_general x4, matrix products, expert_whole(): jnp.dot(active[:, index * piece:(index + 1) * piece], down_w[index * piec...  6.55 us
  transfers between devices with their start and end apart: 4, of which 4 were waited for; matrix products, arithmetic and copies ran while one was open for 8% of the time, Pallas kernels for 0%

commit v1 on v0

v1 whole, which is shorter than its diff:
```python
import jax
import jax.numpy as jnp
import numpy as np
from jax import lax
from jax.experimental import pallas as pl
from jax.experimental.pallas import tpu as pltpu
from jax.sharding import Mesh
from jax.sharding import PartitionSpec as P

PLAIN_HEAD_WIDTH = 128
QK_ROPE = 64
VALUE_WIDTH = 128
GRID_W = 64
SP = ("sp_0", "sp_1")
GRP_SP = ("grp", "sp_0", "sp_1")
GRP_SP_TP = ("grp", "sp_0", "sp_1", "tp")


theta = 10000.0
eps = 1e-06
limit = 7.0
slope = 1.702
STAT_LANES = 128


def turn_tables(place):
    count = QK_ROPE // 4
    freqs = theta ** (-jnp.arange(count, dtype=jnp.float32) / count)
    halves_cos, halves_sin = [], []
    for shift in (place // GRID_W, place % GRID_W):
        angle = shift.astype(jnp.float32)[:, None] * freqs[None, :]
        halves_cos += [jnp.cos(angle)] * 2
        halves_sin += [jnp.sin(angle)] * 2
    return jnp.concatenate(halves_cos, axis=1), jnp.concatenate(halves_sin, axis=1)


def partner_matrix(width):
    count = QK_ROPE // 4
    out = np.zeros((width, width), np.float32)
    for at in range(0, width, 2 * count):
        for i in range(count):
            out[at + count + i, at + i] = -1.0
            out[at + i, at + count + i] = 1.0
    return out


def norm_scale(values, gain):
    wide = values.astype(jnp.float32)
    return (
        wide
        * lax.rsqrt(jnp.mean(wide * wide, axis=-1, keepdims=True) + eps)
        * gain.astype(jnp.float32)
    )


def shifted(array, axis, step):
    count = lax.axis_size(axis)
    return lax.ppermute(array, axis, [(i, (i + step) % count) for i in range(count)])


def expert_active(rows, gate_w, up_w):
    gate_pre = jnp.minimum(jnp.dot(rows, gate_w, preferred_element_type=jnp.float32), limit)
    up_pre = jnp.clip(jnp.dot(rows, up_w, preferred_element_type=jnp.float32), -limit, limit)
    return ((up_pre + 1.0) * gate_pre * jax.nn.sigmoid(slope * gate_pre)).astype(jnp.bfloat16)


def expert_whole(rows, quarters):
    total = jnp.zeros((rows.shape[0], quarters[0][2].shape[1]), jnp.float32)
    for gate_w, up_w, down_w in quarters:
        active = expert_active(rows, gate_w, up_w)
        product = jnp.dot(active, down_w, preferred_element_type=jnp.float32)
        total = total + product.astype(jnp.bfloat16).astype(jnp.float32)
    return total.astype(jnp.bfloat16)


def attend_body(near_ref, other_ref, shares_ref, cos_ref, sin_ref, swap_ref, out_ref, kv_ref):
    shards = shares_ref.shape[0]
    width = shares_ref.shape[2]
    near = near_ref.shape[0]
    latent_width = width
    quarter = out_ref.shape[1]
    tokens = shards * quarter
    value_wide = width // 2
    heads = value_wide // PLAIN_HEAD_WIDTH
    scale = (PLAIN_HEAD_WIDTH + QK_ROPE) ** (-0.5)
    near_rot = near_ref[:, latent_width : latent_width + QK_ROPE]
    other_rot = other_ref[:, latent_width : latent_width + QK_ROPE]
    lane = lax.broadcasted_iota(jnp.int32, (tokens, STAT_LANES), 1)
    stats = jnp.zeros((tokens, STAT_LANES), jnp.float32)
    last = (((1,), (1,)), ((), ()))
    for j in range(shards):
        matrix = shares_ref[j, :latent_width, :]
        kv_ref[:near, :] = jnp.dot(
            near_ref[:, :latent_width], matrix, preferred_element_type=jnp.float32
        ).astype(jnp.bfloat16)
        kv_ref[near:, :] = jnp.dot(
            other_ref[:, :latent_width], matrix, preferred_element_type=jnp.float32
        ).astype(jnp.bfloat16)
        at = latent_width
        half = tokens // 2
        plain = jnp.concatenate(
            (
                shares_ref[j, at : at + half, :value_wide],
                shares_ref[j, at : at + half, value_wide:],
            ),
            axis=0,
        )
        at += half
        raw = jnp.concatenate(
            [
                shares_ref[j, at : at + quarter, i * heads * QK_ROPE : (i + 1) * heads * QK_ROPE]
                for i in range(tokens // quarter)
            ],
            axis=0,
        )
        swapped = jnp.dot(raw, swap_ref[...], preferred_element_type=jnp.float32)
        turned = (raw.astype(jnp.float32) * cos_ref[...] + swapped * sin_ref[...]).astype(
            jnp.bfloat16
        )
        for h in range(heads):
            lo = h * PLAIN_HEAD_WIDTH
            query = plain[:, lo : lo + PLAIN_HEAD_WIDTH]
            query_rot = turned[:, h * QK_ROPE : (h + 1) * QK_ROPE]
            keys = kv_ref[:, lo : lo + PLAIN_HEAD_WIDTH]
            rotary = jnp.concatenate(
                (
                    lax.dot_general(query_rot, near_rot, last, preferred_element_type=jnp.float32),
                    lax.dot_general(query_rot, other_rot, last, preferred_element_type=jnp.float32),
                ),
                axis=1,
            )
            scores = (
                lax.dot_general(query, keys, last, preferred_element_type=jnp.float32) + rotary
            ) * scale
            peak = jnp.max(scores, axis=1, keepdims=True)
            weights = jnp.exp(scores - peak)
            total = jnp.sum(weights, axis=1, keepdims=True)
            head_values = kv_ref[:, value_wide + lo : value_wide + lo + VALUE_WIDTH]
            summed = jnp.dot(
                weights.astype(jnp.bfloat16), head_values, preferred_element_type=jnp.float32
            )
            result = (summed / total).astype(jnp.bfloat16)
            head = j * heads + h
            for i in range(shards):
                out_ref[i, :, head * VALUE_WIDTH : (head + 1) * VALUE_WIDTH] = result[
                    i * quarter : (i + 1) * quarter
                ]
            rest = peak + jnp.log(total)
            for part in range(3):
                top = rest.astype(jnp.bfloat16).astype(jnp.float32)
                rest = rest - top
                stats = jnp.where(lane == part * shards * heads + head, top, stats)
    stats = stats.astype(jnp.bfloat16)
    for i in range(shards):
        out_ref[i, :, shards * value_wide :] = stats[i * quarter : (i + 1) * quarter]


def mix_body(parts_ref, weight_ref, residual_ref, gain_ref, table_ref, hidden_ref, outgoing_ref):
    shards = parts_ref.shape[0]
    wide = weight_ref.shape[0]
    heads = wide // VALUE_WIDTH
    sums = []
    for i in range(shards):
        stat = parts_ref[i, :, wide:].astype(jnp.float32)
        sums.append(
            stat[:, :heads] + (stat[:, heads : 2 * heads] + stat[:, 2 * heads : 3 * heads])
        )
    most = sums[0]
    for s in sums[1:]:
        most = jnp.maximum(most, s)
    shares = [jnp.exp(s - most) for s in sums]
    whole = shares[0]
    for s in shares[1:]:
        whole = whole + s
    shares = [s / whole for s in shares]
    pieces = []
    for h in range(heads):
        lo = h * VALUE_WIDTH
        piece = shares[0][:, h : h + 1] * parts_ref[0, :, lo : lo + VALUE_WIDTH].astype(jnp.float32)
        for i in range(1, shards):
            piece = piece + shares[i][:, h : h + 1] * parts_ref[
                i, :, lo : lo + VALUE_WIDTH
            ].astype(jnp.float32)
        pieces.append(piece.astype(jnp.bfloat16))
    attended = jnp.concatenate(pieces, axis=1)
    projected = jnp.dot(attended, weight_ref[...], preferred_element_type=jnp.float32)
    hidden = (residual_ref[...].astype(jnp.float32) + projected).astype(jnp.bfloat16)
    hidden_ref[...] = hidden
    normed = norm_scale(hidden, gain_ref[...]).astype(jnp.bfloat16)
    outgoing_ref[...] = jnp.dot(
        table_ref[...], normed, preferred_element_type=jnp.float32
    ).astype(jnp.bfloat16)


def on_device(
    query_plain,
    query_turn,
    latent,
    key_turn,
    latent_norm_scale,
    plain_key_matrix,
    value_matrix,
    residual,
    out_weight,
    ffn_gain,
    gate_weight,
    up_weight,
    down_weight,
    routes,
    route_weights,
):
    tok_dev = latent.shape[0]
    rows_dev = residual.shape[0]
    model_width = residual.shape[1]
    latent_width = latent.shape[1]
    group = lax.axis_size("tp")
    heads_dev = query_plain.shape[1] // PLAIN_HEAD_WIDTH
    mine = lax.axis_index("tp") * rows_dev

    half = tok_dev // 2
    quarter = query_turn.shape[0] // (latent_width // query_turn.shape[1])
    share = jnp.concatenate(
        (
            jnp.concatenate((plain_key_matrix, value_matrix), axis=1),
            jnp.concatenate((query_plain[:half], query_plain[half:]), axis=1),
            jnp.concatenate(
                [query_turn[i * quarter : (i + 1) * quarter] for i in range(tok_dev // quarter)],
                axis=1,
            ),
        ),
        axis=0,
    )
    shares = lax.all_to_all(
        jnp.broadcast_to(share[None], (group,) + share.shape), "tp", 0, 0, tiled=True
    )

    place = lax.axis_index(SP) * tok_dev + jnp.arange(tok_dev, dtype=jnp.int32)
    cosines, sines = turn_tables(place)
    own_cos = lax.dynamic_slice_in_dim(cosines, mine, rows_dev, 0)
    own_sin = lax.dynamic_slice_in_dim(sines, mine, rows_dev, 0)
    own_latent = lax.dynamic_slice_in_dim(latent, mine, rows_dev, 0)
    own_key = lax.dynamic_slice_in_dim(key_turn, mine, rows_dev, 0)
    normed_latent = norm_scale(own_latent, latent_norm_scale).astype(jnp.bfloat16)
    swap_key = jnp.asarray(partner_matrix(QK_ROPE), jnp.bfloat16)
    key_rot = (
        own_key.astype(jnp.float32) * own_cos
        + jnp.dot(own_key, swap_key, preferred_element_type=jnp.float32) * own_sin
    ).astype(jnp.bfloat16)
    sent = jnp.concatenate((normed_latent, key_rot, jnp.zeros_like(key_rot)), axis=1)
    near = lax.all_gather(sent, "sp_0", axis=0, tiled=True)
    other = shifted(near, "sp_1", 1)

    parts = pl.pallas_call(
        attend_body,
        out_shape=jax.ShapeDtypeStruct(
            (group, rows_dev, group * heads_dev * VALUE_WIDTH + STAT_LANES), jnp.bfloat16
        ),
        scratch_shapes=[pltpu.VMEM((2 * near.shape[0], 2 * heads_dev * VALUE_WIDTH), jnp.bfloat16)],
        compiler_params=pltpu.CompilerParams(vmem_limit_bytes=24 << 20),
        name="attend",
    )(
        near,
        other,
        shares,
        jnp.concatenate([cosines] * heads_dev, axis=1),
        jnp.concatenate([sines] * heads_dev, axis=1),
        jnp.asarray(partner_matrix(heads_dev * QK_ROPE), jnp.bfloat16),
    )
    gathered = lax.all_to_all(parts, "tp", 0, 0, tiled=True)

    top_count = routes.shape[1]
    experts_all = lax.axis_size(SP) * gate_weight.shape[0]
    capacity = min(rows_dev, max(2, rows_dev * top_count * 3 // (2 * experts_all)))
    flat_routes = routes.reshape(rows_dev * top_count)
    marks = (flat_routes[:, None] == jnp.arange(experts_all, dtype=jnp.int32)[None, :]).astype(
        jnp.int32
    )
    earlier = jnp.cumsum(marks, axis=0, dtype=jnp.int32) - marks
    slots = jnp.sum(earlier * marks, axis=1, dtype=jnp.int32)
    target = flat_routes * capacity + slots
    chosen = (
        target.reshape(rows_dev, top_count)[None, :, :]
        == jnp.arange(experts_all * capacity, dtype=jnp.int32)[:, None, None]
    )
    dispatch_table = jnp.sum(chosen.astype(jnp.bfloat16), axis=2)

    hidden, outgoing = pl.pallas_call(
        mix_body,
        out_shape=(
            jax.ShapeDtypeStruct((rows_dev, model_width), jnp.bfloat16),
            jax.ShapeDtypeStruct((experts_all * capacity, model_width), jnp.bfloat16),
        ),
        compiler_params=pltpu.CompilerParams(vmem_limit_bytes=16 << 20),
        name="mix",
    )(gathered, out_weight, residual, ffn_gain.reshape(1, model_width), dispatch_table)
    arrived = lax.all_to_all(
        outgoing.reshape(experts_all, capacity, model_width), SP, 0, 0, tiled=True
    )

    own = (gate_weight[0], up_weight[0], down_weight[0])
    left, right = [], []
    for w in own:
        left.append(shifted(w, "tp", 1))
        right.append(shifted(w, "tp", -1))
    cut = own[2].shape[0] // 2
    far_gate = shifted(left[0], "tp", 1)
    far_up = shifted(right[1], "tp", -1)
    far_down_l = shifted(left[2][:cut], "tp", 1)
    far_down_r = shifted(right[2][cut:], "tp", -1)
    far = (far_gate, far_up, jnp.concatenate((far_down_l, far_down_r), axis=0))

    result_rows = expert_whole(
        arrived.reshape(experts_all * capacity, model_width), (own, left, right, far)
    )
    returned = lax.all_to_all(
        result_rows.reshape(experts_all, capacity, model_width), SP, 0, 0, tiled=True
    )
    picked = returned.reshape(experts_all * capacity, model_width)[target]
    picked = picked.reshape(rows_dev, top_count, model_width).astype(jnp.float32)
    return (
        hidden.astype(jnp.float32) + jnp.sum(route_weights[..., None] * picked, axis=1)
    ).astype(jnp.bfloat16)


def solution(mesh):
    torus = Mesh(
        mesh.devices.reshape(mesh.shape["grp"], 16, 2, mesh.shape["tp"]),
        ("grp", "sp_0", "sp_1", "tp"),
    )
    placed = (
        P(GRP_SP, "tp"),
        P(GRP_SP, "tp"),
        P(GRP_SP, None),
        P(GRP_SP, None),
        P(),
        P(None, "tp"),
        P(None, "tp"),
        P(GRP_SP_TP, None),
        P(),
        P(),
        P(SP, None, "tp"),
        P(SP, None, "tp"),
        P(SP, "tp", None),
        P(GRP_SP_TP, None),
        P(GRP_SP_TP, None),
    )
    return jax.shard_map(
        on_device, mesh=torus, in_specs=placed, out_specs=P(GRP_SP_TP, None), check_vma=False
    )
```

time: 312 us -> 305 us (0.978); the launches traced: 311 us -> 301 us
  blocking collectives: 120 us -> 35.5 us
  starting transfers between devices: 17.2 us -> 58.8 us
  waiting for transfers between devices: 109 us -> 135 us
  local copies, waits for them, and re-layouts: 10.8 us -> 26.6 us
  between operations: 13.9 us -> 0.35 us
  Pallas kernels: 0 us -> 10.9 us
  matrix products: 29.9 us -> 22.3 us
    ppermute x0 -> x11, waiting for transfers between devices: none -> 71.3 us  [shifted(): lax.ppermute(array, axis, [(i, (i + step) % count) for i in range(count)])]
    all_to_all x2 -> x0, blocking collectives: 67.7 us -> none  [the longest x1 63.2 us: on_device(): lax.all_to_all(outgoing, SP, split_axis=0, concat_axis=0, tiled=True)]
    all_gather x2 -> x0, waiting for transfers between devices: 60.3 us -> none  [the longest x1 38.2 us: turned_gather(): lax.all_gather(both, axis, axis=0, tiled=True)]
    all_to_all x2 -> x4, starting transfers between devices: 17.1 us -> 45.7 us  [the longest x1 23.1 us: on_device(): lax.all_to_all(jnp.broadcast_to(share[None], (group,) + share.shape), 'tp...]
    all_gather x1, blocking collectives: 52.1 us -> 35.5 us  [on_device(): near = lax.all_gather(sent, 'sp_0', axis=0, tiled=True)]
    all_to_all x2 -> x4, waiting for transfers between devices: 48.6 us -> 63.7 us  [the longest x1 55.1 us: on_device(): lax.all_to_all(result_rows.reshape(experts_all, capacity, model_width), S...]
    ppermute x0 -> x11, starting transfers between devices: none -> 13.1 us  [shifted(): lax.ppermute(array, axis, [(i, (i + step) % count) for i in range(count)])]
    dot_general x15 -> x5, matrix products: 26.4 us -> 15.1 us  [the longest x4 14.9 us: expert_whole(): product = jnp.dot(active, down_w, preferred_element_type=jnp.float32)]
  transfers between devices with their start and end apart: 4 -> 15, of which waited for: 4 -> 8; matrix products, arithmetic and copies ran while one was open for 8% -> 12% of each run, Pallas kernels for 0% -> 0%
where the time goes in v1:
time: 305 us; the launch traced here: 301 us
  waiting for transfers between devices  135 us (44%)
  starting transfers between devices  58.8 us (19%)
  blocking collectives  35.5 us (12%)
  local copies, waits for them, and re-layouts  26.6 us (9%)
  matrix products  22.3 us (7%)
  other arithmetic  11.1 us (4%)
  Pallas kernels  10.9 us (4%)
    ppermute x11, waiting for transfers between devices, shifted(): lax.ppermute(array, axis, [(i, (i + step) % count) for i in range(count)])  71.3 us
    all_to_all x1, waiting for transfers between devices, on_device(): lax.all_to_all(result_rows.reshape(experts_all, capacity, model_width), S...  55.1 us
    all_gather x1, blocking collectives, on_device(): near = lax.all_gather(sent, 'sp_0', axis=0, tiled=True)  35.5 us
    all_to_all x1, starting transfers between devices, on_device(): lax.all_to_all(jnp.broadcast_to(share[None], (group,) + share.shape), 'tp...  23.1 us
    dot_general x4, matrix products, expert_whole(): product = jnp.dot(active, down_w, preferred_element_type=jnp.float32)  14.9 us
    ppermute x11, starting transfers between devices, shifted(): lax.ppermute(array, axis, [(i, (i + step) % count) for i in range(count)])  13.1 us
    all_to_all x1, starting transfers between devices, on_device(): lax.all_to_all(result_rows.reshape(experts_all, capacity, model_width), S...  13 us
    pallas_call x1, Pallas kernels, on_device(): pl.pallas_call(attend_body, out_shape=jax.ShapeDtypeStruct((group, rows_d...  9.35 us
  transfers between devices with their start and end apart: 15, of which 8 were waited for; matrix products, arithmetic and copies ran while one was open for 12% of the time, Pallas kernels for 0%

profile of v1, /device:TPU:34, one launch (start us, length us, event | category | flops | bytes accessed | tf_op | source)
XLA Modules:
  0.0 300.5 jit_solution(14137195679378205405)
XLA Ops:
  4.3 23.1 %all-to-all-start = ((bf16[4,632,512]{2,1,0:T(8,128)(2,1)}), bf16[4,632,512]{2,1,0:T(8,128)(2,1)S(1)}, u32[]{:S(2)}, u32[]{:S(2)}) async-start(bf16[4,632,512]{2,1,0:T(8,128)(2,1)} %broadcast_in_dim.5), calls=%async_computation | async-start | bytes 5177344 | tf_op jit(solution)/shard_map/all_to_all | solution.py:233
  29.0 35.5 %all_gather.3.near_ref = bf16[640,640]{1,0:T(8,128)(2,1)S(1)} all-gather(bf16[40,640]{1,0:T(8,128)(2,1)S(1)} %maximum_maximum_fusion.1), channel_id=1, replica_groups=mesh['grp'=2,'sp_0'=16,'sp_1'=2,'tp'=4] {'sp_0'}, dimensions={0}, use_global_device_ids=true | all-gather | bytes 870400 | tf_op jit(solution)/shard_map/all_gather | solution.py:250
  81.9 9.3 %attend.1 = bf16[4,40,1152]{2,1,0:T(8,128)(2,1)S(1)} custom-call(bf16[640,640]{1,0:T(8,128)(2,1)S(1)} %all_gather.3.near_ref, bf16[640,640]{1,0:T(8,128)(2,1)} %collective-permute-done.other_ref, bf16[4,632,512]{2,1,0:T(8,128)(2,1)S(1)} %all-to-all-done.shares_ref, f32[160,128]{1,0:T(8,128)S(1)} %concatenate.39.cos_ref, f32[160,128]{1,0:T(8,128)S(1)} %copy-done.3, ...), custom_call_target="tpu_custom_call" | custom-call | tf_op jit(solution)/shard_map/attend/pallas_call | solution.py:253
  92.0 4.7 %all-to-all-start.1 = ((bf16[4,40,1152]{2,1,0:T(8,128)(2,1)}), bf16[4,40,1152]{2,1,0:T(8,128)(2,1)S(1)}, u32[]{:S(2)}, u32[]{:S(2)}) async-start(bf16[4,40,1152]{2,1,0:T(8,128)(2,1)} %copy-done.2), calls=%async_computation.1 | async-start | bytes 737280 | tf_op jit(solution)/shard_map/all_to_all | solution.py:269
  98.5 5.3 %all-to-all-done.1.parts_ref = bf16[4,40,1152]{2,1,0:T(8,128)(2,1)S(1)} async-done(((bf16[4,40,1152]{2,1,0:T(8,128)(2,1)}), bf16[4,40,1152]{2,1,0:T(8,128)(2,1)S(1)}, u32[]{:S(2)}, u32[]{:S(2)}) %all-to-all-start.1) | async-done | bytes 368672 | tf_op jit(solution)/shard_map/all_to_all | solution.py:269
  103.7 2.2 copy-done.1
  109.8 4.8 %all-to-all-start.2 = ((bf16[32,7,2048]{2,1,0:T(8,128)(2,1)}), bf16[32,7,2048]{2,1,0:T(8,128)(2,1)S(1)}, u32[]{:S(2)}, u32[]{:S(2)}) async-start(bf16[32,7,2048]{2,1,0:T(8,128)(2,1)} %reshape.119), calls=%async_computation.2 | async-start | bytes 2097152 | tf_op jit(solution)/shard_map/all_to_all | solution.py:296
  116.9 2.5 collective-permute-start.4
  119.4 21.6 %collective-permute-done.2 = bf16[2048,256]{1,0:T(8,128)(2,1)} collective-permute-done((bf16[2048,256]{1,0:T(8,128)(2,1)}, bf16[2048,256]{1,0:T(8,128)(2,1)}, u32[]{:S(2)}, u32[]{:S(2)}) %collective-permute-start.2) | collective-permute-done | bytes 1048608 | tf_op jit(solution)/shard_map/ppermute | solution.py:58
  144.7 18.7 %collective-permute-done.3 = bf16[256,2048]{1,0:T(8,128)(2,1)S(1)} collective-permute-done((bf16[256,2048]{1,0:T(8,128)(2,1)S(1)}, bf16[256,2048]{1,0:T(8,128)(2,1)S(1)}, u32[]{:S(2)}, u32[]{:S(2)}) %collective-permute-start.3) | collective-permute-done | bytes 1048608 | tf_op jit(solution)/shard_map/ppermute | solution.py:58
  163.4 2.7 collective-permute-start.10
  167.0 3.4 %all-to-all-done.2 = bf16[32,7,2048]{2,1,0:T(8,128)(2,1)S(1)} async-done(((bf16[32,7,2048]{2,1,0:T(8,128)(2,1)}), bf16[32,7,2048]{2,1,0:T(8,128)(2,1)S(1)}, u32[]{:S(2)}, u32[]{:S(2)}) %all-to-all-start.2) | async-done | bytes 917536 | tf_op jit(solution)/shard_map/all_to_all | solution.py:296
  174.1 12.0 %collective-permute-done.8 = bf16[2048,256]{1,0:T(8,128)(2,1)} collective-permute-done((bf16[2048,256]{1,0:T(8,128)(2,1)}, bf16[2048,256]{1,0:T(8,128)(2,1)}, u32[]{:S(2)}, u32[]{:S(2)}) %collective-permute-start.8) | collective-permute-done | bytes 1048608 | tf_op jit(solution)/shard_map/ppermute | solution.py:58
  186.0 2.7 collective-permute-start.7
  188.7 2.3 convolution_minimum_fusion
  191.0 2.7 fusion.7
  195.4 13.1 %collective-permute-done.1 = bf16[2048,256]{1,0:T(8,128)(2,1)} collective-permute-done((bf16[2048,256]{1,0:T(8,128)(2,1)}, bf16[2048,256]{1,0:T(8,128)(2,1)}, u32[]{:S(2)}, u32[]{:S(2)}) %collective-permute-start.1) | collective-permute-done | bytes 1048608 | tf_op jit(solution)/shard_map/ppermute | solution.py:58
  208.5 4.0 %fusion.6 = f32[224,2048]{1,0:T(8,128)} fusion(f32[224,2048]{1,0:T(8,128)S(1)} %fusion.7, bf16[256,2048]{1,0:T(8,128)(2,1)} %copy-done.11, f32[224,256]{1,0:T(8,128)S(1)} %convolution_minimum_fusion.2, bf16[224,2048]{1,0:T(8,128)(2,1)S(1)} %reshape.120, bf16[2048,256]{1,0:T(8,128)(2,1)} %collective-permute-done.1), kind=kOutput, calls=%fused_computation.10 | convolution fusion | flops 471654400 | bytes 6914048 | tf_op jit(solution)/shard_map/dot_general | solution.py:71
  212.5 5.8 %collective-permute-done.9 = bf16[128,2048]{1,0:T(8,128)(2,1)} collective-permute-done((bf16[128,2048]{1,0:T(8,128)(2,1)}, bf16[128,2048]{1,0:T(8,128)(2,1)}, u32[]{:S(2)}, u32[]{:S(2)}) %collective-permute-start.9) | collective-permute-done | bytes 524320 | tf_op jit(solution)/shard_map/ppermute | solution.py:58
  218.2 4.0 %fusion = f32[224,2048]{1,0:T(8,128)} fusion(f32[224,256]{1,0:T(8,128)} %convolution_minimum_fusion, bf16[224,2048]{1,0:T(8,128)(2,1)S(1)} %reshape.120, bf16[2048,256]{1,0:T(8,128)(2,1)} %collective-permute-done.7, bf16[128,2048]{1,0:T(8,128)(2,1)} %collective-permute-done.10, bf16[128,2048]{1,0:T(8,128)(2,1)} %collective-permute-done.9), kind=kOutput, calls=%fused_computation.2 | convolution fusion | flops 473292800 | bytes 5079040 | tf_op jit(solution)/shard_map/dot_general | solution.py:71
  222.2 4.2 %fusion.4 = bf16[224,2048]{1,0:T(8,128)(2,1)} fusion(f32[224,2048]{1,0:T(8,128)} %fusion, f32[224,2048]{1,0:T(8,128)S(1)} %copy-done.6, bf16[256,2048]{1,0:T(8,128)(2,1)} %copy-done.12, f32[224,256]{1,0:T(8,128)S(1)} %convolution_minimum_fusion.1, bf16[224,2048]{1,0:T(8,128)(2,1)S(1)} %reshape.120, bf16[2048,256]{1,0:T(8,128)(2,1)} %collective-permute-done.4), kind=kOutput, calls=%fused_computation.7 | convolution fusion | flops 472571904 | bytes 7831552 | tf_op jit(solution)/shard_map/dot_general | solution.py:71
  226.4 2.3 reshape.121
  228.8 13.0 %all-to-all-start.3 = ((bf16[32,7,2048]{2,1,0:T(8,128)(2,1)}), bf16[32,7,2048]{2,1,0:T(8,128)(2,1)S(1)}, u32[]{:S(2)}, u32[]{:S(2)}) async-start(bf16[32,7,2048]{2,1,0:T(8,128)(2,1)} %reshape.121), calls=%async_computation.3 | async-start | bytes 2097152 | tf_op jit(solution)/shard_map/all_to_all | solution.py:315
  242.0 55.1 %all-to-all-done.3 = bf16[32,7,2048]{2,1,0:T(8,128)(2,1)S(1)} async-done(((bf16[32,7,2048]{2,1,0:T(8,128)(2,1)}), bf16[32,7,2048]{2,1,0:T(8,128)(2,1)S(1)}, u32[]{:S(2)}, u32[]{:S(2)}) %all-to-all-start.3) | async-done | bytes 917536 | tf_op jit(solution)/shard_map/all_to_all | solution.py:315
  (104 shorter events, 45.1 us)
Async XLA Ops:
  0.0 28.3 %copy-start = (bf16[160,64]{0,1:T(8,128)(2,1)S(1)}, bf16[160,64]{0,1:T(8,128)(2,1)}, u32[]{:S(2)}) copy-start(bf16[160,64]{0,1:T(8,128)(2,1)} %param.20) | copy-start | bytes 61444
  4.3 23.2 %copy-start.14 = (bf16[160,512]{1,0:T(8,128)(2,1)S(1)}, bf16[160,512]{1,0:T(8,128)(2,1)}, u32[]{:S(2)}) copy-start(bf16[160,512]{1,0:T(8,128)(2,1)} %param.19) | copy-start | bytes 491524
  4.3 24.2 %copy-start.18 = (bf16[512]{0:T(512)(128)(2,1)S(1)}, bf16[512]{0:T(512)(128)(2,1)}, u32[]{:S(2)}) copy-start(bf16[512]{0:T(512)(128)(2,1)} %param.21) | copy-start | bytes 3076
  4.3 24.3 %copy-start.15 = (bf16[64,64]{1,0:T(8,128)(2,1)S(1)}, bf16[64,64]{1,0:T(8,128)(2,1)}, u32[]{:S(2)}) copy-start(bf16[64,64]{1,0:T(8,128)(2,1)} %constant.88.clone) | copy-start | bytes 24580
  4.3 76.7 %all-to-all-start = ((bf16[4,632,512]{2,1,0:T(8,128)(2,1)}), bf16[4,632,512]{2,1,0:T(8,128)(2,1)S(1)}, u32[]{:S(2)}, u32[]{:S(2)}) async-start(bf16[4,632,512]{2,1,0:T(8,128)(2,1)} %broadcast_in_dim.5), calls=%async_computation | async-start | bytes 5177344 | tf_op jit(solution)/shard_map/all_to_all | solution.py:233
  27.6 53.4 %copy-start.5 = (bf16[128,128]{1,0:T(8,128)(2,1)S(1)}, bf16[128,128]{1,0:T(8,128)(2,1)}, u32[]{:S(2)}) copy-start(bf16[128,128]{1,0:T(8,128)(2,1)} %constant.89.clone.swap_ref) | copy-start | bytes 98308
  64.6 16.5 %collective-permute-start = (bf16[640,640]{1,0:T(8,128)(2,1)S(1)}, bf16[640,640]{1,0:T(8,128)(2,1)}, u32[]{:S(2)}, u32[]{:S(2)}) collective-permute-start(bf16[640,640]{1,0:T(8,128)(2,1)S(1)} %all_gather.3.near_ref), channel_id=1, source_target_pairs={{0,4},{4,0},{1,5},{5,1},{2,6},{6,2},{3,7},{7,3},{8,12},{12,8},{9,1... | collective-permute-start | bytes 2457608 | tf_op jit(solution)/shard_map/ppermute | solution.py:58
  92.0 11.7 %all-to-all-start.1 = ((bf16[4,40,1152]{2,1,0:T(8,128)(2,1)}), bf16[4,40,1152]{2,1,0:T(8,128)(2,1)S(1)}, u32[]{:S(2)}, u32[]{:S(2)}) async-start(bf16[4,40,1152]{2,1,0:T(8,128)(2,1)} %copy-done.2), calls=%async_computation.1 | async-start | bytes 737280 | tf_op jit(solution)/shard_map/all_to_all | solution.py:269
  109.8 60.6 %all-to-all-start.2 = ((bf16[32,7,2048]{2,1,0:T(8,128)(2,1)}), bf16[32,7,2048]{2,1,0:T(8,128)(2,1)S(1)}, u32[]{:S(2)}, u32[]{:S(2)}) async-start(bf16[32,7,2048]{2,1,0:T(8,128)(2,1)} %reshape.119), calls=%async_computation.2 | async-start | bytes 2097152 | tf_op jit(solution)/shard_map/all_to_all | solution.py:296
  114.6 26.5 %collective-permute-start.2 = (bf16[2048,256]{1,0:T(8,128)(2,1)}, bf16[2048,256]{1,0:T(8,128)(2,1)}, u32[]{:S(2)}, u32[]{:S(2)}) collective-permute-start(bf16[2048,256]{1,0:T(8,128)(2,1)} %bitcast.45), channel_id=1, source_target_pairs={{0,1},{1,2},{2,3},{3,0},{4,5},{5,6},{6,7},{7,4},{8,9},{9,10},{10,1... | collective-permute-start | bytes 3145736 | tf_op jit(solution)/shard_map/ppermute | solution.py:58
  114.8 28.3 %collective-permute-start.6 = (bf16[256,2048]{1,0:T(8,128)(2,1)S(1)}, bf16[256,2048]{1,0:T(8,128)(2,1)S(1)}, u32[]{:S(2)}, u32[]{:S(2)}) collective-permute-start(bf16[256,2048]{1,0:T(8,128)(2,1)S(1)} %bitcast.41), channel_id=1, source_target_pairs={{0,3},{1,0},{2,1},{3,2},{4,7},{5,4},{6,5},{7,6},{8,11},{9,8},{10,9... | collective-permute-start | bytes 3145736 | tf_op jit(solution)/shard_map/ppermute | solution.py:58
  116.8 46.7 %collective-permute-start.3 = (bf16[256,2048]{1,0:T(8,128)(2,1)S(1)}, bf16[256,2048]{1,0:T(8,128)(2,1)S(1)}, u32[]{:S(2)}, u32[]{:S(2)}) collective-permute-start(bf16[256,2048]{1,0:T(8,128)(2,1)S(1)} %bitcast.42), channel_id=1, source_target_pairs={{0,1},{1,2},{2,3},{3,0},{4,5},{5,6},{6,7},{7,4},{8,9},{9,10},{10,1... | collective-permute-start | bytes 3145736 | tf_op jit(solution)/shard_map/ppermute | solution.py:58
  116.9 57.0 %collective-permute-start.4 = (bf16[2048,256]{1,0:T(8,128)(2,1)}, bf16[2048,256]{1,0:T(8,128)(2,1)}, u32[]{:S(2)}, u32[]{:S(2)}) collective-permute-start(bf16[2048,256]{1,0:T(8,128)(2,1)} %bitcast.43), channel_id=1, source_target_pairs={{0,3},{1,0},{2,1},{3,2},{4,7},{5,4},{6,5},{7,6},{8,11},{9,8},{10,9... | collective-permute-start | bytes 3145736 | tf_op jit(solution)/shard_map/ppermute | solution.py:58
  141.1 44.9 %collective-permute-start.8 = (bf16[2048,256]{1,0:T(8,128)(2,1)}, bf16[2048,256]{1,0:T(8,128)(2,1)}, u32[]{:S(2)}, u32[]{:S(2)}) collective-permute-start(bf16[2048,256]{1,0:T(8,128)(2,1)} %collective-permute-done.2), channel_id=1, source_target_pairs={{0,1},{1,2},{2,3},{3,0},{4,5},{5,6},{6,7},{7,4},{8,9},{9,10},{10,1... | collective-permute-start | bytes 3145736 | tf_op jit(solution)/shard_map/ppermute | solution.py:58
  141.1 67.4 %collective-permute-start.1 = (bf16[2048,256]{1,0:T(8,128)(2,1)}, bf16[2048,256]{1,0:T(8,128)(2,1)}, u32[]{:S(2)}, u32[]{:S(2)}) collective-permute-start(bf16[2048,256]{1,0:T(8,128)(2,1)} %bitcast.44), channel_id=1, source_target_pairs={{0,1},{1,2},{2,3},{3,0},{4,5},{5,6},{6,7},{7,4},{8,9},{9,10},{10,1... | collective-permute-start | bytes 3145736 | tf_op jit(solution)/shard_map/ppermute | solution.py:58
  143.1 23.0 %copy-start.12 = (bf16[256,2048]{1,0:T(8,128)(2,1)}, bf16[256,2048]{1,0:T(8,128)(2,1)S(1)}, u32[]{:S(2)}) copy-start(bf16[256,2048]{1,0:T(8,128)(2,1)S(1)} %collective-permute-done.6) | copy-start | bytes 3145732
  143.1 50.6 %collective-permute-start.5 = (bf16[2048,256]{1,0:T(8,128)(2,1)}, bf16[2048,256]{1,0:T(8,128)(2,1)}, u32[]{:S(2)}, u32[]{:S(2)}) collective-permute-start(bf16[2048,256]{1,0:T(8,128)(2,1)} %bitcast.46), channel_id=1, source_target_pairs={{0,3},{1,0},{2,1},{3,2},{4,7},{5,4},{6,5},{7,6},{8,11},{9,8},{10,9... | collective-permute-start | bytes 3145736 | tf_op jit(solution)/shard_map/ppermute | solution.py:58
  163.4 49.0 %collective-permute-start.10 = (bf16[128,2048]{1,0:T(8,128)(2,1)}, bf16[128,2048]{1,0:T(8,128)(2,1)}, u32[]{:S(2)}, u32[]{:S(2)}) collective-permute-start(bf16[128,2048]{1,0:T(8,128)(2,1)} %slice.49), channel_id=1, source_target_pairs={{0,3},{1,0},{2,1},{3,2},{4,7},{5,4},{6,5},{7,6},{8,11},{9,8},{10,9... | collective-permute-start | bytes 1572872 | tf_op jit(solution)/shard_map/ppermute | solution.py:58
  173.9 44.3 %collective-permute-start.9 = (bf16[128,2048]{1,0:T(8,128)(2,1)}, bf16[128,2048]{1,0:T(8,128)(2,1)}, u32[]{:S(2)}, u32[]{:S(2)}) collective-permute-start(bf16[128,2048]{1,0:T(8,128)(2,1)} %slice.48), channel_id=1, source_target_pairs={{0,1},{1,2},{2,3},{3,0},{4,5},{5,6},{6,7},{7,4},{8,9},{9,10},{10,1... | collective-permute-start | bytes 1572872 | tf_op jit(solution)/shard_map/ppermute | solution.py:58
  186.0 32.2 %collective-permute-start.7 = (bf16[2048,256]{1,0:T(8,128)(2,1)}, bf16[2048,256]{1,0:T(8,128)(2,1)}, u32[]{:S(2)}, u32[]{:S(2)}) collective-permute-start(bf16[2048,256]{1,0:T(8,128)(2,1)} %collective-permute-done.4), channel_id=1, source_target_pairs={{0,3},{1,0},{2,1},{3,2},{4,7},{5,4},{6,5},{7,6},{8,11},{9,8},{10,9... | collective-permute-start | bytes 3145736 | tf_op jit(solution)/shard_map/ppermute | solution.py:58
  212.5 9.7 %copy-start.6 = (f32[224,2048]{1,0:T(8,128)S(1)}, f32[224,2048]{1,0:T(8,128)}, u32[]{:S(2)}) copy-start(f32[224,2048]{1,0:T(8,128)} %fusion.6) | copy-start | bytes 5505028
  226.4 15.5 %copy-start.17 = (f32[40,4]{0,1:T(4,128)S(1)}, f32[40,4]{0,1:T(4,128)}, u32[]{:S(2)}) copy-start(f32[40,4]{0,1:T(4,128)} %param.31) | copy-start | bytes 1924
  226.4 15.6 %copy-start.16 = (s32[160]{0:T(256)S(1)}, s32[160]{0:T(256)}, u32[]{:S(2)}) copy-start(s32[160]{0:T(256)} %fusion.71) | copy-start | bytes 1924
  228.8 68.3 %all-to-all-start.3 = ((bf16[32,7,2048]{2,1,0:T(8,128)(2,1)}), bf16[32,7,2048]{2,1,0:T(8,128)(2,1)S(1)}, u32[]{:S(2)}, u32[]{:S(2)}) async-start(bf16[32,7,2048]{2,1,0:T(8,128)(2,1)} %reshape.121), calls=%async_computation.3 | async-start | bytes 2097152 | tf_op jit(solution)/shard_map/all_to_all | solution.py:315
  (10 other events, 16.4 us)

commit v2 on v1

--- a/solution.py
+++ b/solution.py
@@ -23,15 +23,14 @@
 STAT_LANES = 128
 
 
-def turn_tables(place):
+def turn_tables(place, heads):
     count = QK_ROPE // 4
-    freqs = theta ** (-jnp.arange(count, dtype=jnp.float32) / count)
-    halves_cos, halves_sin = [], []
-    for shift in (place // GRID_W, place % GRID_W):
-        angle = shift.astype(jnp.float32)[:, None] * freqs[None, :]
-        halves_cos += [jnp.cos(angle)] * 2
-        halves_sin += [jnp.sin(angle)] * 2
-    return jnp.concatenate(halves_cos, axis=1), jnp.concatenate(halves_sin, axis=1)
+    lane = jnp.arange(heads * QK_ROPE, dtype=jnp.int32)
+    freqs = theta ** (-(lane % count).astype(jnp.float32) / count)
+    by_row = (lane % QK_ROPE) < QK_ROPE // 2
+    shift = jnp.where(by_row[None, :], (place // GRID_W)[:, None], (place % GRID_W)[:, None])
+    angle = shift.astype(jnp.float32) * freqs[None, :]
+    return jnp.cos(angle), jnp.sin(angle)
 
 
 def partner_matrix(width):
@@ -58,19 +57,47 @@
     return lax.ppermute(array, axis, [(i, (i + step) % count) for i in range(count)])
 
 
-def expert_active(rows, gate_w, up_w):
-    gate_pre = jnp.minimum(jnp.dot(rows, gate_w, preferred_element_type=jnp.float32), limit)
-    up_pre = jnp.clip(jnp.dot(rows, up_w, preferred_element_type=jnp.float32), -limit, limit)
-    return ((up_pre + 1.0) * gate_pre * jax.nn.sigmoid(slope * gate_pre)).astype(jnp.bfloat16)
-
-
-def expert_whole(rows, quarters):
-    total = jnp.zeros((rows.shape[0], quarters[0][2].shape[1]), jnp.float32)
-    for gate_w, up_w, down_w in quarters:
-        active = expert_active(rows, gate_w, up_w)
-        product = jnp.dot(active, down_w, preferred_element_type=jnp.float32)
-        total = total + product.astype(jnp.bfloat16).astype(jnp.float32)
-    return total.astype(jnp.bfloat16)
+def prepare_body(
+    index_ref,
+    latent_ref,
+    gain_ref,
+    key_ref,
+    cos_ref,
+    sin_ref,
+    swap_ref,
+    key_matrix_ref,
+    value_matrix_ref,
+    plain_ref,
+    turn_ref,
+    sent_ref,
+    shares_ref,
+):
+    rows, latent_width = latent_ref.shape
+    sent_ref[:, :latent_width] = norm_scale(latent_ref[...], gain_ref[...]).astype(jnp.bfloat16)
+    tokens = key_ref.shape[1]
+    at = lax.broadcasted_iota(jnp.int32, (rows, tokens), 0) + index_ref[0] * rows
+    pick = (at == lax.broadcasted_iota(jnp.int32, (rows, tokens), 1)).astype(jnp.bfloat16)
+    key = lax.dot_general(
+        pick, key_ref[...], (((1,), (1,)), ((), ())), preferred_element_type=jnp.float32
+    )
+    swapped = jnp.dot(
+        key.astype(jnp.bfloat16), swap_ref[...], preferred_element_type=jnp.float32
+    )
+    turned = (key * cos_ref[...] + swapped * sin_ref[...]).astype(jnp.bfloat16)
+    sent_ref[:, latent_width:] = jnp.concatenate((turned, jnp.zeros_like(turned)), axis=1)
+    wide = key_matrix_ref.shape[1]
+    turn_wide = turn_ref.shape[1]
+    half = tokens // 2
+    quarter = tokens * turn_wide // (2 * wide)
+    for j in range(shares_ref.shape[0]):
+        shares_ref[j, :latent_width, :wide] = key_matrix_ref[...]
+        shares_ref[j, :latent_width, wide:] = value_matrix_ref[...]
+        shares_ref[j, latent_width : latent_width + half, :wide] = plain_ref[:half, :]
+        shares_ref[j, latent_width : latent_width + half, wide:] = plain_ref[half:, :]
+        for i in range(tokens // quarter):
+            shares_ref[
+                j, latent_width + half :, i * turn_wide : (i + 1) * turn_wide
+            ] = turn_ref[i * quarter : (i + 1) * quarter, :]
 
 
 def attend_body(near_ref, other_ref, shares_ref, cos_ref, sin_ref, swap_ref, out_ref, kv_ref):
@@ -155,8 +182,20 @@
         out_ref[i, :, shards * value_wide :] = stats[i * quarter : (i + 1) * quarter]
 
 
-def mix_body(parts_ref, weight_ref, residual_ref, gain_ref, table_ref, hidden_ref, outgoing_ref):
+GROUP = 8
+
+
+def lanes_of(index, width):
+    return slice(index * width, (index + 1) * width)
+
+
+def mix_body(
+    parts_ref, weight_hbm, residual_ref, gain_ref, routes_ref, hidden_ref, outgoing_ref, weight_ref, sem
+):
+    load = pltpu.make_async_copy(weight_hbm, weight_ref, sem)
+    load.start()
     shards = parts_ref.shape[0]
+    rows, model_width = residual_ref.shape
     wide = weight_ref.shape[0]
     heads = wide // VALUE_WIDTH
     sums = []
@@ -183,13 +222,132 @@
             ].astype(jnp.float32)
         pieces.append(piece.astype(jnp.bfloat16))
     attended = jnp.concatenate(pieces, axis=1)
+
+    total_rows = outgoing_ref.shape[0]
+    line = lax.broadcasted_iota(jnp.int32, (total_rows, rows), 0)
+    named = jnp.zeros((total_rows, rows), jnp.int32)
+    for k in range(routes_ref.shape[0]):
+        named = named | (routes_ref[k : k + 1, :] == line // GROUP).astype(jnp.int32)
+    before = (
+        lax.broadcasted_iota(jnp.int32, (rows, rows), 0)
+        < lax.broadcasted_iota(jnp.int32, (rows, rows), 1)
+    ).astype(jnp.bfloat16)
+    rank = jnp.dot(
+        named.astype(jnp.float32).astype(jnp.bfloat16), before, preferred_element_type=jnp.float32
+    ).astype(jnp.int32)
+    table = jnp.where((named > 0) & (rank == line % GROUP), 1.0, 0.0).astype(jnp.bfloat16)
+
+    load.wait()
     projected = jnp.dot(attended, weight_ref[...], preferred_element_type=jnp.float32)
     hidden = (residual_ref[...].astype(jnp.float32) + projected).astype(jnp.bfloat16)
     hidden_ref[...] = hidden
     normed = norm_scale(hidden, gain_ref[...]).astype(jnp.bfloat16)
-    outgoing_ref[...] = jnp.dot(
-        table_ref[...], normed, preferred_element_type=jnp.float32
+    tail = model_width - outgoing_ref.shape[1]
+    ends = normed[:, model_width - tail :]
+    for s in range(GROUP - 1):
+        of_last = jnp.where(
+            (named > 0) & (rank == s) & (line % GROUP == GROUP - 1), 1.0, 0.0
+        ).astype(jnp.bfloat16)
+        outgoing_ref[:, lanes_of(s, tail)] = (
+            jnp.dot(table, normed[:, lanes_of(s, tail)], preferred_element_type=jnp.float32)
+            + jnp.dot(of_last, ends, preferred_element_type=jnp.float32)
+        ).astype(jnp.bfloat16)
+
+
+def expert_body(arrived_ref, *refs):
+    count = (len(refs) - 4) // 3
+    weights_hbm = refs[: 3 * count]
+    out_ref, thin_ref, down_ref, sems = refs[3 * count :]
+    gate_up = weights_hbm[0].shape
+    loads = []
+    for q in range(count):
+        for m in range(3):
+            dst = down_ref.at[q] if m == 2 else thin_ref.at[q, m]
+            loads.append(pltpu.make_async_copy(weights_hbm[3 * q + m], dst, sems.at[q, m]))
+            loads[-1].start()
+    rows, main = arrived_ref.shape
+    model_width = gate_up[0]
+    tail = model_width - main
+    line = lax.broadcasted_iota(jnp.int32, (rows, rows), 0)
+    column = lax.broadcasted_iota(jnp.int32, (rows, rows), 1)
+    ends = jnp.zeros((rows, tail), jnp.float32)
+    for s in range(GROUP - 1):
+        pick = jnp.where(
+            (line % GROUP == s) & (column == line - s + GROUP - 1), 1.0, 0.0
+        ).astype(jnp.bfloat16)
+        ends = ends + jnp.dot(
+            pick, arrived_ref[:, lanes_of(s, tail)], preferred_element_type=jnp.float32
+        )
+    ends = ends.astype(jnp.bfloat16)
+    total = jnp.zeros((rows, model_width), jnp.float32)
+    for q in range(count):
+        loads[3 * q].wait()
+        gate_pre = jnp.dot(
+            arrived_ref[...], thin_ref[q, 0, :main, :], preferred_element_type=jnp.float32
+        ) + jnp.dot(ends, thin_ref[q, 0, main:, :], preferred_element_type=jnp.float32)
+        loads[3 * q + 1].wait()
+        up_pre = jnp.dot(
+            arrived_ref[...], thin_ref[q, 1, :main, :], preferred_element_type=jnp.float32
+        ) + jnp.dot(ends, thin_ref[q, 1, main:, :], preferred_element_type=jnp.float32)
+        gate_pre = jnp.minimum(gate_pre, limit)
+        active = (
+            (jnp.clip(up_pre, -limit, limit) + 1.0) * gate_pre * jax.nn.sigmoid(slope * gate_pre)
+        ).astype(jnp.bfloat16)
+        loads[3 * q + 2].wait()
+        product = jnp.dot(active, down_ref[q], preferred_element_type=jnp.float32)
+        total = total + product.astype(jnp.bfloat16).astype(jnp.float32)
+    result = total.astype(jnp.bfloat16)
+    last = result[:, main:]
+    group_end = lax.broadcasted_iota(jnp.int32, (rows, tail), 0) % GROUP == GROUP - 1
+    for s in range(GROUP - 1):
+        pick = jnp.where(
+            (line % GROUP == GROUP - 1) & (column == line - (GROUP - 1) + s), 1.0, 0.0
+        ).astype(jnp.bfloat16)
+        moved = jnp.dot(pick, last, preferred_element_type=jnp.float32).astype(jnp.bfloat16)
+        out_ref[:, lanes_of(s, tail)] = jnp.where(
+            group_end, moved.astype(jnp.float32), result[:, lanes_of(s, tail)].astype(jnp.float32)
+        ).astype(jnp.bfloat16)
+
+
+def combine_body(returned_ref, hidden_ref, routes_ref, weights_ref, out_ref):
+    rows, model_width = hidden_ref.shape
+    total_rows, main = returned_ref.shape
+    tail = model_width - main
+    column = lax.broadcasted_iota(jnp.int32, (rows, total_rows), 1)
+    named = jnp.zeros((rows, total_rows), jnp.float32)
+    weight = jnp.zeros((rows, total_rows), jnp.float32)
+    for k in range(routes_ref.shape[1]):
+        here = routes_ref[:, k : k + 1] == column // GROUP
+        named = jnp.where(here, 1.0, named)
+        weight = jnp.where(here, weights_ref[:, k : k + 1], weight)
+    before = (
+        lax.broadcasted_iota(jnp.int32, (rows, rows), 1)
+        < lax.broadcasted_iota(jnp.int32, (rows, rows), 0)
     ).astype(jnp.bfloat16)
+    rank = jnp.dot(
+        before, named.astype(jnp.bfloat16), preferred_element_type=jnp.float32
+    ).astype(jnp.int32)
+    parts = []
+    rest = weight
+    for _ in range(3):
+        top = rest.astype(jnp.bfloat16).astype(jnp.float32)
+        rest = rest - top
+        parts.append(top)
+
+    def gathered(keep, values):
+        table = jnp.concatenate([jnp.where(keep, p, 0.0) for p in parts], axis=0)
+        got = jnp.dot(table.astype(jnp.bfloat16), values, preferred_element_type=jnp.float32)
+        return got[:rows] + (got[rows : 2 * rows] + got[2 * rows :])
+
+    own = (named > 0) & (rank == column % GROUP)
+    out_ref[:, :main] = (
+        hidden_ref[:, :main].astype(jnp.float32) + gathered(own, returned_ref[...])
+    ).astype(jnp.bfloat16)
+    ends = jnp.zeros((rows, tail), jnp.float32)
+    for s in range(GROUP - 1):
+        keep = (named > 0) & (rank == s) & (column % GROUP == GROUP - 1)
+        ends = ends + gathered(keep, returned_ref[:, lanes_of(s, tail)])
+    out_ref[:, main:] = (hidden_ref[:, main:].astype(jnp.float32) + ends).astype(jnp.bfloat16)
 
 
 def on_device(
@@ -215,38 +373,60 @@
     latent_width = latent.shape[1]
     group = lax.axis_size("tp")
     heads_dev = query_plain.shape[1] // PLAIN_HEAD_WIDTH
-    mine = lax.axis_index("tp") * rows_dev
-
-    half = tok_dev // 2
-    quarter = query_turn.shape[0] // (latent_width // query_turn.shape[1])
-    share = jnp.concatenate(
-        (
-            jnp.concatenate((plain_key_matrix, value_matrix), axis=1),
-            jnp.concatenate((query_plain[:half], query_plain[half:]), axis=1),
-            jnp.concatenate(
-                [query_turn[i * quarter : (i + 1) * quarter] for i in range(tok_dev // quarter)],
-                axis=1,
+    place = lax.axis_index(SP) * tok_dev + jnp.arange(tok_dev, dtype=jnp.int32)
+    at_tp = lax.axis_index("tp")
+    own_place = (
+        lax.axis_index(SP) * tok_dev
+        + at_tp * rows_dev
+        + jnp.arange(rows_dev, dtype=jnp.int32)
+    )
+    own_cos, own_sin = turn_tables(own_place, 1)
+    cosines, sines = turn_tables(place, heads_dev)
+    share_rows = latent_width + tok_dev // 2 + tok_dev * query_turn.shape[1] // latent_width
+    wide = plain_key_matrix.shape[1]
+    whole = lambda *shape: pl.BlockSpec(shape, lambda i, at: (0,) * len(shape))
+    sent, shares = pl.pallas_call(
+        prepare_body,
+        out_shape=(
+            jax.ShapeDtypeStruct((rows_dev, latent_width + 2 * QK_ROPE), jnp.bfloat16),
+            jax.ShapeDtypeStruct((group, share_rows, latent_width), jnp.bfloat16),
+        ),
+        grid_spec=pltpu.PrefetchScalarGridSpec(
+            num_scalar_prefetch=1,
+            grid=(1,),
+            in_specs=[
+                pl.BlockSpec((rows_dev, latent_width), lambda i, at: (at[0], 0)),
+                whole(1, latent_width),
+                whole(QK_ROPE, tok_dev),
+                whole(rows_dev, QK_ROPE),
+                whole(rows_dev, QK_ROPE),
+                whole(QK_ROPE, QK_ROPE),
+                whole(latent_width, wide),
+                whole(latent_width, wide),
+                whole(tok_dev, query_plain.shape[1]),
+                whole(tok_dev, query_turn.shape[1]),
+            ],
+            out_specs=(
+                whole(rows_dev, latent_width + 2 * QK_ROPE),
+                whole(group, share_rows, latent_width),
             ),
         ),
-        axis=0,
-    )
-    shares = lax.all_to_all(
-        jnp.broadcast_to(share[None], (group,) + share.shape), "tp", 0, 0, tiled=True
-    )
-
-    place = lax.axis_index(SP) * tok_dev + jnp.arange(tok_dev, dtype=jnp.int32)
-    cosines, sines = turn_tables(place)
-    own_cos = lax.dynamic_slice_in_dim(cosines, mine, rows_dev, 0)
-    own_sin = lax.dynamic_slice_in_dim(sines, mine, rows_dev, 0)
-    own_latent = lax.dynamic_slice_in_dim(latent, mine, rows_dev, 0)
-    own_key = lax.dynamic_slice_in_dim(key_turn, mine, rows_dev, 0)
-    normed_latent = norm_scale(own_latent, latent_norm_scale).astype(jnp.bfloat16)
-    swap_key = jnp.asarray(partner_matrix(QK_ROPE), jnp.bfloat16)
-    key_rot = (
-        own_key.astype(jnp.float32) * own_cos
-        + jnp.dot(own_key, swap_key, preferred_element_type=jnp.float32) * own_sin
-    ).astype(jnp.bfloat16)
-    sent = jnp.concatenate((normed_latent, key_rot, jnp.zeros_like(key_rot)), axis=1)
+        compiler_params=pltpu.CompilerParams(vmem_limit_bytes=16 << 20),
+        name="prepare",
+    )(
+        at_tp.reshape(1),
+        latent,
+        latent_norm_scale.reshape(1, latent_width),
+        key_turn.T,
+        own_cos,
+        own_sin,
+        jnp.asarray(partner_matrix(QK_ROPE), jnp.bfloat16),
+        plain_key_matrix,
+        value_matrix,
+        query_plain,
+        query_turn,
+    )
+    shares = lax.all_to_all(shares, "tp", 0, 0, tiled=True)
     near = lax.all_gather(sent, "sp_0", axis=0, tiled=True)
     other = shifted(near, "sp_1", 1)
 
@@ -262,40 +442,31 @@
         near,
         other,
         shares,
-        jnp.concatenate([cosines] * heads_dev, axis=1),
-        jnp.concatenate([sines] * heads_dev, axis=1),
+        cosines,
+        sines,
         jnp.asarray(partner_matrix(heads_dev * QK_ROPE), jnp.bfloat16),
     )
     gathered = lax.all_to_all(parts, "tp", 0, 0, tiled=True)
 
+    experts_all = lax.axis_size(SP) * gate_weight.shape[0]
     top_count = routes.shape[1]
-    experts_all = lax.axis_size(SP) * gate_weight.shape[0]
     capacity = min(rows_dev, max(2, rows_dev * top_count * 3 // (2 * experts_all)))
-    flat_routes = routes.reshape(rows_dev * top_count)
-    marks = (flat_routes[:, None] == jnp.arange(experts_all, dtype=jnp.int32)[None, :]).astype(
-        jnp.int32
-    )
-    earlier = jnp.cumsum(marks, axis=0, dtype=jnp.int32) - marks
-    slots = jnp.sum(earlier * marks, axis=1, dtype=jnp.int32)
-    target = flat_routes * capacity + slots
-    chosen = (
-        target.reshape(rows_dev, top_count)[None, :, :]
-        == jnp.arange(experts_all * capacity, dtype=jnp.int32)[:, None, None]
-    )
-    dispatch_table = jnp.sum(chosen.astype(jnp.bfloat16), axis=2)
-
+    assert capacity == GROUP - 1
+    main = model_width * capacity // GROUP
+    vmem = pl.BlockSpec(memory_space=pltpu.VMEM)
+    hbm = pl.BlockSpec(memory_space=pltpu.HBM)
     hidden, outgoing = pl.pallas_call(
         mix_body,
         out_shape=(
             jax.ShapeDtypeStruct((rows_dev, model_width), jnp.bfloat16),
-            jax.ShapeDtypeStruct((experts_all * capacity, model_width), jnp.bfloat16),
+            jax.ShapeDtypeStruct((experts_all * GROUP, main), jnp.bfloat16),
         ),
+        in_specs=[vmem, hbm, vmem, vmem, vmem],
+        scratch_shapes=[pltpu.VMEM(out_weight.shape, jnp.bfloat16), pltpu.SemaphoreType.DMA],
         compiler_params=pltpu.CompilerParams(vmem_limit_bytes=16 << 20),
         name="mix",
-    )(gathered, out_weight, residual, ffn_gain.reshape(1, model_width), dispatch_table)
-    arrived = lax.all_to_all(
-        outgoing.reshape(experts_all, capacity, model_width), SP, 0, 0, tiled=True
-    )
+    )(gathered, out_weight, residual, ffn_gain.reshape(1, model_width), routes.T)
+    arrived = lax.all_to_all(outgoing.reshape(experts_all, GROUP, main), SP, 0, 0, tiled=True)
 
     own = (gate_weight[0], up_weight[0], down_weight[0])
     left, right = [], []
@@ -309,17 +480,28 @@
     far_down_r = shifted(right[2][cut:], "tp", -1)
     far = (far_gate, far_up, jnp.concatenate((far_down_l, far_down_r), axis=0))
 
-    result_rows = expert_whole(
-        arrived.reshape(experts_all * capacity, model_width), (own, left, right, far)
-    )
-    returned = lax.all_to_all(
-        result_rows.reshape(experts_all, capacity, model_width), SP, 0, 0, tiled=True
-    )
-    picked = returned.reshape(experts_all * capacity, model_width)[target]
-    picked = picked.reshape(rows_dev, top_count, model_width).astype(jnp.float32)
-    return (
-        hidden.astype(jnp.float32) + jnp.sum(route_weights[..., None] * picked, axis=1)
-    ).astype(jnp.bfloat16)
+    weights = []
+    for gate_w, up_w, down_w in (own, left, right, far):
+        weights += [gate_w, up_w, down_w]
+    result_rows = pl.pallas_call(
+        expert_body,
+        out_shape=jax.ShapeDtypeStruct((experts_all * GROUP, main), jnp.bfloat16),
+        in_specs=[vmem] + [hbm] * len(weights),
+        scratch_shapes=[
+            pltpu.VMEM((group, 2) + own[0].shape, jnp.bfloat16),
+            pltpu.VMEM((group,) + own[2].shape, jnp.bfloat16),
+            pltpu.SemaphoreType.DMA((group, 3)),
+        ],
+        compiler_params=pltpu.CompilerParams(vmem_limit_bytes=40 << 20),
+        name="expert",
+    )(arrived.reshape(experts_all * GROUP, main), *weights)
+    returned = lax.all_to_all(result_rows.reshape(experts_all, GROUP, main), SP, 0, 0, tiled=True)
+    return pl.pallas_call(
+        combine_body,
+        out_shape=jax.ShapeDtypeStruct((rows_dev, model_width), jnp.bfloat16),
+        compiler_params=pltpu.CompilerParams(vmem_limit_bytes=16 << 20),
+        name="combine",
+    )(returned.reshape(experts_all * GROUP, main), hidden, routes, route_weights)
 
 
 def solution(mesh):

time: 305 us -> 301 us (0.987)
  matrix products: 22.3 us -> 0 us
  waiting for transfers between devices: 135 us -> 151 us
  Pallas kernels: 10.9 us -> 23.4 us
  other arithmetic: 11.1 us -> 1.33 us
    ppermute x11, waiting for transfers between devices: 71.3 us -> 94.9 us  [shifted(): lax.ppermute(array, axis, [(i, (i + step) % count) for i in range(count)])]
    dot_general x9 -> x0, matrix products: 22.3 us -> none  [the longest x4 14.9 us: expert_whole(): product = jnp.dot(active, down_w, preferred_element_type=jnp.float32)]
    unnamed x42 -> x70, local copies, waits for them, and re-layouts: 6.42 us -> 28.1 us
    pallas_call x0 -> x3, Pallas kernels: none -> 11.9 us  [the longest x1 10.4 us: on_device(): pl.pallas_call(expert_body, out_shape=jax.ShapeDtypeStruct((experts_all *...]
    all_to_all x3, waiting for transfers between devices: 58.4 us -> 49.6 us  [the longest x1 49.6 us: on_device(): lax.all_to_all(result_rows.reshape(experts_all, GROUP, main), SP, 0, 0, t...]
    another operation x4 -> x0, other arithmetic: 4.63 us -> none
    reshape x4 -> x1, local copies, waits for them, and re-layouts: 4.29 us -> 0.68 us  [on_device(): latent_norm_scale.reshape(1, latent_width)]
    concatenate x3 -> x0, local copies, waits for them, and re-layouts: 3.53 us -> none  [the longest x1 2.07 us: on_device(): jnp.concatenate([sines] * heads_dev, axis=1)]
  transfers between devices with their start and end apart: 15 -> 15, of which waited for: 8 -> 7; matrix products, arithmetic and copies ran while one was open for 12% -> 0% of each run, Pallas kernels for 0% -> 0%
where the time goes in v2:
time: 301 us; the launch traced here: 297 us
  waiting for transfers between devices  151 us (50%)
  starting transfers between devices  56.4 us (19%)
  blocking collectives  35.6 us (12%)
  local copies, waits for them, and re-layouts  28.9 us (10%)
  Pallas kernels  23.4 us (8%)
    ppermute x11, waiting for transfers between devices, shifted(): lax.ppermute(array, axis, [(i, (i + step) % count) for i in range(count)])  94.9 us
    all_to_all x1, waiting for transfers between devices, on_device(): lax.all_to_all(result_rows.reshape(experts_all, GROUP, main), SP, 0, 0, t...  49.6 us
    all_gather x1, blocking collectives, on_device(): near = lax.all_gather(sent, 'sp_0', axis=0, tiled=True)  35.6 us
    unnamed x70, local copies, waits for them, and re-layouts  28.1 us
    all_to_all x1, starting transfers between devices, on_device(): shares = lax.all_to_all(shares, 'tp', 0, 0, tiled=True)  23.1 us
    all_to_all x1, starting transfers between devices, on_device(): lax.all_to_all(result_rows.reshape(experts_all, GROUP, main), SP, 0, 0, t...  13 us
    ppermute x11, starting transfers between devices, shifted(): lax.ppermute(array, axis, [(i, (i + step) % count) for i in range(count)])  10.9 us
    pallas_call x1, Pallas kernels, on_device(): pl.pallas_call(expert_body, out_shape=jax.ShapeDtypeStruct((experts_all *...  10.4 us
  transfers between devices with their start and end apart: 15, of which 7 were waited for; matrix products, arithmetic and copies ran while one was open for 0% of the time, Pallas kernels for 0%

profile of v2, /device:TPU:34, one launch (start us, length us, event | category | flops | bytes accessed | tf_op | source)
XLA Modules:
  0.0 296.9 jit_solution(11015113902996620090)
XLA Ops:
  7.2 1.5 copy-done.1
  8.7 23.1 %all-to-all-start = ((bf16[4,632,512]{2,1,0:T(8,128)(2,1)}), bf16[4,632,512]{2,1,0:T(8,128)(2,1)S(1)}, u32[]{:S(2)}, u32[]{:S(2)}) async-start(bf16[4,632,512]{2,1,0:T(8,128)(2,1)} %copy-done.1), calls=%async_computation | async-start | bytes 5177344 | tf_op jit(solution)/shard_map/all_to_all | solution.py:429
  31.8 35.6 %all_gather.3.near_ref = bf16[640,640]{1,0:T(8,128)(2,1)S(1)} all-gather(bf16[40,640]{1,0:T(8,128)(2,1)S(1)} %get-tuple-element.9), channel_id=1, replica_groups=mesh['grp'=2,'sp_0'=16,'sp_1'=2,'tp'=4] {'sp_0'}, dimensions={0}, use_global_device_ids=true | all-gather | bytes 870400 | tf_op jit(solution)/shard_map/all_gather | solution.py:430
  68.5 1.2 collective-permute-done.other_ref
  72.7 8.2 %attend.1 = bf16[4,40,1152]{2,1,0:T(8,128)(2,1)S(1)} custom-call(bf16[640,640]{1,0:T(8,128)(2,1)S(1)} %all_gather.3.near_ref, bf16[640,640]{1,0:T(8,128)(2,1)S(1)} %copy-done.20, bf16[4,632,512]{2,1,0:T(8,128)(2,1)S(1)} %all-to-all-done.shares_ref, f32[160,128]{1,0:T(8,128)S(1)} %copy-done.21, f32[160,128]{1,0:T(8,128)S(1)} %get-tuple-element.13.sin_ref, ...), custom_call_target="tpu_custom_call" | custom-call | tf_op jit(solution)/shard_map/attend/pallas_call | solution.py:433
  81.6 4.5 %all-to-all-start.1 = ((bf16[4,40,1152]{2,1,0:T(8,128)(2,1)}), bf16[4,40,1152]{2,1,0:T(8,128)(2,1)S(1)}, u32[]{:S(2)}, u32[]{:S(2)}) async-start(bf16[4,40,1152]{2,1,0:T(8,128)(2,1)} %copy-done.4), calls=%async_computation.1 | async-start | bytes 737280 | tf_op jit(solution)/shard_map/all_to_all | solution.py:449
  86.1 6.6 %all-to-all-done.1.parts_ref = bf16[4,40,1152]{2,1,0:T(8,128)(2,1)S(1)} async-done(((bf16[4,40,1152]{2,1,0:T(8,128)(2,1)}), bf16[4,40,1152]{2,1,0:T(8,128)(2,1)S(1)}, u32[]{:S(2)}, u32[]{:S(2)}) %all-to-all-start.1) | async-done | bytes 368672 | tf_op jit(solution)/shard_map/all_to_all | solution.py:449
  92.8 2.2 copy-done
  95.9 3.3 %mix.1 = (bf16[40,2048]{1,0:T(8,128)(2,1)S(1)}, bf16[256,1792]{1,0:T(8,128)(2,1)}) custom-call(bf16[4,40,1152]{2,1,0:T(8,128)(2,1)S(1)} %all-to-all-done.1.parts_ref, bf16[1024,2048]{1,0:T(8,128)(2,1)S(1)} %copy-done, bf16[40,2048]{1,0:T(8,128)(2,1)S(1)} %copy-done.24, bf16[1,2048]{1,0:T(2,128)(2,1)S(1)} %reshape.133.gain_ref, s32[4,40]{1,0:T(4,128)S(1)} %bitcast.16), custom_call_target="tpu_custom_call" | custom-call | tf_op jit(solution)/shard_map/mix/pallas_call | solution.py:458
  99.1 4.8 %all-to-all-start.2 = ((bf16[32,8,1792]{2,1,0:T(8,128)(2,1)}), bf16[32,8,1792]{2,1,0:T(8,128)(2,1)S(1)}, u32[]{:S(2)}, u32[]{:S(2)}) async-start(bf16[32,8,1792]{2,1,0:T(8,128)(2,1)} %bitcast.3), calls=%async_computation.2 | async-start | bytes 1835008 | tf_op jit(solution)/shard_map/all_to_all | solution.py:469
  104.0 1.8 collective-permute-start.6
  106.4 1.9 collective-permute-start.5
  108.3 22.0 %collective-permute-done.6.refs_8_ = bf16[256,2048]{1,0:T(8,128)(2,1)S(1)} collective-permute-done((bf16[256,2048]{1,0:T(8,128)(2,1)S(1)}, bf16[256,2048]{1,0:T(8,128)(2,1)S(1)}, u32[]{:S(2)}, u32[]{:S(2)}) %collective-permute-start.6) | collective-permute-done | bytes 1048608 | tf_op jit(solution)/shard_map/ppermute | solution.py:57
  130.4 1.6 collective-permute-start.10
  132.5 1.9 collective-permute-start.4
  134.4 19.8 %collective-permute-done.1.refs_3_ = bf16[2048,256]{1,0:T(8,128)(2,1)S(1)} collective-permute-done((bf16[2048,256]{1,0:T(8,128)(2,1)}, bf16[2048,256]{1,0:T(8,128)(2,1)S(1)}, u32[]{:S(2)}, u32[]{:S(2)}) %collective-permute-start.1) | collective-permute-done | bytes 1048608 | tf_op jit(solution)/shard_map/ppermute | solution.py:57
  154.8 1.9 collective-permute-start.8
  156.8 7.2 %collective-permute-done.10 = bf16[128,2048]{1,0:T(8,128)(2,1)S(1)} collective-permute-done((bf16[128,2048]{1,0:T(8,128)(2,1)S(1)}, bf16[128,2048]{1,0:T(8,128)(2,1)S(1)}, u32[]{:S(2)}, u32[]{:S(2)}) %collective-permute-start.10) | collective-permute-done | bytes 524320 | tf_op jit(solution)/shard_map/ppermute | solution.py:57
  164.0 44.6 %collective-permute-done.9 = bf16[128,2048]{1,0:T(8,128)(2,1)S(1)} collective-permute-done((bf16[128,2048]{1,0:T(8,128)(2,1)S(1)}, bf16[128,2048]{1,0:T(8,128)(2,1)S(1)}, u32[]{:S(2)}, u32[]{:S(2)}) %collective-permute-start.9) | collective-permute-done | bytes 524320 | tf_op jit(solution)/shard_map/ppermute | solution.py:57
  212.7 1.2 copy-done.3
  222.5 10.4 %expert.1 = bf16[256,1792]{1,0:T(8,128)(2,1)} custom-call(bf16[256,1792]{1,0:T(8,128)(2,1)S(1)} %bitcast.10, bf16[2048,256]{1,0:T(8,128)(2,1)} %bitcast.5.refs_0_, bf16[2048,256]{1,0:T(8,128)(2,1)} %bitcast.6.refs_1_, bf16[256,2048]{1,0:T(8,128)(2,1)S(1)} %bitcast.14, bf16[2048,256]{1,0:T(8,128)(2,1)S(1)} %copy-done.8, bf16[2048,256]{1,0:T(8,128)(2,1)S(1)} %copy-done.12, ...), custom_call_target="tpu_custom_call" | custom-call | tf_op jit(solution)/shard_map/expert/pallas_call | solution.py:486
  232.9 13.0 %all-to-all-start.3 = ((bf16[32,8,1792]{2,1,0:T(8,128)(2,1)}), bf16[32,8,1792]{2,1,0:T(8,128)(2,1)S(1)}, u32[]{:S(2)}, u32[]{:S(2)}) async-start(bf16[32,8,1792]{2,1,0:T(8,128)(2,1)} %bitcast.8), calls=%async_computation.3 | async-start | bytes 1835008 | tf_op jit(solution)/shard_map/all_to_all | solution.py:498
  246.1 49.6 %all-to-all-done.3 = bf16[32,8,1792]{2,1,0:T(8,128)(2,1)S(1)} async-done(((bf16[32,8,1792]{2,1,0:T(8,128)(2,1)}), bf16[32,8,1792]{2,1,0:T(8,128)(2,1)S(1)}, u32[]{:S(2)}, u32[]{:S(2)}) %all-to-all-start.3) | async-done | bytes 917536 | tf_op jit(solution)/shard_map/all_to_all | solution.py:498
  295.6 1.3 combine.1
  (95 shorter events, 27.5 us)
Async XLA Ops:
  8.7 62.0 %copy-start.28 = (bf16[128,128]{1,0:T(8,128)(2,1)S(1)}, bf16[128,128]{1,0:T(8,128)(2,1)}, u32[]{:S(2)}) copy-start(bf16[128,128]{1,0:T(8,128)(2,1)} %constant.117.clone.swap_ref) | copy-start | bytes 98308
  8.7 62.0 %all-to-all-start = ((bf16[4,632,512]{2,1,0:T(8,128)(2,1)}), bf16[4,632,512]{2,1,0:T(8,128)(2,1)S(1)}, u32[]{:S(2)}, u32[]{:S(2)}) async-start(bf16[4,632,512]{2,1,0:T(8,128)(2,1)} %copy-done.1), calls=%async_computation | async-start | bytes 5177344 | tf_op jit(solution)/shard_map/all_to_all | solution.py:429
  67.4 2.3 collective-permute-start
  72.7 13.4 %copy-start.32 = (bf16[2048]{0:T(1024)(128)(2,1)S(1)}, bf16[2048]{0:T(1024)(128)(2,1)}, u32[]{:S(2)}) copy-start(bf16[2048]{0:T(1024)(128)(2,1)} %param.26) | copy-start | bytes 12292
  72.7 20.1 %copy-start.31 = (s32[40,4]{0,1:T(4,128)S(1)}, s32[40,4]{0,1:T(4,128)}, u32[]{:S(2)}) copy-start(s32[40,4]{0,1:T(4,128)} %param.30) | copy-start | bytes 1924
  81.6 11.1 %all-to-all-start.1 = ((bf16[4,40,1152]{2,1,0:T(8,128)(2,1)}), bf16[4,40,1152]{2,1,0:T(8,128)(2,1)S(1)}, u32[]{:S(2)}, u32[]{:S(2)}) async-start(bf16[4,40,1152]{2,1,0:T(8,128)(2,1)} %copy-done.4), calls=%async_computation.1 | async-start | bytes 737280 | tf_op jit(solution)/shard_map/all_to_all | solution.py:449
  92.8 2.2 copy-start
  95.9 8.1 %copy-start.5 = (bf16[1,256,2048]{2,1,0:T(8,128)(2,1)S(1)}, bf16[1,256,2048]{2,1,0:T(8,128)(2,1)}, u32[]{:S(2)}) copy-start(bf16[1,256,2048]{2,1,0:T(8,128)(2,1)} %param.29) | copy-start | bytes 3145732
  99.1 113.6 %all-to-all-start.2 = ((bf16[32,8,1792]{2,1,0:T(8,128)(2,1)}), bf16[32,8,1792]{2,1,0:T(8,128)(2,1)S(1)}, u32[]{:S(2)}, u32[]{:S(2)}) async-start(bf16[32,8,1792]{2,1,0:T(8,128)(2,1)} %bitcast.3), calls=%async_computation.2 | async-start | bytes 1835008 | tf_op jit(solution)/shard_map/all_to_all | solution.py:469
  104.0 26.3 %collective-permute-start.6 = (bf16[256,2048]{1,0:T(8,128)(2,1)S(1)}, bf16[256,2048]{1,0:T(8,128)(2,1)S(1)}, u32[]{:S(2)}, u32[]{:S(2)}) collective-permute-start(bf16[256,2048]{1,0:T(8,128)(2,1)S(1)} %bitcast.12), channel_id=1, source_target_pairs={{0,3},{1,0},{2,1},{3,2},{4,7},{5,4},{6,5},{7,6},{8,11},{9,8},{10,9... | collective-permute-start | bytes 3145736 | tf_op jit(solution)/shard_map/ppermute | solution.py:57
  105.7 26.8 %collective-permute-start.3 = (bf16[256,2048]{1,0:T(8,128)(2,1)S(1)}, bf16[256,2048]{1,0:T(8,128)(2,1)S(1)}, u32[]{:S(2)}, u32[]{:S(2)}) collective-permute-start(bf16[256,2048]{1,0:T(8,128)(2,1)S(1)} %bitcast.13), channel_id=1, source_target_pairs={{0,1},{1,2},{2,3},{3,0},{4,5},{5,6},{6,7},{7,4},{8,9},{9,10},{10,1... | collective-permute-start | bytes 3145736 | tf_op jit(solution)/shard_map/ppermute | solution.py:57
  106.3 47.9 %collective-permute-start.1 = (bf16[2048,256]{1,0:T(8,128)(2,1)}, bf16[2048,256]{1,0:T(8,128)(2,1)S(1)}, u32[]{:S(2)}, u32[]{:S(2)}) collective-permute-start(bf16[2048,256]{1,0:T(8,128)(2,1)} %bitcast.5.refs_0_), channel_id=1, source_target_pairs={{0,1},{1,2},{2,3},{3,0},{4,5},{5,6},{6,7},{7,4},{8,9},{9,10},{10,1... | collective-permute-start | bytes 3145736 | tf_op jit(solution)/shard_map/ppermute | solution.py:57
  106.4 48.4 %collective-permute-start.5 = (bf16[2048,256]{1,0:T(8,128)(2,1)}, bf16[2048,256]{1,0:T(8,128)(2,1)S(1)}, u32[]{:S(2)}, u32[]{:S(2)}) collective-permute-start(bf16[2048,256]{1,0:T(8,128)(2,1)} %bitcast.6.refs_1_), channel_id=1, source_target_pairs={{0,3},{1,0},{2,1},{3,2},{4,7},{5,4},{6,5},{7,6},{8,11},{9,8},{10,9... | collective-permute-start | bytes 3145736 | tf_op jit(solution)/shard_map/ppermute | solution.py:57
  130.4 33.7 %collective-permute-start.10 = (bf16[128,2048]{1,0:T(8,128)(2,1)S(1)}, bf16[128,2048]{1,0:T(8,128)(2,1)S(1)}, u32[]{:S(2)}, u32[]{:S(2)}) collective-permute-start(bf16[128,2048]{1,0:T(8,128)(2,1)S(1)} %slice.9), channel_id=1, source_target_pairs={{0,3},{1,0},{2,1},{3,2},{4,7},{5,4},{6,5},{7,6},{8,11},{9,8},{10,9... | collective-permute-start | bytes 1572872 | tf_op jit(solution)/shard_map/ppermute | solution.py:57
  131.9 76.8 %collective-permute-start.2 = (bf16[2048,256]{1,0:T(8,128)(2,1)}, bf16[2048,256]{1,0:T(8,128)(2,1)S(1)}, u32[]{:S(2)}, u32[]{:S(2)}) collective-permute-start(bf16[2048,256]{1,0:T(8,128)(2,1)} %bitcast.6.refs_1_), channel_id=1, source_target_pairs={{0,1},{1,2},{2,3},{3,0},{4,5},{5,6},{6,7},{7,4},{8,9},{9,10},{10,1... | collective-permute-start | bytes 3145736 | tf_op jit(solution)/shard_map/ppermute | solution.py:57
  132.5 31.5 %copy-start.2 = (bf16[256,2048]{1,0:T(8,128)(2,1)}, bf16[256,2048]{1,0:T(8,128)(2,1)S(1)}, u32[]{:S(2)}) copy-start(bf16[256,2048]{1,0:T(8,128)(2,1)S(1)} %collective-permute-done.3.refs_5_) | copy-start | bytes 3145732
  132.5 77.2 %collective-permute-start.4 = (bf16[2048,256]{1,0:T(8,128)(2,1)}, bf16[2048,256]{1,0:T(8,128)(2,1)S(1)}, u32[]{:S(2)}, u32[]{:S(2)}) collective-permute-start(bf16[2048,256]{1,0:T(8,128)(2,1)} %bitcast.5.refs_0_), channel_id=1, source_target_pairs={{0,3},{1,0},{2,1},{3,2},{4,7},{5,4},{6,5},{7,6},{8,11},{9,8},{10,9... | collective-permute-start | bytes 3145736 | tf_op jit(solution)/shard_map/ppermute | solution.py:57
  154.2 56.4 %copy-start.7 = (bf16[2048,256]{1,0:T(8,128)(2,1)}, bf16[2048,256]{1,0:T(8,128)(2,1)S(1)}, u32[]{:S(2)}) copy-start(bf16[2048,256]{1,0:T(8,128)(2,1)S(1)} %collective-permute-done.1.refs_3_) | copy-start | bytes 3145732
  154.2 56.4 %collective-permute-start.7 = (bf16[2048,256]{1,0:T(8,128)(2,1)S(1)}, bf16[2048,256]{1,0:T(8,128)(2,1)S(1)}, u32[]{:S(2)}, u32[]{:S(2)}) collective-permute-start(bf16[2048,256]{1,0:T(8,128)(2,1)S(1)} %collective-permute-done.1.refs_3_), channel_id=1, source_target_pairs={{0,1},{1,2},{2,3},{3,0},{4,5},{5,6},{6,7},{7,4},{8,9},{9,10},{10,1... | collective-permute-start | bytes 3145736 | tf_op jit(solution)/shard_map/ppermute | solution.py:57
  154.8 55.9 %copy-start.9 = (bf16[2048,256]{1,0:T(8,128)(2,1)}, bf16[2048,256]{1,0:T(8,128)(2,1)S(1)}, u32[]{:S(2)}) copy-start(bf16[2048,256]{1,0:T(8,128)(2,1)S(1)} %collective-permute-done.5.refs_7_) | copy-start | bytes 3145732
  154.8 56.9 %collective-permute-start.8 = (bf16[2048,256]{1,0:T(8,128)(2,1)S(1)}, bf16[2048,256]{1,0:T(8,128)(2,1)S(1)}, u32[]{:S(2)}, u32[]{:S(2)}) collective-permute-start(bf16[2048,256]{1,0:T(8,128)(2,1)S(1)} %collective-permute-done.5.refs_7_), channel_id=1, source_target_pairs={{0,3},{1,0},{2,1},{3,2},{4,7},{5,4},{6,5},{7,6},{8,11},{9,8},{10,9... | collective-permute-start | bytes 3145736 | tf_op jit(solution)/shard_map/ppermute | solution.py:57
  164.0 44.6 %collective-permute-start.9 = (bf16[128,2048]{1,0:T(8,128)(2,1)S(1)}, bf16[128,2048]{1,0:T(8,128)(2,1)S(1)}, u32[]{:S(2)}, u32[]{:S(2)}) collective-permute-start(bf16[128,2048]{1,0:T(8,128)(2,1)S(1)} %slice.8), channel_id=1, source_target_pairs={{0,1},{1,2},{2,3},{3,0},{4,5},{5,6},{6,7},{7,4},{8,9},{9,10},{10,1... | collective-permute-start | bytes 1572872 | tf_op jit(solution)/shard_map/ppermute | solution.py:57
  222.5 23.5 %copy-start.33 = (f32[40,4]{0,1:T(4,128)S(1)}, f32[40,4]{0,1:T(4,128)}, u32[]{:S(2)}) copy-start(f32[40,4]{0,1:T(4,128)} %param.31) | copy-start | bytes 1924
  232.9 62.8 %all-to-all-start.3 = ((bf16[32,8,1792]{2,1,0:T(8,128)(2,1)}), bf16[32,8,1792]{2,1,0:T(8,128)(2,1)S(1)}, u32[]{:S(2)}, u32[]{:S(2)}) async-start(bf16[32,8,1792]{2,1,0:T(8,128)(2,1)} %bitcast.8), calls=%async_computation.3 | async-start | bytes 1835008 | tf_op jit(solution)/shard_map/all_to_all | solution.py:498
  (25 other events, 25.8 us)

commit v3 on v2

--- a/solution.py
+++ b/solution.py
@@ -52,9 +52,20 @@
     )
 
 
+def in_hbm(array):
+    return pltpu.with_memory_space_constraint(array, pltpu.HBM)
+
+
 def shifted(array, axis, step):
     count = lax.axis_size(axis)
     return lax.ppermute(array, axis, [(i, (i + step) % count) for i in range(count)])
+
+
+GROUP = 8
+
+
+def lanes_of(index, width):
+    return slice(index * width, (index + 1) * width)
 
 
 def prepare_body(
@@ -86,21 +97,25 @@
     turned = (key * cos_ref[...] + swapped * sin_ref[...]).astype(jnp.bfloat16)
     sent_ref[:, latent_width:] = jnp.concatenate((turned, jnp.zeros_like(turned)), axis=1)
     wide = key_matrix_ref.shape[1]
+    depth = latent_width // 2
+    matrix = jnp.where(index_ref[1] == 0, key_matrix_ref[...], value_matrix_ref[...])
     turn_wide = turn_ref.shape[1]
     half = tokens // 2
     quarter = tokens * turn_wide // (2 * wide)
     for j in range(shares_ref.shape[0]):
-        shares_ref[j, :latent_width, :wide] = key_matrix_ref[...]
-        shares_ref[j, :latent_width, wide:] = value_matrix_ref[...]
-        shares_ref[j, latent_width : latent_width + half, :wide] = plain_ref[:half, :]
-        shares_ref[j, latent_width : latent_width + half, wide:] = plain_ref[half:, :]
+        shares_ref[j, :depth, :wide] = matrix[:depth, :]
+        shares_ref[j, :depth, wide:] = matrix[depth:, :]
+        shares_ref[j, depth : depth + half, :wide] = plain_ref[:half, :]
+        shares_ref[j, depth : depth + half, wide:] = plain_ref[half:, :]
         for i in range(tokens // quarter):
-            shares_ref[
-                j, latent_width + half :, i * turn_wide : (i + 1) * turn_wide
-            ] = turn_ref[i * quarter : (i + 1) * quarter, :]
-
-
-def attend_body(near_ref, other_ref, shares_ref, cos_ref, sin_ref, swap_ref, out_ref, kv_ref):
+            shares_ref[j, depth + half :, lanes_of(i, turn_wide)] = turn_ref[
+                i * quarter : (i + 1) * quarter, :
+            ]
+
+
+def attend_body(
+    core_ref, near_ref, other_ref, shares_ref, theirs_ref, cos_ref, sin_ref, swap_ref, out_ref, kv_ref
+):
     shards = shares_ref.shape[0]
     width = shares_ref.shape[2]
     near = near_ref.shape[0]
@@ -116,14 +131,17 @@
     stats = jnp.zeros((tokens, STAT_LANES), jnp.float32)
     last = (((1,), (1,)), ((), ()))
     for j in range(shards):
-        matrix = shares_ref[j, :latent_width, :]
-        kv_ref[:near, :] = jnp.dot(
-            near_ref[:, :latent_width], matrix, preferred_element_type=jnp.float32
-        ).astype(jnp.bfloat16)
-        kv_ref[near:, :] = jnp.dot(
-            other_ref[:, :latent_width], matrix, preferred_element_type=jnp.float32
-        ).astype(jnp.bfloat16)
-        at = latent_width
+        depth = latent_width // 2
+        mine = shares_ref[j, :depth, :]
+        other = theirs_ref[j, :depth, :]
+        for first, second, base in ((mine, other, 0), (other, mine, value_wide)):
+            packed = jnp.where(core_ref[0] == 0, first, second)
+            matrix = jnp.concatenate((packed[:, :value_wide], packed[:, value_wide:]), axis=0)
+            for rows_ref, at in ((near_ref, 0), (other_ref, near)):
+                kv_ref[at : at + near, base : base + value_wide] = jnp.dot(
+                    rows_ref[:, :latent_width], matrix, preferred_element_type=jnp.float32
+                ).astype(jnp.bfloat16)
+        at = depth
         half = tokens // 2
         plain = jnp.concatenate(
             (
@@ -182,13 +200,6 @@
         out_ref[i, :, shards * value_wide :] = stats[i * quarter : (i + 1) * quarter]
 
 
-GROUP = 8
-
-
-def lanes_of(index, width):
-    return slice(index * width, (index + 1) * width)
-
-
 def mix_body(
     parts_ref, weight_hbm, residual_ref, gain_ref, routes_ref, hidden_ref, outgoing_ref, weight_ref, sem
 ):
@@ -255,16 +266,22 @@
 
 
 def expert_body(arrived_ref, *refs):
-    count = (len(refs) - 4) // 3
-    weights_hbm = refs[: 3 * count]
-    out_ref, thin_ref, down_ref, sems = refs[3 * count :]
+    count = (len(refs) - 5) // 3
+    weights_hbm = refs[: 3 * count + 1]
+    out_ref, thin_ref, down_ref, sems = refs[3 * count + 1 :]
     gate_up = weights_hbm[0].shape
+    cut = weights_hbm[-1].shape[0]
     loads = []
-    for q in range(count):
-        for m in range(3):
-            dst = down_ref.at[q] if m == 2 else thin_ref.at[q, m]
-            loads.append(pltpu.make_async_copy(weights_hbm[3 * q + m], dst, sems.at[q, m]))
-            loads[-1].start()
+    for i, source in enumerate(weights_hbm):
+        q, m = divmod(i, 3) if i < 3 * count else (count - 1, 3)
+        if m < 2:
+            dst = thin_ref.at[q, m]
+        elif q < count - 1:
+            dst = down_ref.at[q]
+        else:
+            dst = down_ref.at[q, pl.ds((m - 2) * cut, cut)]
+        loads.append(pltpu.make_async_copy(source, dst, sems.at[i]))
+        loads[-1].start()
     rows, main = arrived_ref.shape
     model_width = gate_up[0]
     tail = model_width - main
@@ -294,6 +311,8 @@
             (jnp.clip(up_pre, -limit, limit) + 1.0) * gate_pre * jax.nn.sigmoid(slope * gate_pre)
         ).astype(jnp.bfloat16)
         loads[3 * q + 2].wait()
+        if q == count - 1:
+            loads[-1].wait()
         product = jnp.dot(active, down_ref[q], preferred_element_type=jnp.float32)
         total = total + product.astype(jnp.bfloat16).astype(jnp.float32)
     result = total.astype(jnp.bfloat16)
@@ -375,6 +394,7 @@
     heads_dev = query_plain.shape[1] // PLAIN_HEAD_WIDTH
     place = lax.axis_index(SP) * tok_dev + jnp.arange(tok_dev, dtype=jnp.int32)
     at_tp = lax.axis_index("tp")
+    at_core = lax.axis_index("sp_1")
     own_place = (
         lax.axis_index(SP) * tok_dev
         + at_tp * rows_dev
@@ -382,7 +402,7 @@
     )
     own_cos, own_sin = turn_tables(own_place, 1)
     cosines, sines = turn_tables(place, heads_dev)
-    share_rows = latent_width + tok_dev // 2 + tok_dev * query_turn.shape[1] // latent_width
+    share_rows = latent_width // 2 + tok_dev // 2 + tok_dev * query_turn.shape[1] // latent_width
     wide = plain_key_matrix.shape[1]
     whole = lambda *shape: pl.BlockSpec(shape, lambda i, at: (0,) * len(shape))
     sent, shares = pl.pallas_call(
@@ -414,37 +434,47 @@
         compiler_params=pltpu.CompilerParams(vmem_limit_bytes=16 << 20),
         name="prepare",
     )(
-        at_tp.reshape(1),
-        latent,
-        latent_norm_scale.reshape(1, latent_width),
-        key_turn.T,
-        own_cos,
-        own_sin,
-        jnp.asarray(partner_matrix(QK_ROPE), jnp.bfloat16),
-        plain_key_matrix,
-        value_matrix,
-        query_plain,
-        query_turn,
+        jnp.stack((at_tp, at_core)),
+        *map(
+            in_hbm,
+            (
+                latent,
+                latent_norm_scale.reshape(1, latent_width),
+                key_turn.T,
+                own_cos,
+                own_sin,
+                jnp.asarray(partner_matrix(QK_ROPE), jnp.bfloat16),
+                plain_key_matrix,
+                value_matrix,
+                query_plain,
+                query_turn,
+            ),
+        ),
     )
     shares = lax.all_to_all(shares, "tp", 0, 0, tiled=True)
+    theirs = shifted(shares, "sp_1", 1)
     near = lax.all_gather(sent, "sp_0", axis=0, tiled=True)
     other = shifted(near, "sp_1", 1)
 
     parts = pl.pallas_call(
         attend_body,
-        out_shape=jax.ShapeDtypeStruct(
-            (group, rows_dev, group * heads_dev * VALUE_WIDTH + STAT_LANES), jnp.bfloat16
-        ),
-        scratch_shapes=[pltpu.VMEM((2 * near.shape[0], 2 * heads_dev * VALUE_WIDTH), jnp.bfloat16)],
+        out_shape=jax.ShapeDtypeStruct((group, rows_dev, group * heads_dev * VALUE_WIDTH + STAT_LANES), jnp.bfloat16),
+        in_specs=[pl.BlockSpec(memory_space=pltpu.SMEM)]
+        + [pl.BlockSpec(memory_space=pltpu.VMEM)] * 7,
+        scratch_shapes=[
+            pltpu.VMEM((2 * near.shape[0], 2 * heads_dev * VALUE_WIDTH), jnp.bfloat16)
+        ],
         compiler_params=pltpu.CompilerParams(vmem_limit_bytes=24 << 20),
         name="attend",
     )(
+        at_core.reshape(1),
         near,
         other,
         shares,
-        cosines,
-        sines,
-        jnp.asarray(partner_matrix(heads_dev * QK_ROPE), jnp.bfloat16),
+        theirs,
+        in_hbm(cosines),
+        in_hbm(sines),
+        in_hbm(jnp.asarray(partner_matrix(heads_dev * QK_ROPE), jnp.bfloat16)),
     )
     gathered = lax.all_to_all(parts, "tp", 0, 0, tiled=True)
 
@@ -462,11 +492,16 @@
             jax.ShapeDtypeStruct((experts_all * GROUP, main), jnp.bfloat16),
         ),
         in_specs=[vmem, hbm, vmem, vmem, vmem],
-        scratch_shapes=[pltpu.VMEM(out_weight.shape, jnp.bfloat16), pltpu.SemaphoreType.DMA],
+        scratch_shapes=[
+            pltpu.VMEM(out_weight.shape, jnp.bfloat16),
+            pltpu.SemaphoreType.DMA,
+        ],
         compiler_params=pltpu.CompilerParams(vmem_limit_bytes=16 << 20),
         name="mix",
-    )(gathered, out_weight, residual, ffn_gain.reshape(1, model_width), routes.T)
-    arrived = lax.all_to_all(outgoing.reshape(experts_all, GROUP, main), SP, 0, 0, tiled=True)
+    )(gathered, in_hbm(out_weight), in_hbm(residual), in_hbm(ffn_gain.reshape(1, model_width)), in_hbm(routes.T))
+    arrived = lax.all_to_all(
+        outgoing.reshape(experts_all, GROUP, main), SP, 0, 0, tiled=True
+    )
 
     own = (gate_weight[0], up_weight[0], down_weight[0])
     left, right = [], []
@@ -478,11 +513,11 @@
     far_up = shifted(right[1], "tp", -1)
     far_down_l = shifted(left[2][:cut], "tp", 1)
     far_down_r = shifted(right[2][cut:], "tp", -1)
-    far = (far_gate, far_up, jnp.concatenate((far_down_l, far_down_r), axis=0))
 
     weights = []
-    for gate_w, up_w, down_w in (own, left, right, far):
-        weights += [gate_w, up_w, down_w]
+    for quarter_weights in (own, left, right):
+        weights += list(quarter_weights)
+    weights += [far_gate, far_up, far_down_l, far_down_r]
     result_rows = pl.pallas_call(
         expert_body,
         out_shape=jax.ShapeDtypeStruct((experts_all * GROUP, main), jnp.bfloat16),
@@ -490,18 +525,20 @@
         scratch_shapes=[
             pltpu.VMEM((group, 2) + own[0].shape, jnp.bfloat16),
             pltpu.VMEM((group,) + own[2].shape, jnp.bfloat16),
-            pltpu.SemaphoreType.DMA((group, 3)),
+            pltpu.SemaphoreType.DMA((len(weights),)),
         ],
         compiler_params=pltpu.CompilerParams(vmem_limit_bytes=40 << 20),
         name="expert",
-    )(arrived.reshape(experts_all * GROUP, main), *weights)
-    returned = lax.all_to_all(result_rows.reshape(experts_all, GROUP, main), SP, 0, 0, tiled=True)
+    )(arrived.reshape(experts_all * GROUP, main), *map(in_hbm, weights))
+    returned = lax.all_to_all(
+        result_rows.reshape(experts_all, GROUP, main), SP, 0, 0, tiled=True
+    )
     return pl.pallas_call(
         combine_body,
         out_shape=jax.ShapeDtypeStruct((rows_dev, model_width), jnp.bfloat16),
         compiler_params=pltpu.CompilerParams(vmem_limit_bytes=16 << 20),
         name="combine",
-    )(returned.reshape(experts_all * GROUP, main), hidden, routes, route_weights)
+    )(returned.reshape(experts_all * GROUP, main), hidden, in_hbm(routes), in_hbm(route_weights))
 
 
 def solution(mesh):

time: 301 us -> 301 us (level)
  blocking collectives: 35.6 us -> 76.9 us
  local copies, waits for them, and re-layouts: 28.9 us -> 5.09 us
  starting transfers between devices: 56.4 us -> 37.7 us
  Pallas kernels: 23.4 us -> 30.2 us
  waiting for transfers between devices: 151 us -> 146 us
    all_to_all x0 -> x1, blocking collectives: none -> 33.9 us  [on_device(): shares = lax.all_to_all(shares, 'tp', 0, 0, tiled=True)]
    unnamed x70 -> x26, local copies, waits for them, and re-layouts: 28.1 us -> 3.14 us
    all_to_all x1 -> x0, starting transfers between devices: 23.1 us -> none  [on_device(): shares = lax.all_to_all(shares, 'tp', 0, 0, tiled=True)]
    all_gather x1, blocking collectives: 35.6 us -> 43 us  [on_device(): near = lax.all_gather(sent, 'sp_0', axis=0, tiled=True)]
    ppermute x11 -> x12, starting transfers between devices: 10.9 us -> 14.7 us  [shifted(): lax.ppermute(array, axis, [(i, (i + step) % count) for i in range(count)])]
    ppermute x11 -> x12, waiting for transfers between devices: 94.9 us -> 91.7 us  [shifted(): lax.ppermute(array, axis, [(i, (i + step) % count) for i in range(count)])]
  transfers between devices with their start and end apart: 15 -> 15, of which waited for: 7 -> 8; matrix products, arithmetic and copies ran while one was open for 0% -> 1% of each run, Pallas kernels for 0% -> 0%
where the time goes in v3:
time: 301 us; the launch traced here: 298 us
  waiting for transfers between devices  146 us (49%)
  blocking collectives  76.9 us (26%)
  starting transfers between devices  37.7 us (13%)
  Pallas kernels  30.2 us (10%)
  local copies, waits for them, and re-layouts  5.09 us (2%)
    ppermute x12, waiting for transfers between devices, shifted(): lax.ppermute(array, axis, [(i, (i + step) % count) for i in range(count)])  91.7 us
    all_to_all x1, waiting for transfers between devices, on_device(): lax.all_to_all(result_rows.reshape(experts_all, GROUP, main), SP, 0, 0, t...  48.4 us
    all_gather x1, blocking collectives, on_device(): near = lax.all_gather(sent, 'sp_0', axis=0, tiled=True)  43 us
    all_to_all x1, blocking collectives, on_device(): shares = lax.all_to_all(shares, 'tp', 0, 0, tiled=True)  33.9 us
    ppermute x12, starting transfers between devices, shifted(): lax.ppermute(array, axis, [(i, (i + step) % count) for i in range(count)])  14.7 us
    all_to_all x1, starting transfers between devices, on_device(): lax.all_to_all(result_rows.reshape(experts_all, GROUP, main), SP, 0, 0, t...  13 us
    pallas_call x1, Pallas kernels, on_device(): pl.pallas_call(expert_body, out_shape=jax.ShapeDtypeStruct((experts_all *...  10.4 us
    pallas_call x1, Pallas kernels, on_device(): pl.pallas_call(attend_body, out_shape=jax.ShapeDtypeStruct((group, rows_d...  10.1 us
  transfers between devices with their start and end apart: 15, of which 8 were waited for; matrix products, arithmetic and copies ran while one was open for 1% of the time, Pallas kernels for 0%

profile of v3, /device:TPU:34, one launch (start us, length us, event | category | flops | bytes accessed | tf_op | source)
XLA Modules:
  0.0 298.4 jit_solution(4799946796043917027)
XLA Ops:
  0.0 1.3 reshape.132.gain_ref
  2.1 2.0 prepare.1
  4.2 33.9 %all_to_all.20.shares_ref = bf16[4,376,512]{2,1,0:T(8,128)(2,1)S(1)} all-to-all(bf16[4,376,512]{2,1,0:T(8,128)(2,1)S(1)} %get-tuple-element.10), channel_id=1, replica_groups=mesh['grp'=2,'sp_0'=16,'sp_1'=2,'tp'=4] {'tp'}, dimensions={0} | all-to-all | bytes 3080192 | tf_op jit(solution)/shard_map/all_to_all | solution.py:454
  38.1 43.0 %all_gather.3.near_ref = bf16[640,640]{1,0:T(8,128)(2,1)S(1)} all-gather(bf16[40,640]{1,0:T(8,128)(2,1)S(1)} %get-tuple-element.9), channel_id=1, replica_groups=mesh['grp'=2,'sp_0'=16,'sp_1'=2,'tp'=4] {'sp_0'}, dimensions={0}, use_global_device_ids=true | all-gather | bytes 870400 | tf_op jit(solution)/shard_map/all_gather | solution.py:456
  83.4 10.1 %attend.1 = bf16[4,40,1152]{2,1,0:T(8,128)(2,1)} custom-call(s32[1]{0:T(128)} %bitcast.core_ref, bf16[640,640]{1,0:T(8,128)(2,1)S(1)} %all_gather.3.near_ref, bf16[640,640]{1,0:T(8,128)(2,1)S(1)} %collective-permute-done.other_ref, bf16[4,376,512]{2,1,0:T(8,128)(2,1)S(1)} %all_to_all.20.shares_ref, ...), custom_call_target="tpu_custom_call" | custom-call | tf_op jit(solution)/shard_map/attend/pallas_call | solution.py:459
  93.5 4.9 %all-to-all-start.1 = ((bf16[4,40,1152]{2,1,0:T(8,128)(2,1)}), bf16[4,40,1152]{2,1,0:T(8,128)(2,1)S(1)}, u32[]{:S(2)}, u32[]{:S(2)}) async-start(bf16[4,40,1152]{2,1,0:T(8,128)(2,1)} %attend.1), calls=%async_computation.1 | async-start | bytes 737280 | tf_op jit(solution)/shard_map/all_to_all | solution.py:479
  99.0 6.4 %all-to-all-done.1.parts_ref = bf16[4,40,1152]{2,1,0:T(8,128)(2,1)S(1)} async-done(((bf16[4,40,1152]{2,1,0:T(8,128)(2,1)}), bf16[4,40,1152]{2,1,0:T(8,128)(2,1)S(1)}, u32[]{:S(2)}, u32[]{:S(2)}) %all-to-all-start.1) | async-done | bytes 368672 | tf_op jit(solution)/shard_map/all_to_all | solution.py:479
  105.3 5.7 %mix.1 = (bf16[40,2048]{1,0:T(8,128)(2,1)S(1)}, bf16[256,1792]{1,0:T(8,128)(2,1)}) custom-call(bf16[4,40,1152]{2,1,0:T(8,128)(2,1)S(1)} %all-to-all-done.1.parts_ref, bf16[1024,2048]{1,0:T(8,128)(2,1)} %weight_hbm.1, bf16[40,2048]{1,0:T(8,128)(2,1)} %residual_ref.1, bf16[1,2048]{1,0:T(2,128)(2,1)} %reshape.133.gain_ref, s32[4,40]{1,0:T(4,128)} %bitcast.14), custom_call_target="tpu_custom_call" | custom-call | tf_op jit(solution)/shard_map/mix/pallas_call | solution.py:488
  111.0 5.0 %all-to-all-start.2 = ((bf16[32,8,1792]{2,1,0:T(8,128)(2,1)}), bf16[32,8,1792]{2,1,0:T(8,128)(2,1)S(1)}, u32[]{:S(2)}, u32[]{:S(2)}) async-start(bf16[32,8,1792]{2,1,0:T(8,128)(2,1)} %bitcast.4), calls=%async_computation.2 | async-start | bytes 1835008 | tf_op jit(solution)/shard_map/all_to_all | solution.py:502
  116.2 2.0 collective-permute-start.2
  118.3 3.1 %collective-permute-start.7 = (bf16[256,2048]{1,0:T(8,128)(2,1)}, bf16[256,2048]{1,0:T(8,128)(2,1)S(1)}, u32[]{:S(2)}, u32[]{:S(2)}) collective-permute-start(bf16[256,2048]{1,0:T(8,128)(2,1)} %bitcast.8.refs_2_), channel_id=1, source_target_pairs={{0,3},{1,0},{2,1},{3,2},{4,7},{5,4},{6,5},{7,6},{8,11},{9,8},{10,9... | collective-permute-start | bytes 3145736 | tf_op jit(solution)/shard_map/ppermute | solution.py:61
  121.4 21.0 %collective-permute-done.4.refs_5_ = bf16[256,2048]{1,0:T(8,128)(2,1)S(1)} collective-permute-done((bf16[256,2048]{1,0:T(8,128)(2,1)}, bf16[256,2048]{1,0:T(8,128)(2,1)S(1)}, u32[]{:S(2)}, u32[]{:S(2)}) %collective-permute-start.4) | collective-permute-done | bytes 1048608 | tf_op jit(solution)/shard_map/ppermute | solution.py:61
  142.4 2.7 collective-permute-start.5
  145.1 19.8 %collective-permute-done.2.refs_3_ = bf16[2048,256]{1,0:T(8,128)(2,1)S(1)} collective-permute-done((bf16[2048,256]{1,0:T(8,128)(2,1)}, bf16[2048,256]{1,0:T(8,128)(2,1)S(1)}, u32[]{:S(2)}, u32[]{:S(2)}) %collective-permute-start.2) | collective-permute-done | bytes 1048608 | tf_op jit(solution)/shard_map/ppermute | solution.py:61
  164.9 2.8 collective-permute-start.9
  167.8 1.2 collective-permute-start.10
  169.0 18.3 %collective-permute-done.3.refs_4_ = bf16[2048,256]{1,0:T(8,128)(2,1)S(1)} collective-permute-done((bf16[2048,256]{1,0:T(8,128)(2,1)}, bf16[2048,256]{1,0:T(8,128)(2,1)S(1)}, u32[]{:S(2)}, u32[]{:S(2)}) %collective-permute-start.3) | collective-permute-done | bytes 1048608 | tf_op jit(solution)/shard_map/ppermute | solution.py:61
  187.4 2.7 collective-permute-start.11
  190.0 29.6 %collective-permute-done.10.refs_11_ = bf16[128,2048]{1,0:T(8,128)(2,1)S(1)} collective-permute-done((bf16[128,2048]{1,0:T(8,128)(2,1)S(1)}, bf16[128,2048]{1,0:T(8,128)(2,1)S(1)}, u32[]{:S(2)}, u32[]{:S(2)}) %collective-permute-start.10) | collective-permute-done | bytes 524320 | tf_op jit(solution)/shard_map/ppermute | solution.py:61
  219.6 1.8 collective-permute-done.11.refs_12_
  223.2 10.4 %expert.1 = bf16[256,1792]{1,0:T(8,128)(2,1)} custom-call(bf16[256,1792]{1,0:T(8,128)(2,1)S(1)} %bitcast.11, bf16[2048,256]{1,0:T(8,128)(2,1)} %bitcast.6.refs_0_, bf16[2048,256]{1,0:T(8,128)(2,1)} %bitcast.7.refs_1_, bf16[256,2048]{1,0:T(8,128)(2,1)} %bitcast.8.refs_2_, bf16[2048,256]{1,0:T(8,128)(2,1)} %copy-done.2, bf16[2048,256]{1,0:T(8,128)(2,1)} %copy-done.4, ...), custom_call_target="tpu_custom_call" | custom-call | tf_op jit(solution)/shard_map/expert/pallas_call | solution.py:521
  233.6 13.0 %all-to-all-start.3 = ((bf16[32,8,1792]{2,1,0:T(8,128)(2,1)}), bf16[32,8,1792]{2,1,0:T(8,128)(2,1)S(1)}, u32[]{:S(2)}, u32[]{:S(2)}) async-start(bf16[32,8,1792]{2,1,0:T(8,128)(2,1)} %bitcast.9), calls=%async_computation.3 | async-start | bytes 1835008 | tf_op jit(solution)/shard_map/all_to_all | solution.py:533
  248.0 48.4 %all-to-all-done.3 = bf16[32,8,1792]{2,1,0:T(8,128)(2,1)S(1)} async-done(((bf16[32,8,1792]{2,1,0:T(8,128)(2,1)}), bf16[32,8,1792]{2,1,0:T(8,128)(2,1)S(1)}, u32[]{:S(2)}, u32[]{:S(2)}) %all-to-all-start.3) | async-done | bytes 917536 | tf_op jit(solution)/shard_map/all_to_all | solution.py:533
  296.4 2.0 combine.1
  (52 shorter events, 7.4 us)
Async XLA Ops:
  38.1 45.3 %collective-permute-start.1 = (bf16[4,376,512]{2,1,0:T(8,128)(2,1)S(1)}, bf16[4,376,512]{2,1,0:T(8,128)(2,1)S(1)}, u32[]{:S(2)}, u32[]{:S(2)}) collective-permute-start(bf16[4,376,512]{2,1,0:T(8,128)(2,1)S(1)} %all_to_all.20.shares_ref), channel_id=1, source_target_pairs={{0,4},{4,0},{1,5},{5,1},{2,6},{6,2},{3,7},{7,3},{8,12},{12,8},{9,1... | collective-permute-start | bytes 4620296 | tf_op jit(solution)/shard_map/ppermute | solution.py:61
  81.1 2.3 collective-permute-start
  83.4 15.0 %copy-start.10 = (bf16[2048]{0:T(1024)(128)(2,1)S(1)}, bf16[2048]{0:T(1024)(128)(2,1)}, u32[]{:S(2)}) copy-start(bf16[2048]{0:T(1024)(128)(2,1)} %param.26) | copy-start | bytes 12292
  93.5 11.9 %all-to-all-start.1 = ((bf16[4,40,1152]{2,1,0:T(8,128)(2,1)}), bf16[4,40,1152]{2,1,0:T(8,128)(2,1)S(1)}, u32[]{:S(2)}, u32[]{:S(2)}) async-start(bf16[4,40,1152]{2,1,0:T(8,128)(2,1)} %attend.1), calls=%async_computation.1 | async-start | bytes 737280 | tf_op jit(solution)/shard_map/all_to_all | solution.py:479
  111.0 112.1 %all-to-all-start.2 = ((bf16[32,8,1792]{2,1,0:T(8,128)(2,1)}), bf16[32,8,1792]{2,1,0:T(8,128)(2,1)S(1)}, u32[]{:S(2)}, u32[]{:S(2)}) async-start(bf16[32,8,1792]{2,1,0:T(8,128)(2,1)} %bitcast.4), calls=%async_computation.2 | async-start | bytes 1835008 | tf_op jit(solution)/shard_map/all_to_all | solution.py:502
  116.1 26.4 %collective-permute-start.4 = (bf16[256,2048]{1,0:T(8,128)(2,1)}, bf16[256,2048]{1,0:T(8,128)(2,1)S(1)}, u32[]{:S(2)}, u32[]{:S(2)}) collective-permute-start(bf16[256,2048]{1,0:T(8,128)(2,1)} %bitcast.8.refs_2_), channel_id=1, source_target_pairs={{0,1},{1,2},{2,3},{3,0},{4,5},{5,6},{6,7},{7,4},{8,9},{9,10},{10,1... | collective-permute-start | bytes 3145736 | tf_op jit(solution)/shard_map/ppermute | solution.py:61
  116.2 48.7 %collective-permute-start.2 = (bf16[2048,256]{1,0:T(8,128)(2,1)}, bf16[2048,256]{1,0:T(8,128)(2,1)S(1)}, u32[]{:S(2)}, u32[]{:S(2)}) collective-permute-start(bf16[2048,256]{1,0:T(8,128)(2,1)} %bitcast.6.refs_0_), channel_id=1, source_target_pairs={{0,1},{1,2},{2,3},{3,0},{4,5},{5,6},{6,7},{7,4},{8,9},{9,10},{10,1... | collective-permute-start | bytes 3145736 | tf_op jit(solution)/shard_map/ppermute | solution.py:61
  118.2 46.8 %collective-permute-start.6 = (bf16[2048,256]{1,0:T(8,128)(2,1)}, bf16[2048,256]{1,0:T(8,128)(2,1)S(1)}, u32[]{:S(2)}, u32[]{:S(2)}) collective-permute-start(bf16[2048,256]{1,0:T(8,128)(2,1)} %bitcast.7.refs_1_), channel_id=1, source_target_pairs={{0,3},{1,0},{2,1},{3,2},{4,7},{5,4},{6,5},{7,6},{8,11},{9,8},{10,9... | collective-permute-start | bytes 3145736 | tf_op jit(solution)/shard_map/ppermute | solution.py:61
  118.3 49.4 %collective-permute-start.7 = (bf16[256,2048]{1,0:T(8,128)(2,1)}, bf16[256,2048]{1,0:T(8,128)(2,1)S(1)}, u32[]{:S(2)}, u32[]{:S(2)}) collective-permute-start(bf16[256,2048]{1,0:T(8,128)(2,1)} %bitcast.8.refs_2_), channel_id=1, source_target_pairs={{0,3},{1,0},{2,1},{3,2},{4,7},{5,4},{6,5},{7,6},{8,11},{9,8},{10,9... | collective-permute-start | bytes 3145736 | tf_op jit(solution)/shard_map/ppermute | solution.py:61
  121.4 65.9 %collective-permute-start.3 = (bf16[2048,256]{1,0:T(8,128)(2,1)}, bf16[2048,256]{1,0:T(8,128)(2,1)S(1)}, u32[]{:S(2)}, u32[]{:S(2)}) collective-permute-start(bf16[2048,256]{1,0:T(8,128)(2,1)} %bitcast.7.refs_1_), channel_id=1, source_target_pairs={{0,1},{1,2},{2,3},{3,0},{4,5},{5,6},{6,7},{7,4},{8,9},{9,10},{10,1... | collective-permute-start | bytes 3145736 | tf_op jit(solution)/shard_map/ppermute | solution.py:61
  142.4 80.7 %copy-start = (bf16[256,2048]{1,0:T(8,128)(2,1)}, bf16[256,2048]{1,0:T(8,128)(2,1)S(1)}, u32[]{:S(2)}) copy-start(bf16[256,2048]{1,0:T(8,128)(2,1)S(1)} %collective-permute-done.4.refs_5_) | copy-start | bytes 3145732
  142.4 47.6 %collective-permute-start.5 = (bf16[2048,256]{1,0:T(8,128)(2,1)}, bf16[2048,256]{1,0:T(8,128)(2,1)S(1)}, u32[]{:S(2)}, u32[]{:S(2)}) collective-permute-start(bf16[2048,256]{1,0:T(8,128)(2,1)} %bitcast.6.refs_0_), channel_id=1, source_target_pairs={{0,3},{1,0},{2,1},{3,2},{4,7},{5,4},{6,5},{7,6},{8,11},{9,8},{10,9... | collective-permute-start | bytes 3145736 | tf_op jit(solution)/shard_map/ppermute | solution.py:61
  164.9 56.5 %copy-start.2 = (bf16[2048,256]{1,0:T(8,128)(2,1)}, bf16[2048,256]{1,0:T(8,128)(2,1)S(1)}, u32[]{:S(2)}) copy-start(bf16[2048,256]{1,0:T(8,128)(2,1)S(1)} %collective-permute-done.2.refs_3_) | copy-start | bytes 3145732
  164.9 56.5 %collective-permute-start.8 = (bf16[2048,256]{1,0:T(8,128)(2,1)S(1)}, bf16[2048,256]{1,0:T(8,128)(2,1)S(1)}, u32[]{:S(2)}, u32[]{:S(2)}) collective-permute-start(bf16[2048,256]{1,0:T(8,128)(2,1)S(1)} %collective-permute-done.2.refs_3_), channel_id=1, source_target_pairs={{0,1},{1,2},{2,3},{3,0},{4,5},{5,6},{6,7},{7,4},{8,9},{9,10},{10,1... | collective-permute-start | bytes 3145736 | tf_op jit(solution)/shard_map/ppermute | solution.py:61
  164.9 56.4 %copy-start.3 = (bf16[2048,256]{1,0:T(8,128)(2,1)}, bf16[2048,256]{1,0:T(8,128)(2,1)S(1)}, u32[]{:S(2)}) copy-start(bf16[2048,256]{1,0:T(8,128)(2,1)S(1)} %collective-permute-done.6.refs_7_) | copy-start | bytes 3145732
  164.9 58.2 %collective-permute-start.9 = (bf16[2048,256]{1,0:T(8,128)(2,1)S(1)}, bf16[2048,256]{1,0:T(8,128)(2,1)}, u32[]{:S(2)}, u32[]{:S(2)}) collective-permute-start(bf16[2048,256]{1,0:T(8,128)(2,1)S(1)} %collective-permute-done.6.refs_7_), channel_id=1, source_target_pairs={{0,3},{1,0},{2,1},{3,2},{4,7},{5,4},{6,5},{7,6},{8,11},{9,8},{10,9... | collective-permute-start | bytes 3145736 | tf_op jit(solution)/shard_map/ppermute | solution.py:61
  167.7 55.4 %copy-start.1 = (bf16[256,2048]{1,0:T(8,128)(2,1)}, bf16[256,2048]{1,0:T(8,128)(2,1)S(1)}, u32[]{:S(2)}) copy-start(bf16[256,2048]{1,0:T(8,128)(2,1)S(1)} %collective-permute-done.7.refs_8_) | copy-start | bytes 3145732
  167.8 51.8 %collective-permute-start.10 = (bf16[128,2048]{1,0:T(8,128)(2,1)S(1)}, bf16[128,2048]{1,0:T(8,128)(2,1)S(1)}, u32[]{:S(2)}, u32[]{:S(2)}) collective-permute-start(bf16[128,2048]{1,0:T(8,128)(2,1)S(1)} %slice.8), channel_id=1, source_target_pairs={{0,1},{1,2},{2,3},{3,0},{4,5},{5,6},{6,7},{7,4},{8,9},{9,10},{10,1... | collective-permute-start | bytes 1572872 | tf_op jit(solution)/shard_map/ppermute | solution.py:61
  187.4 34.0 %copy-start.4 = (bf16[2048,256]{1,0:T(8,128)(2,1)}, bf16[2048,256]{1,0:T(8,128)(2,1)S(1)}, u32[]{:S(2)}) copy-start(bf16[2048,256]{1,0:T(8,128)(2,1)S(1)} %collective-permute-done.3.refs_4_) | copy-start | bytes 3145732
  187.4 34.0 %collective-permute-start.11 = (bf16[128,2048]{1,0:T(8,128)(2,1)S(1)}, bf16[128,2048]{1,0:T(8,128)(2,1)S(1)}, u32[]{:S(2)}, u32[]{:S(2)}) collective-permute-start(bf16[128,2048]{1,0:T(8,128)(2,1)S(1)} %slice.9), channel_id=1, source_target_pairs={{0,3},{1,0},{2,1},{3,2},{4,7},{5,4},{6,5},{7,6},{8,11},{9,8},{10,9... | collective-permute-start | bytes 1572872 | tf_op jit(solution)/shard_map/ppermute | solution.py:61
  190.0 31.4 %copy-start.5 = (bf16[2048,256]{1,0:T(8,128)(2,1)}, bf16[2048,256]{1,0:T(8,128)(2,1)S(1)}, u32[]{:S(2)}) copy-start(bf16[2048,256]{1,0:T(8,128)(2,1)S(1)} %collective-permute-done.5.refs_6_) | copy-start | bytes 3145732
  233.6 13.1 %copy-start.9 = (s32[40,4]{0,1:T(4,128)S(1)}, s32[40,4]{0,1:T(4,128)}, u32[]{:S(2)}) copy-start(s32[40,4]{0,1:T(4,128)} %param.30) | copy-start | bytes 1924
  233.6 13.8 %copy-start.11 = (f32[40,4]{0,1:T(4,128)S(1)}, f32[40,4]{0,1:T(4,128)}, u32[]{:S(2)}) copy-start(f32[40,4]{0,1:T(4,128)} %param.31) | copy-start | bytes 1924
  233.6 62.8 %all-to-all-start.3 = ((bf16[32,8,1792]{2,1,0:T(8,128)(2,1)}), bf16[32,8,1792]{2,1,0:T(8,128)(2,1)S(1)}, u32[]{:S(2)}, u32[]{:S(2)}) async-start(bf16[32,8,1792]{2,1,0:T(8,128)(2,1)} %bitcast.9), calls=%async_computation.3 | async-start | bytes 1835008 | tf_op jit(solution)/shard_map/all_to_all | solution.py:533
  (3 other events, 3.6 us)

commit v4 on v3

--- a/solution.py
+++ b/solution.py
@@ -114,7 +114,17 @@
 
 
 def attend_body(
-    core_ref, near_ref, other_ref, shares_ref, theirs_ref, cos_ref, sin_ref, swap_ref, out_ref, kv_ref
+    core_ref,
+    near_ref,
+    other_ref,
+    shares_ref,
+    theirs_ref,
+    cos_ref,
+    sin_ref,
+    swap_ref,
+    out_ref,
+    keys_ref,
+    values_ref,
 ):
     shards = shares_ref.shape[0]
     width = shares_ref.shape[2]
@@ -125,8 +135,9 @@
     value_wide = width // 2
     heads = value_wide // PLAIN_HEAD_WIDTH
     scale = (PLAIN_HEAD_WIDTH + QK_ROPE) ** (-0.5)
-    near_rot = near_ref[:, latent_width : latent_width + QK_ROPE]
-    other_rot = other_ref[:, latent_width : latent_width + QK_ROPE]
+    for h in range(heads):
+        for rows_ref, at in ((near_ref, 0), (other_ref, near)):
+            keys_ref[h, at : at + near, PLAIN_HEAD_WIDTH:] = rows_ref[:, latent_width:]
     lane = lax.broadcasted_iota(jnp.int32, (tokens, STAT_LANES), 1)
     stats = jnp.zeros((tokens, STAT_LANES), jnp.float32)
     last = (((1,), (1,)), ((), ()))
@@ -134,13 +145,20 @@
         depth = latent_width // 2
         mine = shares_ref[j, :depth, :]
         other = theirs_ref[j, :depth, :]
-        for first, second, base in ((mine, other, 0), (other, mine, value_wide)):
+        for first, second, is_key in ((mine, other, True), (other, mine, False)):
             packed = jnp.where(core_ref[0] == 0, first, second)
             matrix = jnp.concatenate((packed[:, :value_wide], packed[:, value_wide:]), axis=0)
             for rows_ref, at in ((near_ref, 0), (other_ref, near)):
-                kv_ref[at : at + near, base : base + value_wide] = jnp.dot(
+                made = jnp.dot(
                     rows_ref[:, :latent_width], matrix, preferred_element_type=jnp.float32
                 ).astype(jnp.bfloat16)
+                if is_key:
+                    for h in range(heads):
+                        keys_ref[h, at : at + near, :PLAIN_HEAD_WIDTH] = made[
+                            :, lanes_of(h, PLAIN_HEAD_WIDTH)
+                        ]
+                else:
+                    values_ref[at : at + near, :] = made
         at = depth
         half = tokens // 2
         plain = jnp.concatenate(
@@ -164,25 +182,18 @@
         )
         for h in range(heads):
             lo = h * PLAIN_HEAD_WIDTH
-            query = plain[:, lo : lo + PLAIN_HEAD_WIDTH]
-            query_rot = turned[:, h * QK_ROPE : (h + 1) * QK_ROPE]
-            keys = kv_ref[:, lo : lo + PLAIN_HEAD_WIDTH]
-            rotary = jnp.concatenate(
-                (
-                    lax.dot_general(query_rot, near_rot, last, preferred_element_type=jnp.float32),
-                    lax.dot_general(query_rot, other_rot, last, preferred_element_type=jnp.float32),
-                ),
-                axis=1,
+            query_rot = turned[:, lanes_of(h, QK_ROPE)]
+            query = jnp.concatenate(
+                (plain[:, lo : lo + PLAIN_HEAD_WIDTH], query_rot, jnp.zeros_like(query_rot)), axis=1
             )
-            scores = (
-                lax.dot_general(query, keys, last, preferred_element_type=jnp.float32) + rotary
-            ) * scale
+            scores = lax.dot_general(query, keys_ref[h], last, preferred_element_type=jnp.float32)
             peak = jnp.max(scores, axis=1, keepdims=True)
-            weights = jnp.exp(scores - peak)
+            weights = jnp.exp((scores - peak) * scale)
             total = jnp.sum(weights, axis=1, keepdims=True)
-            head_values = kv_ref[:, value_wide + lo : value_wide + lo + VALUE_WIDTH]
             summed = jnp.dot(
-                weights.astype(jnp.bfloat16), head_values, preferred_element_type=jnp.float32
+                weights.astype(jnp.bfloat16),
+                values_ref[:, lanes_of(h, VALUE_WIDTH)],
+                preferred_element_type=jnp.float32,
             )
             result = (summed / total).astype(jnp.bfloat16)
             head = j * heads + h
@@ -190,7 +201,7 @@
                 out_ref[i, :, head * VALUE_WIDTH : (head + 1) * VALUE_WIDTH] = result[
                     i * quarter : (i + 1) * quarter
                 ]
-            rest = peak + jnp.log(total)
+            rest = peak * scale + jnp.log(total)
             for part in range(3):
                 top = rest.astype(jnp.bfloat16).astype(jnp.float32)
                 rest = rest - top
@@ -201,10 +212,15 @@
 
 
 def mix_body(
-    parts_ref, weight_hbm, residual_ref, gain_ref, routes_ref, hidden_ref, outgoing_ref, weight_ref, sem
+    parts_ref, weight_hbm, residual_ref, gain_ref, routes_ref, hidden_ref, outgoing_ref, weight_ref, sems
 ):
-    load = pltpu.make_async_copy(weight_hbm, weight_ref, sem)
-    load.start()
+    pieces = sems.shape[0]
+    depth = weight_ref.shape[0] // pieces
+    loads = []
+    for i in range(pieces):
+        part = pl.ds(i * depth, depth)
+        loads.append(pltpu.make_async_copy(weight_hbm.at[part], weight_ref.at[part], sems.at[i]))
+        loads[-1].start()
     shards = parts_ref.shape[0]
     rows, model_width = residual_ref.shape
     wide = weight_ref.shape[0]
@@ -223,7 +239,7 @@
     for s in shares[1:]:
         whole = whole + s
     shares = [s / whole for s in shares]
-    pieces = []
+    joined = []
     for h in range(heads):
         lo = h * VALUE_WIDTH
         piece = shares[0][:, h : h + 1] * parts_ref[0, :, lo : lo + VALUE_WIDTH].astype(jnp.float32)
@@ -231,8 +247,8 @@
             piece = piece + shares[i][:, h : h + 1] * parts_ref[
                 i, :, lo : lo + VALUE_WIDTH
             ].astype(jnp.float32)
-        pieces.append(piece.astype(jnp.bfloat16))
-    attended = jnp.concatenate(pieces, axis=1)
+        joined.append(piece.astype(jnp.bfloat16))
+    attended = jnp.concatenate(joined, axis=1)
 
     total_rows = outgoing_ref.shape[0]
     line = lax.broadcasted_iota(jnp.int32, (total_rows, rows), 0)
@@ -248,7 +264,8 @@
     ).astype(jnp.int32)
     table = jnp.where((named > 0) & (rank == line % GROUP), 1.0, 0.0).astype(jnp.bfloat16)
 
-    load.wait()
+    for load in loads:
+        load.wait()
     projected = jnp.dot(attended, weight_ref[...], preferred_element_type=jnp.float32)
     hidden = (residual_ref[...].astype(jnp.float32) + projected).astype(jnp.bfloat16)
     hidden_ref[...] = hidden
@@ -296,7 +313,7 @@
             pick, arrived_ref[:, lanes_of(s, tail)], preferred_element_type=jnp.float32
         )
     ends = ends.astype(jnp.bfloat16)
-    total = jnp.zeros((rows, model_width), jnp.float32)
+    actives = []
     for q in range(count):
         loads[3 * q].wait()
         gate_pre = jnp.dot(
@@ -307,25 +324,34 @@
             arrived_ref[...], thin_ref[q, 1, :main, :], preferred_element_type=jnp.float32
         ) + jnp.dot(ends, thin_ref[q, 1, main:, :], preferred_element_type=jnp.float32)
         gate_pre = jnp.minimum(gate_pre, limit)
-        active = (
-            (jnp.clip(up_pre, -limit, limit) + 1.0) * gate_pre * jax.nn.sigmoid(slope * gate_pre)
-        ).astype(jnp.bfloat16)
+        actives.append(
+            (
+                (jnp.clip(up_pre, -limit, limit) + 1.0) * gate_pre * jax.nn.sigmoid(slope * gate_pre)
+            ).astype(jnp.bfloat16)
+        )
+    for q in range(count):
         loads[3 * q + 2].wait()
-        if q == count - 1:
-            loads[-1].wait()
-        product = jnp.dot(active, down_ref[q], preferred_element_type=jnp.float32)
-        total = total + product.astype(jnp.bfloat16).astype(jnp.float32)
-    result = total.astype(jnp.bfloat16)
-    last = result[:, main:]
+    loads[-1].wait()
+
+    def result_of(piece):
+        total = jnp.zeros((rows, tail), jnp.float32)
+        for q in range(count):
+            product = jnp.dot(
+                actives[q], down_ref[q, :, lanes_of(piece, tail)], preferred_element_type=jnp.float32
+            )
+            total = total + product.astype(jnp.bfloat16).astype(jnp.float32)
+        return total
+
+    last = result_of(GROUP - 1).astype(jnp.bfloat16)
     group_end = lax.broadcasted_iota(jnp.int32, (rows, tail), 0) % GROUP == GROUP - 1
     for s in range(GROUP - 1):
         pick = jnp.where(
             (line % GROUP == GROUP - 1) & (column == line - (GROUP - 1) + s), 1.0, 0.0
         ).astype(jnp.bfloat16)
-        moved = jnp.dot(pick, last, preferred_element_type=jnp.float32).astype(jnp.bfloat16)
-        out_ref[:, lanes_of(s, tail)] = jnp.where(
-            group_end, moved.astype(jnp.float32), result[:, lanes_of(s, tail)].astype(jnp.float32)
-        ).astype(jnp.bfloat16)
+        moved = jnp.dot(pick, last, preferred_element_type=jnp.float32)
+        out_ref[:, lanes_of(s, tail)] = jnp.where(group_end, moved, result_of(s)).astype(
+            jnp.bfloat16
+        )
 
 
 def combine_body(returned_ref, hidden_ref, routes_ref, weights_ref, out_ref):
@@ -462,7 +488,8 @@
         in_specs=[pl.BlockSpec(memory_space=pltpu.SMEM)]
         + [pl.BlockSpec(memory_space=pltpu.VMEM)] * 7,
         scratch_shapes=[
-            pltpu.VMEM((2 * near.shape[0], 2 * heads_dev * VALUE_WIDTH), jnp.bfloat16)
+            pltpu.VMEM((heads_dev, 2 * near.shape[0], PLAIN_HEAD_WIDTH + 2 * QK_ROPE), jnp.bfloat16),
+            pltpu.VMEM((2 * near.shape[0], heads_dev * VALUE_WIDTH), jnp.bfloat16),
         ],
         compiler_params=pltpu.CompilerParams(vmem_limit_bytes=24 << 20),
         name="attend",
@@ -494,7 +521,7 @@
         in_specs=[vmem, hbm, vmem, vmem, vmem],
         scratch_shapes=[
             pltpu.VMEM(out_weight.shape, jnp.bfloat16),
-            pltpu.SemaphoreType.DMA,
+            pltpu.SemaphoreType.DMA((8,)),
         ],
         compiler_params=pltpu.CompilerParams(vmem_limit_bytes=16 << 20),
         name="mix",
@@ -529,7 +556,7 @@
         ],
         compiler_params=pltpu.CompilerParams(vmem_limit_bytes=40 << 20),
         name="expert",
-    )(arrived.reshape(experts_all * GROUP, main), *map(in_hbm, weights))
+    )(arrived.reshape(experts_all * GROUP, main), *map(in_hbm, weights[:-4]), *weights[-4:])
     returned = lax.all_to_all(
         result_rows.reshape(experts_all, GROUP, main), SP, 0, 0, tiled=True
     )

time: 301 us -> 300 us (level)
  no operation moved by 1% of the time
where the time goes in v4:
time: 300 us; the launch traced here: 298 us
  waiting for transfers between devices  146 us (49%)
  blocking collectives  76.9 us (26%)
  starting transfers between devices  37.7 us (13%)
  Pallas kernels  28.9 us (10%)
  local copies, waits for them, and re-layouts  5.89 us (2%)
    ppermute x12, waiting for transfers between devices, shifted(): lax.ppermute(array, axis, [(i, (i + step) % count) for i in range(count)])  91.7 us
    all_to_all x1, waiting for transfers between devices, on_device(): lax.all_to_all(result_rows.reshape(experts_all, GROUP, main), SP, 0, 0, t...  48.4 us
    all_gather x1, blocking collectives, on_device(): near = lax.all_gather(sent, 'sp_0', axis=0, tiled=True)  43 us
    all_to_all x1, blocking collectives, on_device(): shares = lax.all_to_all(shares, 'tp', 0, 0, tiled=True)  33.9 us
    ppermute x12, starting transfers between devices, shifted(): lax.ppermute(array, axis, [(i, (i + step) % count) for i in range(count)])  14.8 us
    all_to_all x1, starting transfers between devices, on_device(): lax.all_to_all(result_rows.reshape(experts_all, GROUP, main), SP, 0, 0, t...  13.2 us
    pallas_call x1, Pallas kernels, on_device(): pl.pallas_call(expert_body, out_shape=jax.ShapeDtypeStruct((experts_all *...  9.71 us
    pallas_call x1, Pallas kernels, on_device(): pl.pallas_call(attend_body, out_shape=jax.ShapeDtypeStruct((group, rows_d...  9.53 us
  transfers between devices with their start and end apart: 15, of which 8 were waited for; matrix products, arithmetic and copies ran while one was open for 1% of the time, Pallas kernels for 0%

profile of v4, /device:TPU:34, one launch (start us, length us, event | category | flops | bytes accessed | tf_op | source)
XLA Modules:
  0.0 298.1 jit_solution(7308890342662186984)
XLA Ops:
  0.0 1.3 reshape.132.gain_ref
  2.2 2.0 prepare.1
  4.2 33.9 %all_to_all.20.shares_ref = bf16[4,376,512]{2,1,0:T(8,128)(2,1)S(1)} all-to-all(bf16[4,376,512]{2,1,0:T(8,128)(2,1)S(1)} %get-tuple-element.10), channel_id=1, replica_groups=mesh['grp'=2,'sp_0'=16,'sp_1'=2,'tp'=4] {'tp'}, dimensions={0} | all-to-all | bytes 3080192 | tf_op jit(solution)/shard_map/all_to_all | solution.py:480
  38.1 43.0 %all_gather.3.near_ref = bf16[640,640]{1,0:T(8,128)(2,1)S(1)} all-gather(bf16[40,640]{1,0:T(8,128)(2,1)S(1)} %get-tuple-element.9), channel_id=1, replica_groups=mesh['grp'=2,'sp_0'=16,'sp_1'=2,'tp'=4] {'sp_0'}, dimensions={0}, use_global_device_ids=true | all-gather | bytes 870400 | tf_op jit(solution)/shard_map/all_gather | solution.py:482
  83.4 9.5 %attend.1 = bf16[4,40,1152]{2,1,0:T(8,128)(2,1)} custom-call(s32[1]{0:T(128)} %bitcast.core_ref, bf16[640,640]{1,0:T(8,128)(2,1)S(1)} %all_gather.3.near_ref, bf16[640,640]{1,0:T(8,128)(2,1)S(1)} %collective-permute-done.other_ref, bf16[4,376,512]{2,1,0:T(8,128)(2,1)S(1)} %all_to_all.20.shares_ref, ...), custom_call_target="tpu_custom_call" | custom-call | tf_op jit(solution)/shard_map/attend/pallas_call | solution.py:485
  93.0 4.9 %all-to-all-start.1 = ((bf16[4,40,1152]{2,1,0:T(8,128)(2,1)}), bf16[4,40,1152]{2,1,0:T(8,128)(2,1)S(1)}, u32[]{:S(2)}, u32[]{:S(2)}) async-start(bf16[4,40,1152]{2,1,0:T(8,128)(2,1)} %attend.1), calls=%async_computation.1 | async-start | bytes 737280 | tf_op jit(solution)/shard_map/all_to_all | solution.py:506
  98.5 6.4 %all-to-all-done.1.parts_ref = bf16[4,40,1152]{2,1,0:T(8,128)(2,1)S(1)} async-done(((bf16[4,40,1152]{2,1,0:T(8,128)(2,1)}), bf16[4,40,1152]{2,1,0:T(8,128)(2,1)S(1)}, u32[]{:S(2)}, u32[]{:S(2)}) %all-to-all-start.1) | async-done | bytes 368672 | tf_op jit(solution)/shard_map/all_to_all | solution.py:506
  104.8 5.6 %mix.1 = (bf16[40,2048]{1,0:T(8,128)(2,1)S(1)}, bf16[256,1792]{1,0:T(8,128)(2,1)}) custom-call(bf16[4,40,1152]{2,1,0:T(8,128)(2,1)S(1)} %all-to-all-done.1.parts_ref, bf16[1024,2048]{1,0:T(8,128)(2,1)} %weight_hbm.1, bf16[40,2048]{1,0:T(8,128)(2,1)} %residual_ref.1, bf16[1,2048]{1,0:T(2,128)(2,1)} %reshape.133.gain_ref, s32[4,40]{1,0:T(4,128)} %bitcast.14), custom_call_target="tpu_custom_call" | custom-call | tf_op jit(solution)/shard_map/mix/pallas_call | solution.py:515
  111.1 4.8 %all-to-all-start.2 = ((bf16[32,8,1792]{2,1,0:T(8,128)(2,1)}), bf16[32,8,1792]{2,1,0:T(8,128)(2,1)S(1)}, u32[]{:S(2)}, u32[]{:S(2)}) async-start(bf16[32,8,1792]{2,1,0:T(8,128)(2,1)} %bitcast.4), calls=%async_computation.2 | async-start | bytes 1835008 | tf_op jit(solution)/shard_map/all_to_all | solution.py:529
  116.3 2.0 collective-permute-start.2
  118.4 3.1 %collective-permute-start.7 = (bf16[256,2048]{1,0:T(8,128)(2,1)}, bf16[256,2048]{1,0:T(8,128)(2,1)S(1)}, u32[]{:S(2)}, u32[]{:S(2)}) collective-permute-start(bf16[256,2048]{1,0:T(8,128)(2,1)} %bitcast.8.refs_2_), channel_id=1, source_target_pairs={{0,3},{1,0},{2,1},{3,2},{4,7},{5,4},{6,5},{7,6},{8,11},{9,8},{10,9... | collective-permute-start | bytes 3145736 | tf_op jit(solution)/shard_map/ppermute | solution.py:61
  121.5 21.0 %collective-permute-done.4.refs_5_ = bf16[256,2048]{1,0:T(8,128)(2,1)S(1)} collective-permute-done((bf16[256,2048]{1,0:T(8,128)(2,1)}, bf16[256,2048]{1,0:T(8,128)(2,1)S(1)}, u32[]{:S(2)}, u32[]{:S(2)}) %collective-permute-start.4) | collective-permute-done | bytes 1048608 | tf_op jit(solution)/shard_map/ppermute | solution.py:61
  142.5 2.6 collective-permute-start.5
  145.2 19.8 %collective-permute-done.2.refs_3_ = bf16[2048,256]{1,0:T(8,128)(2,1)S(1)} collective-permute-done((bf16[2048,256]{1,0:T(8,128)(2,1)}, bf16[2048,256]{1,0:T(8,128)(2,1)S(1)}, u32[]{:S(2)}, u32[]{:S(2)}) %collective-permute-start.2) | collective-permute-done | bytes 1048608 | tf_op jit(solution)/shard_map/ppermute | solution.py:61
  165.0 2.8 collective-permute-start.9
  167.8 1.2 collective-permute-start.10
  169.1 18.4 %collective-permute-done.3.refs_4_ = bf16[2048,256]{1,0:T(8,128)(2,1)S(1)} collective-permute-done((bf16[2048,256]{1,0:T(8,128)(2,1)}, bf16[2048,256]{1,0:T(8,128)(2,1)S(1)}, u32[]{:S(2)}, u32[]{:S(2)}) %collective-permute-start.3) | collective-permute-done | bytes 1048608 | tf_op jit(solution)/shard_map/ppermute | solution.py:61
  187.5 2.6 collective-permute-start.11
  190.1 29.6 %collective-permute-done.10.refs_11_ = bf16[128,2048]{1,0:T(8,128)(2,1)S(1)} collective-permute-done((bf16[128,2048]{1,0:T(8,128)(2,1)S(1)}, bf16[128,2048]{1,0:T(8,128)(2,1)S(1)}, u32[]{:S(2)}, u32[]{:S(2)}) %collective-permute-start.10) | collective-permute-done | bytes 524320 | tf_op jit(solution)/shard_map/ppermute | solution.py:61
  219.7 1.8 collective-permute-done.11.refs_12_
  223.4 9.7 %expert.1 = bf16[256,1792]{1,0:T(8,128)(2,1)} custom-call(bf16[256,1792]{1,0:T(8,128)(2,1)S(1)} %bitcast.11, bf16[2048,256]{1,0:T(8,128)(2,1)} %bitcast.6.refs_0_, bf16[2048,256]{1,0:T(8,128)(2,1)} %bitcast.7.refs_1_, bf16[256,2048]{1,0:T(8,128)(2,1)} %bitcast.8.refs_2_, bf16[2048,256]{1,0:T(8,128)(2,1)} %copy-done.6, bf16[2048,256]{1,0:T(8,128)(2,1)} %copy-done.8, ...), custom_call_target="tpu_custom_call" | custom-call | tf_op jit(solution)/shard_map/expert/pallas_call | solution.py:548
  233.1 13.2 %all-to-all-start.3 = ((bf16[32,8,1792]{2,1,0:T(8,128)(2,1)}), bf16[32,8,1792]{2,1,0:T(8,128)(2,1)S(1)}, u32[]{:S(2)}, u32[]{:S(2)}) async-start(bf16[32,8,1792]{2,1,0:T(8,128)(2,1)} %bitcast.9), calls=%async_computation.3 | async-start | bytes 1835008 | tf_op jit(solution)/shard_map/all_to_all | solution.py:560
  247.7 48.4 %all-to-all-done.3 = bf16[32,8,1792]{2,1,0:T(8,128)(2,1)S(1)} async-done(((bf16[32,8,1792]{2,1,0:T(8,128)(2,1)}), bf16[32,8,1792]{2,1,0:T(8,128)(2,1)S(1)}, u32[]{:S(2)}, u32[]{:S(2)}) %all-to-all-start.3) | async-done | bytes 917536 | tf_op jit(solution)/shard_map/all_to_all | solution.py:560
  296.0 2.0 combine.1
  (54 shorter events, 8.3 us)
Async XLA Ops:
  38.1 45.3 %collective-permute-start.1 = (bf16[4,376,512]{2,1,0:T(8,128)(2,1)S(1)}, bf16[4,376,512]{2,1,0:T(8,128)(2,1)S(1)}, u32[]{:S(2)}, u32[]{:S(2)}) collective-permute-start(bf16[4,376,512]{2,1,0:T(8,128)(2,1)S(1)} %all_to_all.20.shares_ref), channel_id=1, source_target_pairs={{0,4},{4,0},{1,5},{5,1},{2,6},{6,2},{3,7},{7,3},{8,12},{12,8},{9,1... | collective-permute-start | bytes 4620296 | tf_op jit(solution)/shard_map/ppermute | solution.py:61
  81.1 2.3 collective-permute-start
  83.4 14.4 %copy-start.11 = (bf16[2048]{0:T(1024)(128)(2,1)S(1)}, bf16[2048]{0:T(1024)(128)(2,1)}, u32[]{:S(2)}) copy-start(bf16[2048]{0:T(1024)(128)(2,1)} %param.26) | copy-start | bytes 12292
  93.0 11.9 %all-to-all-start.1 = ((bf16[4,40,1152]{2,1,0:T(8,128)(2,1)}), bf16[4,40,1152]{2,1,0:T(8,128)(2,1)S(1)}, u32[]{:S(2)}, u32[]{:S(2)}) async-start(bf16[4,40,1152]{2,1,0:T(8,128)(2,1)} %attend.1), calls=%async_computation.1 | async-start | bytes 737280 | tf_op jit(solution)/shard_map/all_to_all | solution.py:506
  111.1 111.2 %all-to-all-start.2 = ((bf16[32,8,1792]{2,1,0:T(8,128)(2,1)}), bf16[32,8,1792]{2,1,0:T(8,128)(2,1)S(1)}, u32[]{:S(2)}, u32[]{:S(2)}) async-start(bf16[32,8,1792]{2,1,0:T(8,128)(2,1)} %bitcast.4), calls=%async_computation.2 | async-start | bytes 1835008 | tf_op jit(solution)/shard_map/all_to_all | solution.py:529
  116.0 26.5 %collective-permute-start.4 = (bf16[256,2048]{1,0:T(8,128)(2,1)}, bf16[256,2048]{1,0:T(8,128)(2,1)S(1)}, u32[]{:S(2)}, u32[]{:S(2)}) collective-permute-start(bf16[256,2048]{1,0:T(8,128)(2,1)} %bitcast.8.refs_2_), channel_id=1, source_target_pairs={{0,1},{1,2},{2,3},{3,0},{4,5},{5,6},{6,7},{7,4},{8,9},{9,10},{10,1... | collective-permute-start | bytes 3145736 | tf_op jit(solution)/shard_map/ppermute | solution.py:61
  116.3 48.7 %collective-permute-start.2 = (bf16[2048,256]{1,0:T(8,128)(2,1)}, bf16[2048,256]{1,0:T(8,128)(2,1)S(1)}, u32[]{:S(2)}, u32[]{:S(2)}) collective-permute-start(bf16[2048,256]{1,0:T(8,128)(2,1)} %bitcast.6.refs_0_), channel_id=1, source_target_pairs={{0,1},{1,2},{2,3},{3,0},{4,5},{5,6},{6,7},{7,4},{8,9},{9,10},{10,1... | collective-permute-start | bytes 3145736 | tf_op jit(solution)/shard_map/ppermute | solution.py:61
  118.3 46.8 %collective-permute-start.6 = (bf16[2048,256]{1,0:T(8,128)(2,1)}, bf16[2048,256]{1,0:T(8,128)(2,1)S(1)}, u32[]{:S(2)}, u32[]{:S(2)}) collective-permute-start(bf16[2048,256]{1,0:T(8,128)(2,1)} %bitcast.7.refs_1_), channel_id=1, source_target_pairs={{0,3},{1,0},{2,1},{3,2},{4,7},{5,4},{6,5},{7,6},{8,11},{9,8},{10,9... | collective-permute-start | bytes 3145736 | tf_op jit(solution)/shard_map/ppermute | solution.py:61
  118.4 49.4 %collective-permute-start.7 = (bf16[256,2048]{1,0:T(8,128)(2,1)}, bf16[256,2048]{1,0:T(8,128)(2,1)S(1)}, u32[]{:S(2)}, u32[]{:S(2)}) collective-permute-start(bf16[256,2048]{1,0:T(8,128)(2,1)} %bitcast.8.refs_2_), channel_id=1, source_target_pairs={{0,3},{1,0},{2,1},{3,2},{4,7},{5,4},{6,5},{7,6},{8,11},{9,8},{10,9... | collective-permute-start | bytes 3145736 | tf_op jit(solution)/shard_map/ppermute | solution.py:61
  121.5 65.9 %collective-permute-start.3 = (bf16[2048,256]{1,0:T(8,128)(2,1)}, bf16[2048,256]{1,0:T(8,128)(2,1)S(1)}, u32[]{:S(2)}, u32[]{:S(2)}) collective-permute-start(bf16[2048,256]{1,0:T(8,128)(2,1)} %bitcast.7.refs_1_), channel_id=1, source_target_pairs={{0,1},{1,2},{2,3},{3,0},{4,5},{5,6},{6,7},{7,4},{8,9},{9,10},{10,1... | collective-permute-start | bytes 3145736 | tf_op jit(solution)/shard_map/ppermute | solution.py:61
  142.5 79.8 %copy-start.4 = (bf16[256,2048]{1,0:T(8,128)(2,1)}, bf16[256,2048]{1,0:T(8,128)(2,1)S(1)}, u32[]{:S(2)}) copy-start(bf16[256,2048]{1,0:T(8,128)(2,1)S(1)} %collective-permute-done.4.refs_5_) | copy-start | bytes 3145732
  142.5 47.6 %collective-permute-start.5 = (bf16[2048,256]{1,0:T(8,128)(2,1)}, bf16[2048,256]{1,0:T(8,128)(2,1)S(1)}, u32[]{:S(2)}, u32[]{:S(2)}) collective-permute-start(bf16[2048,256]{1,0:T(8,128)(2,1)} %bitcast.6.refs_0_), channel_id=1, source_target_pairs={{0,3},{1,0},{2,1},{3,2},{4,7},{5,4},{6,5},{7,6},{8,11},{9,8},{10,9... | collective-permute-start | bytes 3145736 | tf_op jit(solution)/shard_map/ppermute | solution.py:61
  165.0 57.3 %copy-start.6 = (bf16[2048,256]{1,0:T(8,128)(2,1)}, bf16[2048,256]{1,0:T(8,128)(2,1)S(1)}, u32[]{:S(2)}) copy-start(bf16[2048,256]{1,0:T(8,128)(2,1)S(1)} %collective-permute-done.2.refs_3_) | copy-start | bytes 3145732
  165.0 57.3 %collective-permute-start.8 = (bf16[2048,256]{1,0:T(8,128)(2,1)S(1)}, bf16[2048,256]{1,0:T(8,128)(2,1)S(1)}, u32[]{:S(2)}, u32[]{:S(2)}) collective-permute-start(bf16[2048,256]{1,0:T(8,128)(2,1)S(1)} %collective-permute-done.2.refs_3_), channel_id=1, source_target_pairs={{0,1},{1,2},{2,3},{3,0},{4,5},{5,6},{6,7},{7,4},{8,9},{9,10},{10,1... | collective-permute-start | bytes 3145736 | tf_op jit(solution)/shard_map/ppermute | solution.py:61
  165.0 57.3 %copy-start.7 = (bf16[2048,256]{1,0:T(8,128)(2,1)}, bf16[2048,256]{1,0:T(8,128)(2,1)S(1)}, u32[]{:S(2)}) copy-start(bf16[2048,256]{1,0:T(8,128)(2,1)S(1)} %collective-permute-done.6.refs_7_) | copy-start | bytes 3145732
  165.0 57.3 %collective-permute-start.9 = (bf16[2048,256]{1,0:T(8,128)(2,1)S(1)}, bf16[2048,256]{1,0:T(8,128)(2,1)S(1)}, u32[]{:S(2)}, u32[]{:S(2)}) collective-permute-start(bf16[2048,256]{1,0:T(8,128)(2,1)S(1)} %collective-permute-done.6.refs_7_), channel_id=1, source_target_pairs={{0,3},{1,0},{2,1},{3,2},{4,7},{5,4},{6,5},{7,6},{8,11},{9,8},{10,9... | collective-permute-start | bytes 3145736 | tf_op jit(solution)/shard_map/ppermute | solution.py:61
  167.8 54.5 %copy-start.5 = (bf16[256,2048]{1,0:T(8,128)(2,1)}, bf16[256,2048]{1,0:T(8,128)(2,1)S(1)}, u32[]{:S(2)}) copy-start(bf16[256,2048]{1,0:T(8,128)(2,1)S(1)} %collective-permute-done.7.refs_8_) | copy-start | bytes 3145732
  167.8 51.8 %collective-permute-start.10 = (bf16[128,2048]{1,0:T(8,128)(2,1)S(1)}, bf16[128,2048]{1,0:T(8,128)(2,1)S(1)}, u32[]{:S(2)}, u32[]{:S(2)}) collective-permute-start(bf16[128,2048]{1,0:T(8,128)(2,1)S(1)} %slice.8), channel_id=1, source_target_pairs={{0,1},{1,2},{2,3},{3,0},{4,5},{5,6},{6,7},{7,4},{8,9},{9,10},{10,1... | collective-permute-start | bytes 1572872 | tf_op jit(solution)/shard_map/ppermute | solution.py:61
  187.5 34.8 %copy-start.8 = (bf16[2048,256]{1,0:T(8,128)(2,1)}, bf16[2048,256]{1,0:T(8,128)(2,1)S(1)}, u32[]{:S(2)}) copy-start(bf16[2048,256]{1,0:T(8,128)(2,1)S(1)} %collective-permute-done.3.refs_4_) | copy-start | bytes 3145732
  187.5 34.0 %collective-permute-start.11 = (bf16[128,2048]{1,0:T(8,128)(2,1)S(1)}, bf16[128,2048]{1,0:T(8,128)(2,1)S(1)}, u32[]{:S(2)}, u32[]{:S(2)}) collective-permute-start(bf16[128,2048]{1,0:T(8,128)(2,1)S(1)} %slice.9), channel_id=1, source_target_pairs={{0,3},{1,0},{2,1},{3,2},{4,7},{5,4},{6,5},{7,6},{8,11},{9,8},{10,9... | collective-permute-start | bytes 1572872 | tf_op jit(solution)/shard_map/ppermute | solution.py:61
  190.1 32.2 %copy-start.9 = (bf16[2048,256]{1,0:T(8,128)(2,1)}, bf16[2048,256]{1,0:T(8,128)(2,1)S(1)}, u32[]{:S(2)}) copy-start(bf16[2048,256]{1,0:T(8,128)(2,1)S(1)} %collective-permute-done.5.refs_6_) | copy-start | bytes 3145732
  233.1 13.9 %copy-start.12 = (f32[40,4]{0,1:T(4,128)S(1)}, f32[40,4]{0,1:T(4,128)}, u32[]{:S(2)}) copy-start(f32[40,4]{0,1:T(4,128)} %param.31) | copy-start | bytes 1924
  233.1 62.9 %copy-start.3 = (bf16[40,2048]{1,0:T(8,128)(2,1)S(1)}, bf16[40,2048]{1,0:T(8,128)(2,1)}, u32[]{:S(2)}) copy-start(bf16[40,2048]{1,0:T(8,128)(2,1)} %copy-done.2) | copy-start | bytes 491524
  233.1 62.9 %all-to-all-start.3 = ((bf16[32,8,1792]{2,1,0:T(8,128)(2,1)}), bf16[32,8,1792]{2,1,0:T(8,128)(2,1)S(1)}, u32[]{:S(2)}, u32[]{:S(2)}) async-start(bf16[32,8,1792]{2,1,0:T(8,128)(2,1)} %bitcast.9), calls=%async_computation.3 | async-start | bytes 1835008 | tf_op jit(solution)/shard_map/all_to_all | solution.py:560
  (4 other events, 15.7 us)

commit v5 on v4

--- a/solution.py
+++ b/solution.py
@@ -442,7 +442,7 @@
             grid=(1,),
             in_specs=[
                 pl.BlockSpec((rows_dev, latent_width), lambda i, at: (at[0], 0)),
-                whole(1, latent_width),
+                whole(latent_width),
                 whole(QK_ROPE, tok_dev),
                 whole(rows_dev, QK_ROPE),
                 whole(rows_dev, QK_ROPE),
@@ -465,7 +465,7 @@
             in_hbm,
             (
                 latent,
-                latent_norm_scale.reshape(1, latent_width),
+                latent_norm_scale,
                 key_turn.T,
                 own_cos,
                 own_sin,
@@ -484,7 +484,9 @@
 
     parts = pl.pallas_call(
         attend_body,
-        out_shape=jax.ShapeDtypeStruct((group, rows_dev, group * heads_dev * VALUE_WIDTH + STAT_LANES), jnp.bfloat16),
+        out_shape=pltpu.HBM(
+            (group, rows_dev, group * heads_dev * VALUE_WIDTH + STAT_LANES), jnp.bfloat16
+        ),
         in_specs=[pl.BlockSpec(memory_space=pltpu.SMEM)]
         + [pl.BlockSpec(memory_space=pltpu.VMEM)] * 7,
         scratch_shapes=[
@@ -516,7 +518,7 @@
         mix_body,
         out_shape=(
             jax.ShapeDtypeStruct((rows_dev, model_width), jnp.bfloat16),
-            jax.ShapeDtypeStruct((experts_all * GROUP, main), jnp.bfloat16),
+            pltpu.HBM((experts_all * GROUP, main), jnp.bfloat16),
         ),
         in_specs=[vmem, hbm, vmem, vmem, vmem],
         scratch_shapes=[
@@ -525,7 +527,13 @@
         ],
         compiler_params=pltpu.CompilerParams(vmem_limit_bytes=16 << 20),
         name="mix",
-    )(gathered, in_hbm(out_weight), in_hbm(residual), in_hbm(ffn_gain.reshape(1, model_width)), in_hbm(routes.T))
+    )(
+        gathered,
+        in_hbm(out_weight),
+        in_hbm(residual),
+        in_hbm(ffn_gain),
+        in_hbm(routes.T),
+    )
     arrived = lax.all_to_all(
         outgoing.reshape(experts_all, GROUP, main), SP, 0, 0, tiled=True
     )
@@ -542,12 +550,12 @@
     far_down_r = shifted(right[2][cut:], "tp", -1)
 
     weights = []
-    for quarter_weights in (own, left, right):
-        weights += list(quarter_weights)
+    for gate_w, up_w, down_w in (own, left, right):
+        weights += [gate_w, up_w, down_w]
     weights += [far_gate, far_up, far_down_l, far_down_r]
     result_rows = pl.pallas_call(
         expert_body,
-        out_shape=jax.ShapeDtypeStruct((experts_all * GROUP, main), jnp.bfloat16),
+        out_shape=pltpu.HBM((experts_all * GROUP, main), jnp.bfloat16),
         in_specs=[vmem] + [hbm] * len(weights),
         scratch_shapes=[
             pltpu.VMEM((group, 2) + own[0].shape, jnp.bfloat16),
@@ -556,7 +564,7 @@
         ],
         compiler_params=pltpu.CompilerParams(vmem_limit_bytes=40 << 20),
         name="expert",
-    )(arrived.reshape(experts_all * GROUP, main), *map(in_hbm, weights[:-4]), *weights[-4:])
+    )(arrived.reshape(experts_all * GROUP, main), *map(in_hbm, weights))
     returned = lax.all_to_all(
         result_rows.reshape(experts_all, GROUP, main), SP, 0, 0, tiled=True
     )

time: 300 us -> 298 us (level)
  blocking collectives: 76.9 us -> 88.7 us
  waiting for transfers between devices: 146 us -> 140 us
  starting transfers between devices: 37.7 us -> 32.7 us
    all_to_all x0 -> x1, blocking collectives: none -> 11.9 us  [on_device(): gathered = lax.all_to_all(parts, 'tp', 0, 0, tiled=True)]
    all_to_all x1 -> x0, waiting for transfers between devices: 6.36 us -> none  [on_device(): gathered = lax.all_to_all(parts, 'tp', 0, 0, tiled=True)]
    all_to_all x1 -> x0, starting transfers between devices: 4.89 us -> none  [on_device(): gathered = lax.all_to_all(parts, 'tp', 0, 0, tiled=True)]
  transfers between devices with their start and end apart: 15 -> 14, of which waited for: 8 -> 7; matrix products, arithmetic and copies ran while one was open for 1% -> 1% of each run, Pallas kernels for 0% -> 0%
where the time goes in v5:
time: 298 us; the launch traced here: 296 us
  waiting for transfers between devices  140 us (47%)
  blocking collectives  88.7 us (30%)
  starting transfers between devices  32.7 us (11%)
  Pallas kernels  29 us (10%)
  local copies, waits for them, and re-layouts  3.24 us (1%)
    ppermute x12, waiting for transfers between devices, shifted(): lax.ppermute(array, axis, [(i, (i + step) % count) for i in range(count)])  91.7 us
    all_to_all x1, waiting for transfers between devices, on_device(): lax.all_to_all(result_rows.reshape(experts_all, GROUP, main), SP, 0, 0, t...  48.3 us
    all_gather x1, blocking collectives, on_device(): near = lax.all_gather(sent, 'sp_0', axis=0, tiled=True)  43 us
    all_to_all x1, blocking collectives, on_device(): shares = lax.all_to_all(shares, 'tp', 0, 0, tiled=True)  33.9 us
    ppermute x12, starting transfers between devices, shifted(): lax.ppermute(array, axis, [(i, (i + step) % count) for i in range(count)])  14.9 us
    all_to_all x1, starting transfers between devices, on_device(): lax.all_to_all(result_rows.reshape(experts_all, GROUP, main), SP, 0, 0, t...  13 us
    all_to_all x1, blocking collectives, on_device(): gathered = lax.all_to_all(parts, 'tp', 0, 0, tiled=True)  11.9 us
    pallas_call x1, Pallas kernels, on_device(): pl.pallas_call(expert_body, out_shape=pltpu.HBM((experts_all * GROUP, mai...  9.86 us
  transfers between devices with their start and end apart: 14, of which 7 were waited for; matrix products, arithmetic and copies ran while one was open for 1% of the time, Pallas kernels for 0%

profile of v5, /device:TPU:34, one launch (start us, length us, event | category | flops | bytes accessed | tf_op | source)
XLA Modules:
  0.0 296.0 jit_solution(7508515209791570339)
XLA Ops:
  0.9 2.0 prepare.1
  2.9 33.9 %all_to_all.20.shares_ref = bf16[4,376,512]{2,1,0:T(8,128)(2,1)S(1)} all-to-all(bf16[4,376,512]{2,1,0:T(8,128)(2,1)S(1)} %get-tuple-element.10), channel_id=1, replica_groups=mesh['grp'=2,'sp_0'=16,'sp_1'=2,'tp'=4] {'tp'}, dimensions={0} | all-to-all | bytes 3080192 | tf_op jit(solution)/shard_map/all_to_all | solution.py:480
  36.9 43.0 %all_gather.3.near_ref = bf16[640,640]{1,0:T(8,128)(2,1)S(1)} all-gather(bf16[40,640]{1,0:T(8,128)(2,1)S(1)} %get-tuple-element.9), channel_id=1, replica_groups=mesh['grp'=2,'sp_0'=16,'sp_1'=2,'tp'=4] {'sp_0'}, dimensions={0}, use_global_device_ids=true | all-gather | bytes 870400 | tf_op jit(solution)/shard_map/all_gather | solution.py:482
  79.9 1.1 fusion
  80.9 1.2 collective-permute-done.other_ref
  82.2 9.4 %attend.1 = bf16[4,40,1152]{2,1,0:T(8,128)(2,1)} custom-call(s32[1]{0:T(128)} %bitcast.core_ref, bf16[640,640]{1,0:T(8,128)(2,1)S(1)} %all_gather.3.near_ref, bf16[640,640]{1,0:T(8,128)(2,1)S(1)} %collective-permute-done.other_ref, bf16[4,376,512]{2,1,0:T(8,128)(2,1)S(1)} %all_to_all.20.shares_ref, ...), custom_call_target="tpu_custom_call" | custom-call | tf_op jit(solution)/shard_map/attend/pallas_call | solution.py:485
  91.6 11.9 %all_to_all.21.parts_ref = bf16[4,40,1152]{2,1,0:T(8,128)(2,1)S(1)} all-to-all(bf16[4,40,1152]{2,1,0:T(8,128)(2,1)} %attend.1), channel_id=1, replica_groups=mesh['grp'=2,'sp_0'=16,'sp_1'=2,'tp'=4] {'tp'}, dimensions={0} | all-to-all | bytes 737280 | tf_op jit(solution)/shard_map/all_to_all | solution.py:508
  103.4 5.7 %mix.1 = (bf16[40,2048]{1,0:T(8,128)(2,1)S(1)}, bf16[256,1792]{1,0:T(8,128)(2,1)}) custom-call(bf16[4,40,1152]{2,1,0:T(8,128)(2,1)S(1)} %all_to_all.21.parts_ref, bf16[1024,2048]{1,0:T(8,128)(2,1)} %weight_hbm.1, bf16[40,2048]{1,0:T(8,128)(2,1)} %residual_ref.1, bf16[2048]{0:T(1024)(128)(2,1)} %gain_ref.3, s32[4,40]{1,0:T(4,128)} %bitcast.16), custom_call_target="tpu_custom_call" | custom-call | tf_op jit(solution)/shard_map/mix/pallas_call | solution.py:517
  109.1 4.8 %all-to-all-start.2 = ((bf16[32,8,1792]{2,1,0:T(8,128)(2,1)}), bf16[32,8,1792]{2,1,0:T(8,128)(2,1)S(1)}, u32[]{:S(2)}, u32[]{:S(2)}) async-start(bf16[32,8,1792]{2,1,0:T(8,128)(2,1)} %bitcast.14), calls=%async_computation.2 | async-start | bytes 1835008 | tf_op jit(solution)/shard_map/all_to_all | solution.py:537
  114.6 1.7 collective-permute-start.2
  116.6 3.0 collective-permute-start.7
  119.6 21.0 %collective-permute-done.4.refs_5_ = bf16[256,2048]{1,0:T(8,128)(2,1)S(1)} collective-permute-done((bf16[256,2048]{1,0:T(8,128)(2,1)}, bf16[256,2048]{1,0:T(8,128)(2,1)S(1)}, u32[]{:S(2)}, u32[]{:S(2)}) %collective-permute-start.4) | collective-permute-done | bytes 1048608 | tf_op jit(solution)/shard_map/ppermute | solution.py:61
  140.5 2.7 collective-permute-start.5
  143.2 19.8 %collective-permute-done.2.refs_3_ = bf16[2048,256]{1,0:T(8,128)(2,1)S(1)} collective-permute-done((bf16[2048,256]{1,0:T(8,128)(2,1)}, bf16[2048,256]{1,0:T(8,128)(2,1)S(1)}, u32[]{:S(2)}, u32[]{:S(2)}) %collective-permute-start.2) | collective-permute-done | bytes 1048608 | tf_op jit(solution)/shard_map/ppermute | solution.py:61
  163.3 2.5 collective-permute-start.9
  165.9 1.2 collective-permute-start.10
  167.1 18.3 %collective-permute-done.3.refs_4_ = bf16[2048,256]{1,0:T(8,128)(2,1)S(1)} collective-permute-done((bf16[2048,256]{1,0:T(8,128)(2,1)}, bf16[2048,256]{1,0:T(8,128)(2,1)S(1)}, u32[]{:S(2)}, u32[]{:S(2)}) %collective-permute-start.3) | collective-permute-done | bytes 1048608 | tf_op jit(solution)/shard_map/ppermute | solution.py:61
  185.5 2.7 collective-permute-start.11
  188.1 29.6 %collective-permute-done.10.refs_11_ = bf16[128,2048]{1,0:T(8,128)(2,1)S(1)} collective-permute-done((bf16[128,2048]{1,0:T(8,128)(2,1)S(1)}, bf16[128,2048]{1,0:T(8,128)(2,1)S(1)}, u32[]{:S(2)}, u32[]{:S(2)}) %collective-permute-start.10) | collective-permute-done | bytes 524320 | tf_op jit(solution)/shard_map/ppermute | solution.py:61
  217.7 1.8 collective-permute-done.11.refs_12_
  221.3 9.9 %expert.1 = bf16[256,1792]{1,0:T(8,128)(2,1)} custom-call(bf16[256,1792]{1,0:T(8,128)(2,1)S(1)} %bitcast.11, bf16[2048,256]{1,0:T(8,128)(2,1)} %bitcast.6.refs_0_, bf16[2048,256]{1,0:T(8,128)(2,1)} %bitcast.7.refs_1_, bf16[256,2048]{1,0:T(8,128)(2,1)} %bitcast.8.refs_2_, bf16[2048,256]{1,0:T(8,128)(2,1)} %copy-done.2, bf16[2048,256]{1,0:T(8,128)(2,1)} %copy-done.4, ...), custom_call_target="tpu_custom_call" | custom-call | tf_op jit(solution)/shard_map/expert/pallas_call | solution.py:556
  231.2 13.0 %all-to-all-start.3 = ((bf16[32,8,1792]{2,1,0:T(8,128)(2,1)}), bf16[32,8,1792]{2,1,0:T(8,128)(2,1)S(1)}, u32[]{:S(2)}, u32[]{:S(2)}) async-start(bf16[32,8,1792]{2,1,0:T(8,128)(2,1)} %bitcast.13), calls=%async_computation.3 | async-start | bytes 1835008 | tf_op jit(solution)/shard_map/all_to_all | solution.py:568
  245.6 48.3 %all-to-all-done.3 = bf16[32,8,1792]{2,1,0:T(8,128)(2,1)S(1)} async-done(((bf16[32,8,1792]{2,1,0:T(8,128)(2,1)}), bf16[32,8,1792]{2,1,0:T(8,128)(2,1)S(1)}, u32[]{:S(2)}, u32[]{:S(2)}) %all-to-all-start.3) | async-done | bytes 917536 | tf_op jit(solution)/shard_map/all_to_all | solution.py:568
  293.9 2.0 combine.1
  (47 shorter events, 5.3 us)
Async XLA Ops:
  36.9 45.3 %collective-permute-start.1 = (bf16[4,376,512]{2,1,0:T(8,128)(2,1)S(1)}, bf16[4,376,512]{2,1,0:T(8,128)(2,1)S(1)}, u32[]{:S(2)}, u32[]{:S(2)}) collective-permute-start(bf16[4,376,512]{2,1,0:T(8,128)(2,1)S(1)} %all_to_all.20.shares_ref), channel_id=1, source_target_pairs={{0,4},{4,0},{1,5},{5,1},{2,6},{6,2},{3,7},{7,3},{8,12},{12,8},{9,1... | collective-permute-start | bytes 4620296 | tf_op jit(solution)/shard_map/ppermute | solution.py:61
  79.8 2.3 collective-permute-start
  109.1 112.1 %all-to-all-start.2 = ((bf16[32,8,1792]{2,1,0:T(8,128)(2,1)}), bf16[32,8,1792]{2,1,0:T(8,128)(2,1)S(1)}, u32[]{:S(2)}, u32[]{:S(2)}) async-start(bf16[32,8,1792]{2,1,0:T(8,128)(2,1)} %bitcast.14), calls=%async_computation.2 | async-start | bytes 1835008 | tf_op jit(solution)/shard_map/all_to_all | solution.py:537
  114.0 26.5 %collective-permute-start.4 = (bf16[256,2048]{1,0:T(8,128)(2,1)}, bf16[256,2048]{1,0:T(8,128)(2,1)S(1)}, u32[]{:S(2)}, u32[]{:S(2)}) collective-permute-start(bf16[256,2048]{1,0:T(8,128)(2,1)} %bitcast.8.refs_2_), channel_id=1, source_target_pairs={{0,1},{1,2},{2,3},{3,0},{4,5},{5,6},{6,7},{7,4},{8,9},{9,10},{10,1... | collective-permute-start | bytes 3145736 | tf_op jit(solution)/shard_map/ppermute | solution.py:61
  114.6 48.4 %collective-permute-start.2 = (bf16[2048,256]{1,0:T(8,128)(2,1)}, bf16[2048,256]{1,0:T(8,128)(2,1)S(1)}, u32[]{:S(2)}, u32[]{:S(2)}) collective-permute-start(bf16[2048,256]{1,0:T(8,128)(2,1)} %bitcast.6.refs_0_), channel_id=1, source_target_pairs={{0,1},{1,2},{2,3},{3,0},{4,5},{5,6},{6,7},{7,4},{8,9},{9,10},{10,1... | collective-permute-start | bytes 3145736 | tf_op jit(solution)/shard_map/ppermute | solution.py:61
  116.3 47.0 %collective-permute-start.6 = (bf16[2048,256]{1,0:T(8,128)(2,1)}, bf16[2048,256]{1,0:T(8,128)(2,1)S(1)}, u32[]{:S(2)}, u32[]{:S(2)}) collective-permute-start(bf16[2048,256]{1,0:T(8,128)(2,1)} %bitcast.7.refs_1_), channel_id=1, source_target_pairs={{0,3},{1,0},{2,1},{3,2},{4,7},{5,4},{6,5},{7,6},{8,11},{9,8},{10,9... | collective-permute-start | bytes 3145736 | tf_op jit(solution)/shard_map/ppermute | solution.py:61
  116.6 49.2 %collective-permute-start.7 = (bf16[256,2048]{1,0:T(8,128)(2,1)}, bf16[256,2048]{1,0:T(8,128)(2,1)S(1)}, u32[]{:S(2)}, u32[]{:S(2)}) collective-permute-start(bf16[256,2048]{1,0:T(8,128)(2,1)} %bitcast.8.refs_2_), channel_id=1, source_target_pairs={{0,3},{1,0},{2,1},{3,2},{4,7},{5,4},{6,5},{7,6},{8,11},{9,8},{10,9... | collective-permute-start | bytes 3145736 | tf_op jit(solution)/shard_map/ppermute | solution.py:61
  119.6 65.9 %collective-permute-start.3 = (bf16[2048,256]{1,0:T(8,128)(2,1)}, bf16[2048,256]{1,0:T(8,128)(2,1)S(1)}, u32[]{:S(2)}, u32[]{:S(2)}) collective-permute-start(bf16[2048,256]{1,0:T(8,128)(2,1)} %bitcast.7.refs_1_), channel_id=1, source_target_pairs={{0,1},{1,2},{2,3},{3,0},{4,5},{5,6},{6,7},{7,4},{8,9},{9,10},{10,1... | collective-permute-start | bytes 3145736 | tf_op jit(solution)/shard_map/ppermute | solution.py:61
  140.5 80.7 %copy-start = (bf16[256,2048]{1,0:T(8,128)(2,1)}, bf16[256,2048]{1,0:T(8,128)(2,1)S(1)}, u32[]{:S(2)}) copy-start(bf16[256,2048]{1,0:T(8,128)(2,1)S(1)} %collective-permute-done.4.refs_5_) | copy-start | bytes 3145732
  140.5 47.6 %collective-permute-start.5 = (bf16[2048,256]{1,0:T(8,128)(2,1)}, bf16[2048,256]{1,0:T(8,128)(2,1)S(1)}, u32[]{:S(2)}, u32[]{:S(2)}) collective-permute-start(bf16[2048,256]{1,0:T(8,128)(2,1)} %bitcast.6.refs_0_), channel_id=1, source_target_pairs={{0,3},{1,0},{2,1},{3,2},{4,7},{5,4},{6,5},{7,6},{8,11},{9,8},{10,9... | collective-permute-start | bytes 3145736 | tf_op jit(solution)/shard_map/ppermute | solution.py:61
  163.0 56.5 %copy-start.2 = (bf16[2048,256]{1,0:T(8,128)(2,1)}, bf16[2048,256]{1,0:T(8,128)(2,1)S(1)}, u32[]{:S(2)}) copy-start(bf16[2048,256]{1,0:T(8,128)(2,1)S(1)} %collective-permute-done.2.refs_3_) | copy-start | bytes 3145732
  163.0 56.5 %collective-permute-start.8 = (bf16[2048,256]{1,0:T(8,128)(2,1)S(1)}, bf16[2048,256]{1,0:T(8,128)(2,1)S(1)}, u32[]{:S(2)}, u32[]{:S(2)}) collective-permute-start(bf16[2048,256]{1,0:T(8,128)(2,1)S(1)} %collective-permute-done.2.refs_3_), channel_id=1, source_target_pairs={{0,1},{1,2},{2,3},{3,0},{4,5},{5,6},{6,7},{7,4},{8,9},{9,10},{10,1... | collective-permute-start | bytes 3145736 | tf_op jit(solution)/shard_map/ppermute | solution.py:61
  163.3 56.2 %copy-start.3 = (bf16[2048,256]{1,0:T(8,128)(2,1)}, bf16[2048,256]{1,0:T(8,128)(2,1)S(1)}, u32[]{:S(2)}) copy-start(bf16[2048,256]{1,0:T(8,128)(2,1)S(1)} %collective-permute-done.6.refs_7_) | copy-start | bytes 3145732
  163.3 58.0 %collective-permute-start.9 = (bf16[2048,256]{1,0:T(8,128)(2,1)S(1)}, bf16[2048,256]{1,0:T(8,128)(2,1)}, u32[]{:S(2)}, u32[]{:S(2)}) collective-permute-start(bf16[2048,256]{1,0:T(8,128)(2,1)S(1)} %collective-permute-done.6.refs_7_), channel_id=1, source_target_pairs={{0,3},{1,0},{2,1},{3,2},{4,7},{5,4},{6,5},{7,6},{8,11},{9,8},{10,9... | collective-permute-start | bytes 3145736 | tf_op jit(solution)/shard_map/ppermute | solution.py:61
  165.8 55.4 %copy-start.1 = (bf16[256,2048]{1,0:T(8,128)(2,1)}, bf16[256,2048]{1,0:T(8,128)(2,1)S(1)}, u32[]{:S(2)}) copy-start(bf16[256,2048]{1,0:T(8,128)(2,1)S(1)} %collective-permute-done.7.refs_8_) | copy-start | bytes 3145732
  165.9 51.8 %collective-permute-start.10 = (bf16[128,2048]{1,0:T(8,128)(2,1)S(1)}, bf16[128,2048]{1,0:T(8,128)(2,1)S(1)}, u32[]{:S(2)}, u32[]{:S(2)}) collective-permute-start(bf16[128,2048]{1,0:T(8,128)(2,1)S(1)} %slice.8), channel_id=1, source_target_pairs={{0,1},{1,2},{2,3},{3,0},{4,5},{5,6},{6,7},{7,4},{8,9},{9,10},{10,1... | collective-permute-start | bytes 1572872 | tf_op jit(solution)/shard_map/ppermute | solution.py:61
  185.5 34.0 %copy-start.4 = (bf16[2048,256]{1,0:T(8,128)(2,1)}, bf16[2048,256]{1,0:T(8,128)(2,1)S(1)}, u32[]{:S(2)}) copy-start(bf16[2048,256]{1,0:T(8,128)(2,1)S(1)} %collective-permute-done.3.refs_4_) | copy-start | bytes 3145732
  185.5 34.0 %collective-permute-start.11 = (bf16[128,2048]{1,0:T(8,128)(2,1)S(1)}, bf16[128,2048]{1,0:T(8,128)(2,1)S(1)}, u32[]{:S(2)}, u32[]{:S(2)}) collective-permute-start(bf16[128,2048]{1,0:T(8,128)(2,1)S(1)} %slice.9), channel_id=1, source_target_pairs={{0,3},{1,0},{2,1},{3,2},{4,7},{5,4},{6,5},{7,6},{8,11},{9,8},{10,9... | collective-permute-start | bytes 1572872 | tf_op jit(solution)/shard_map/ppermute | solution.py:61
  188.1 31.4 %copy-start.5 = (bf16[2048,256]{1,0:T(8,128)(2,1)}, bf16[2048,256]{1,0:T(8,128)(2,1)S(1)}, u32[]{:S(2)}) copy-start(bf16[2048,256]{1,0:T(8,128)(2,1)S(1)} %collective-permute-done.5.refs_6_) | copy-start | bytes 3145732
  217.7 1.8 copy-start.7
  220.3 1.0 copy-start.6
  231.1 13.1 %copy-start.9 = (s32[40,4]{0,1:T(4,128)S(1)}, s32[40,4]{0,1:T(4,128)}, u32[]{:S(2)}) copy-start(s32[40,4]{0,1:T(4,128)} %param.30) | copy-start | bytes 1924
  231.2 13.8 %copy-start.10 = (f32[40,4]{0,1:T(4,128)S(1)}, f32[40,4]{0,1:T(4,128)}, u32[]{:S(2)}) copy-start(f32[40,4]{0,1:T(4,128)} %param.31) | copy-start | bytes 1924
  231.2 62.8 %all-to-all-start.3 = ((bf16[32,8,1792]{2,1,0:T(8,128)(2,1)}), bf16[32,8,1792]{2,1,0:T(8,128)(2,1)S(1)}, u32[]{:S(2)}, u32[]{:S(2)}) async-start(bf16[32,8,1792]{2,1,0:T(8,128)(2,1)} %bitcast.13), calls=%async_computation.3 | async-start | bytes 1835008 | tf_op jit(solution)/shard_map/all_to_all | solution.py:568
  (1 other events, 0.8 us)

commit v6 on v5

--- a/solution.py
+++ b/solution.py
@@ -66,6 +66,36 @@
 
 def lanes_of(index, width):
     return slice(index * width, (index + 1) * width)
+
+
+def stage_body(*refs):
+    count = (len(refs) - 1) // 2
+    sems = refs[-1]
+    pieces = sems.shape[1]
+    loads = []
+    for n in range(count):
+        depth = refs[count + n].shape[0] // pieces
+        for i in range(pieces):
+            part = pl.ds(i * depth, depth)
+            loads.append(
+                pltpu.make_async_copy(refs[n].at[part], refs[count + n].at[part], sems.at[n, i])
+            )
+            loads[-1].start()
+    for load in loads:
+        load.wait()
+
+
+def staged(arrays, rows):
+    hbm = pl.BlockSpec(memory_space=pltpu.HBM)
+    vmem = pl.BlockSpec(memory_space=pltpu.VMEM)
+    return pl.pallas_call(
+        stage_body,
+        out_shape=tuple(pltpu.VMEM((rows,) + a.shape[1:], a.dtype) for a in arrays),
+        in_specs=[hbm] * len(arrays),
+        out_specs=(vmem,) * len(arrays),
+        scratch_shapes=[pltpu.SemaphoreType.DMA((len(arrays), 4))],
+        compiler_params=pltpu.CompilerParams(vmem_limit_bytes=16 << 20),
+    )(*map(in_hbm, arrays))
 
 
 def prepare_body(
@@ -212,18 +242,30 @@
 
 
 def mix_body(
-    parts_ref, weight_hbm, residual_ref, gain_ref, routes_ref, hidden_ref, outgoing_ref, weight_ref, sems
+    parts_ref,
+    near_ref,
+    weight_hbm,
+    residual_ref,
+    gain_ref,
+    routes_ref,
+    hidden_ref,
+    outgoing_ref,
+    weight_ref,
+    sems,
 ):
     pieces = sems.shape[0]
     depth = weight_ref.shape[0] // pieces
+    above = near_ref.shape[0]
     loads = []
     for i in range(pieces):
-        part = pl.ds(i * depth, depth)
-        loads.append(pltpu.make_async_copy(weight_hbm.at[part], weight_ref.at[part], sems.at[i]))
+        source = weight_hbm.at[pl.ds(above + i * depth, depth)]
+        loads.append(
+            pltpu.make_async_copy(source, weight_ref.at[pl.ds(i * depth, depth)], sems.at[i])
+        )
         loads[-1].start()
     shards = parts_ref.shape[0]
     rows, model_width = residual_ref.shape
-    wide = weight_ref.shape[0]
+    wide = weight_hbm.shape[0]
     heads = wide // VALUE_WIDTH
     sums = []
     for i in range(shards):
@@ -264,9 +306,12 @@
     ).astype(jnp.int32)
     table = jnp.where((named > 0) & (rank == line % GROUP), 1.0, 0.0).astype(jnp.bfloat16)
 
+    projected = jnp.dot(attended[:, :above], near_ref[...], preferred_element_type=jnp.float32)
     for load in loads:
         load.wait()
-    projected = jnp.dot(attended, weight_ref[...], preferred_element_type=jnp.float32)
+    projected = projected + jnp.dot(
+        attended[:, above:], weight_ref[...], preferred_element_type=jnp.float32
+    )
     hidden = (residual_ref[...].astype(jnp.float32) + projected).astype(jnp.bfloat16)
     hidden_ref[...] = hidden
     normed = norm_scale(hidden, gain_ref[...]).astype(jnp.bfloat16)
@@ -283,24 +328,40 @@
 
 
 def expert_body(arrived_ref, *refs):
-    count = (len(refs) - 5) // 3
-    weights_hbm = refs[: 3 * count + 1]
-    out_ref, thin_ref, down_ref, sems = refs[3 * count + 1 :]
-    gate_up = weights_hbm[0].shape
-    cut = weights_hbm[-1].shape[0]
-    loads = []
-    for i, source in enumerate(weights_hbm):
-        q, m = divmod(i, 3) if i < 3 * count else (count - 1, 3)
-        if m < 2:
-            dst = thin_ref.at[q, m]
-        elif q < count - 1:
-            dst = down_ref.at[q]
-        else:
-            dst = down_ref.at[q, pl.ds((m - 2) * cut, cut)]
-        loads.append(pltpu.make_async_copy(source, dst, sems.at[i]))
-        loads[-1].start()
+    out_ref, gates_ref, ups_ref, down_ref, sems = refs[-5:]
+    own_gate_ref, own_up_ref, *sources = refs[:-5]
+    count = down_ref.shape[0]
+    wanted = []
+    for q in range(count):
+        wanted.append((gates_ref.at[q - 1], ups_ref.at[q - 1], down_ref.at[q]))
+    cut = sources[7].shape[0]
+    long = sources[8].shape[0]
+    short = sources[9].shape[0]
+    targets = [
+        ("down", 0, wanted[0][2]),
+        ("gate", 1, wanted[1][0]),
+        ("down", 1, wanted[1][2]),
+        ("gate", 2, wanted[2][0]),
+        ("down", 2, wanted[2][2]),
+        ("gate", 3, wanted[3][0]),
+        ("down", 3, down_ref.at[3, pl.ds(0, cut)]),
+        ("down", 3, down_ref.at[3, pl.ds(cut, cut)]),
+    ]
+    for q in range(1, count):
+        targets.append(("up", q, ups_ref.at[q - 1, pl.ds(0, long)]))
+        targets.append(("up", q, ups_ref.at[q - 1, pl.ds(long, short)]))
+    loads = {}
+    for i, (source, (kind, q, target)) in enumerate(zip(sources, targets, strict=True)):
+        load = pltpu.make_async_copy(source, target, sems.at[i])
+        load.start()
+        loads.setdefault((kind, q), []).append(load)
+
+    def ready(kind, q):
+        for load in loads.pop((kind, q), ()):
+            load.wait()
+
     rows, main = arrived_ref.shape
-    model_width = gate_up[0]
+    model_width = own_gate_ref.shape[0]
     tail = model_width - main
     line = lax.broadcasted_iota(jnp.int32, (rows, rows), 0)
     column = lax.broadcasted_iota(jnp.int32, (rows, rows), 1)
@@ -315,14 +376,16 @@
     ends = ends.astype(jnp.bfloat16)
     actives = []
     for q in range(count):
-        loads[3 * q].wait()
+        gate_ref = gates_ref.at[q - 1] if q else own_gate_ref
+        up_ref = ups_ref.at[q - 1] if q else own_up_ref
+        ready("gate", q)
         gate_pre = jnp.dot(
-            arrived_ref[...], thin_ref[q, 0, :main, :], preferred_element_type=jnp.float32
-        ) + jnp.dot(ends, thin_ref[q, 0, main:, :], preferred_element_type=jnp.float32)
-        loads[3 * q + 1].wait()
+            arrived_ref[...], gate_ref[:main, :], preferred_element_type=jnp.float32
+        ) + jnp.dot(ends, gate_ref[main:, :], preferred_element_type=jnp.float32)
+        ready("up", q)
         up_pre = jnp.dot(
-            arrived_ref[...], thin_ref[q, 1, :main, :], preferred_element_type=jnp.float32
-        ) + jnp.dot(ends, thin_ref[q, 1, main:, :], preferred_element_type=jnp.float32)
+            arrived_ref[...], up_ref[:main, :], preferred_element_type=jnp.float32
+        ) + jnp.dot(ends, up_ref[main:, :], preferred_element_type=jnp.float32)
         gate_pre = jnp.minimum(gate_pre, limit)
         actives.append(
             (
@@ -330,8 +393,7 @@
             ).astype(jnp.bfloat16)
         )
     for q in range(count):
-        loads[3 * q + 2].wait()
-    loads[-1].wait()
+        ready("down", q)
 
     def result_of(piece):
         total = jnp.zeros((rows, tail), jnp.float32)
@@ -514,60 +576,75 @@
     main = model_width * capacity // GROUP
     vmem = pl.BlockSpec(memory_space=pltpu.VMEM)
     hbm = pl.BlockSpec(memory_space=pltpu.HBM)
+    half_wide = out_weight.shape[0] // 2
+    (weight_near,) = staged((out_weight,), half_wide)
     hidden, outgoing = pl.pallas_call(
         mix_body,
         out_shape=(
             jax.ShapeDtypeStruct((rows_dev, model_width), jnp.bfloat16),
             pltpu.HBM((experts_all * GROUP, main), jnp.bfloat16),
         ),
-        in_specs=[vmem, hbm, vmem, vmem, vmem],
+        in_specs=[vmem, vmem, hbm, vmem, vmem, vmem],
         scratch_shapes=[
-            pltpu.VMEM(out_weight.shape, jnp.bfloat16),
-            pltpu.SemaphoreType.DMA((8,)),
+            pltpu.VMEM((half_wide, model_width), jnp.bfloat16),
+            pltpu.SemaphoreType.DMA((4,)),
         ],
         compiler_params=pltpu.CompilerParams(vmem_limit_bytes=16 << 20),
         name="mix",
     )(
         gathered,
+        weight_near,
         in_hbm(out_weight),
         in_hbm(residual),
         in_hbm(ffn_gain),
         in_hbm(routes.T),
     )
-    arrived = lax.all_to_all(
-        outgoing.reshape(experts_all, GROUP, main), SP, 0, 0, tiled=True
-    )
-
-    own = (gate_weight[0], up_weight[0], down_weight[0])
-    left, right = [], []
-    for w in own:
-        left.append(shifted(w, "tp", 1))
-        right.append(shifted(w, "tp", -1))
-    cut = own[2].shape[0] // 2
-    far_gate = shifted(left[0], "tp", 1)
-    far_up = shifted(right[1], "tp", -1)
-    far_down_l = shifted(left[2][:cut], "tp", 1)
-    far_down_r = shifted(right[2][cut:], "tp", -1)
-
-    weights = []
-    for gate_w, up_w, down_w in (own, left, right):
-        weights += [gate_w, up_w, down_w]
-    weights += [far_gate, far_up, far_down_l, far_down_r]
+    arrived = lax.all_to_all(outgoing.reshape(experts_all, GROUP, main), SP, 0, 0, tiled=True)
+
+    gate_own, up_own, down_own = gate_weight[0], up_weight[0], down_weight[0]
+    own_near = staged((gate_own, up_own), model_width)
+    long = model_width * 11 // 16
+    names = ("gate", "up", "more", "down")
+    left, right = {}, {}
+    for name, w in zip(names, (gate_own, up_own[:long], up_own[long:], down_own)):
+        left[name] = shifted(w, "tp", 1)
+        right[name] = shifted(w, "tp", -1)
+    cut = down_own.shape[0] // 2
+    far_gate = shifted(left["gate"], "tp", 1)
+    far_up = shifted(right["up"], "tp", -1)
+    far_more = shifted(right["more"], "tp", -1)
+    far_down_l = shifted(left["down"][:cut], "tp", 1)
+    far_down_r = shifted(right["down"][cut:], "tp", -1)
+    weights = (
+        down_own,
+        left["gate"],
+        left["down"],
+        right["gate"],
+        right["down"],
+        far_gate,
+        far_down_l,
+        far_down_r,
+        left["up"],
+        left["more"],
+        right["up"],
+        right["more"],
+        far_up,
+        far_more,
+    )
     result_rows = pl.pallas_call(
         expert_body,
         out_shape=pltpu.HBM((experts_all * GROUP, main), jnp.bfloat16),
-        in_specs=[vmem] + [hbm] * len(weights),
+        in_specs=[vmem] * 3 + [hbm] * len(weights),
         scratch_shapes=[
-            pltpu.VMEM((group, 2) + own[0].shape, jnp.bfloat16),
-            pltpu.VMEM((group,) + own[2].shape, jnp.bfloat16),
+            pltpu.VMEM((group - 1,) + gate_own.shape, jnp.bfloat16),
+            pltpu.VMEM((group - 1,) + gate_own.shape, jnp.bfloat16),
+            pltpu.VMEM((group,) + down_own.shape, jnp.bfloat16),
             pltpu.SemaphoreType.DMA((len(weights),)),
         ],
         compiler_params=pltpu.CompilerParams(vmem_limit_bytes=40 << 20),
         name="expert",
-    )(arrived.reshape(experts_all * GROUP, main), *map(in_hbm, weights))
-    returned = lax.all_to_all(
-        result_rows.reshape(experts_all, GROUP, main), SP, 0, 0, tiled=True
-    )
+    )(arrived.reshape(experts_all * GROUP, main), *own_near, *map(in_hbm, weights))
+    returned = lax.all_to_all(result_rows.reshape(experts_all, GROUP, main), SP, 0, 0, tiled=True)
     return pl.pallas_call(
         combine_body,
         out_shape=jax.ShapeDtypeStruct((rows_dev, model_width), jnp.bfloat16),

time: 298 us -> 307 us (1.030)
  starting transfers between devices: 32.7 us -> 45.5 us
  blocking collectives: 88.7 us -> 76.9 us
  Pallas kernels: 29 us -> 32.5 us
    all_to_all x1 -> x0, blocking collectives: 11.9 us -> none  [on_device(): gathered = lax.all_to_all(parts, 'tp', 0, 0, tiled=True)]
    ppermute x12 -> x15, starting transfers between devices: 14.9 us -> 22 us  [shifted(): lax.ppermute(array, axis, [(i, (i + step) % count) for i in range(count)])]
    all_to_all x0 -> x1, waiting for transfers between devices: none -> 5.41 us  [on_device(): gathered = lax.all_to_all(parts, 'tp', 0, 0, tiled=True)]
    all_to_all x0 -> x1, starting transfers between devices: none -> 4.88 us  [on_device(): gathered = lax.all_to_all(parts, 'tp', 0, 0, tiled=True)]
    pallas_call x0 -> x2, Pallas kernels: none -> 3.12 us  [staged(): pl.pallas_call(stage_body, out_shape=tuple((pltpu.VMEM((rows,) + a.shape[...]
    ppermute x12 -> x15, waiting for transfers between devices: 91.7 us -> 89.4 us  [shifted(): lax.ppermute(array, axis, [(i, (i + step) % count) for i in range(count)])]
  transfers between devices with their start and end apart: 14 -> 18, of which waited for: 7 -> 9; matrix products, arithmetic and copies ran while one was open for 1% -> 1% of each run, Pallas kernels for 0% -> 1%
where the time goes in v6:
time: 307 us; the launch traced here: 303 us
  waiting for transfers between devices  143 us (47%)
  blocking collectives  76.9 us (25%)
  starting transfers between devices  45.5 us (15%)
  Pallas kernels  32.5 us (11%)
    ppermute x15, waiting for transfers between devices, shifted(): lax.ppermute(array, axis, [(i, (i + step) % count) for i in range(count)])  89.4 us
    all_to_all x1, waiting for transfers between devices, on_device(): lax.all_to_all(result_rows.reshape(experts_all, GROUP, main), SP, 0, 0, t...  48.4 us
    all_gather x1, blocking collectives, on_device(): near = lax.all_gather(sent, 'sp_0', axis=0, tiled=True)  43 us
    all_to_all x1, blocking collectives, on_device(): shares = lax.all_to_all(shares, 'tp', 0, 0, tiled=True)  33.9 us
    ppermute x15, starting transfers between devices, shifted(): lax.ppermute(array, axis, [(i, (i + step) % count) for i in range(count)])  22 us
    all_to_all x1, starting transfers between devices, on_device(): lax.all_to_all(result_rows.reshape(experts_all, GROUP, main), SP, 0, 0, t...  13.7 us
    pallas_call x1, Pallas kernels, on_device(): pl.pallas_call(expert_body, out_shape=pltpu.HBM((experts_all * GROUP, mai...  10.8 us
    pallas_call x1, Pallas kernels, on_device(): pl.pallas_call(attend_body, out_shape=pltpu.HBM((group, rows_dev, group *...  9.4 us
  transfers between devices with their start and end apart: 18, of which 9 were waited for; matrix products, arithmetic and copies ran while one was open for 1% of the time, Pallas kernels for 1%

profile of v6, /device:TPU:34, one launch (start us, length us, event | category | flops | bytes accessed | tf_op | source)
XLA Modules:
  0.0 303.1 jit_solution(17343381711982908059)
XLA Ops:
  0.9 2.0 prepare.1
  2.9 33.9 %all_to_all.20.shares_ref = bf16[4,376,512]{2,1,0:T(8,128)(2,1)S(1)} all-to-all(bf16[4,376,512]{2,1,0:T(8,128)(2,1)S(1)} %get-tuple-element.12), channel_id=1, replica_groups=mesh['grp'=2,'sp_0'=16,'sp_1'=2,'tp'=4] {'tp'}, dimensions={0} | all-to-all | bytes 3080192 | tf_op jit(solution)/shard_map/all_to_all | solution.py:542
  36.9 43.0 %all_gather.3.near_ref = bf16[640,640]{1,0:T(8,128)(2,1)S(1)} all-gather(bf16[40,640]{1,0:T(8,128)(2,1)S(1)} %get-tuple-element.11), channel_id=1, replica_groups=mesh['grp'=2,'sp_0'=16,'sp_1'=2,'tp'=4] {'sp_0'}, dimensions={0}, use_global_device_ids=true | all-gather | bytes 870400 | tf_op jit(solution)/shard_map/all_gather | solution.py:544
  82.2 9.4 %attend.1 = bf16[4,40,1152]{2,1,0:T(8,128)(2,1)} custom-call(s32[1]{0:T(128)} %bitcast.core_ref, bf16[640,640]{1,0:T(8,128)(2,1)S(1)} %all_gather.3.near_ref, bf16[640,640]{1,0:T(8,128)(2,1)S(1)} %collective-permute-done.other_ref, bf16[4,376,512]{2,1,0:T(8,128)(2,1)S(1)} %all_to_all.20.shares_ref, ...), custom_call_target="tpu_custom_call" | custom-call | tf_op jit(solution)/shard_map/attend/pallas_call | solution.py:547
  91.6 4.9 %all-to-all-start.1 = ((bf16[4,40,1152]{2,1,0:T(8,128)(2,1)}), bf16[4,40,1152]{2,1,0:T(8,128)(2,1)S(1)}, u32[]{:S(2)}, u32[]{:S(2)}) async-start(bf16[4,40,1152]{2,1,0:T(8,128)(2,1)} %attend.1), calls=%async_computation.1 | async-start | bytes 737280 | tf_op jit(solution)/shard_map/all_to_all | solution.py:570
  98.0 5.4 %all-to-all-done.1.parts_ref = bf16[4,40,1152]{2,1,0:T(8,128)(2,1)S(1)} async-done(((bf16[4,40,1152]{2,1,0:T(8,128)(2,1)}), bf16[4,40,1152]{2,1,0:T(8,128)(2,1)S(1)}, u32[]{:S(2)}, u32[]{:S(2)}) %all-to-all-start.1) | async-done | bytes 368672 | tf_op jit(solution)/shard_map/all_to_all | solution.py:570
  103.4 5.1 %mix.1 = (bf16[40,2048]{1,0:T(8,128)(2,1)S(1)}, bf16[256,1792]{1,0:T(8,128)(2,1)}) custom-call(bf16[4,40,1152]{2,1,0:T(8,128)(2,1)S(1)} %all-to-all-done.1.parts_ref, bf16[512,2048]{1,0:T(8,128)(2,1)S(1)} %shard_map.163.near_ref, bf16[1024,2048]{1,0:T(8,128)(2,1)} %weight_hbm.1, bf16[40,2048]{1,0:T(8,128)(2,1)} %residual_ref.1, bf16[2048]{0:T(1024)(128)(2,1)} %gain_ref.3, ...), custom_call_target="tpu_custom_call" | custom-call | tf_op jit(solution)/shard_map/mix/pallas_call | solution.py:581
  108.6 5.0 %all-to-all-start.2 = ((bf16[32,8,1792]{2,1,0:T(8,128)(2,1)}), bf16[32,8,1792]{2,1,0:T(8,128)(2,1)S(1)}, u32[]{:S(2)}, u32[]{:S(2)}) async-start(bf16[32,8,1792]{2,1,0:T(8,128)(2,1)} %bitcast.25), calls=%async_computation.2 | async-start | bytes 1835008 | tf_op jit(solution)/shard_map/all_to_all | solution.py:602
  116.2 3.2 %collective-permute-start.11 = (bf16[1408,256]{1,0:T(8,128)(2,1)S(1)}, bf16[1408,256]{1,0:T(8,128)(2,1)S(1)}, u32[]{:S(2)}, u32[]{:S(2)}) collective-permute-start(bf16[1408,256]{1,0:T(8,128)(2,1)S(1)} %slice_bitcast_fusion), channel_id=1, source_target_pairs={{0,3},{1,0},{2,1},{3,2},{4,7},{5,4},{6,5},{7,6},{8,11},{9,8},{10,9... | collective-permute-start | bytes 2162696 | tf_op jit(solution)/shard_map/ppermute | solution.py:61
  120.9 5.8 %collective-permute-done.12.refs_13_ = bf16[640,256]{1,0:T(8,128)(2,1)S(1)} collective-permute-done((bf16[640,256]{1,0:T(8,128)(2,1)S(1)}, bf16[640,256]{1,0:T(8,128)(2,1)S(1)}, u32[]{:S(2)}, u32[]{:S(2)}) %collective-permute-start.12) | collective-permute-done | bytes 327712 | tf_op jit(solution)/shard_map/ppermute | solution.py:61
  126.7 2.0 collective-permute-start.10
  128.7 39.4 %collective-permute-done.10.refs_11_ = bf16[640,256]{1,0:T(8,128)(2,1)S(1)} collective-permute-done((bf16[640,256]{1,0:T(8,128)(2,1)S(1)}, bf16[640,256]{1,0:T(8,128)(2,1)S(1)}, u32[]{:S(2)}, u32[]{:S(2)}) %collective-permute-start.10) | collective-permute-done | bytes 327712 | tf_op jit(solution)/shard_map/ppermute | solution.py:61
  168.4 2.5 collective-permute-start.4
  171.0 3.3 %collective-permute-start.14 = (bf16[640,256]{1,0:T(8,128)(2,1)S(1)}, bf16[640,256]{1,0:T(8,128)(2,1)S(1)}, u32[]{:S(2)}, u32[]{:S(2)}) collective-permute-start(bf16[640,256]{1,0:T(8,128)(2,1)S(1)} %collective-permute-done.12.refs_13_), channel_id=1, source_target_pairs={{0,3},{1,0},{2,1},{3,2},{4,7},{5,4},{6,5},{7,6},{8,11},{9,8},{10,9... | collective-permute-start | bytes 983048 | tf_op jit(solution)/shard_map/ppermute | solution.py:61
  174.3 3.2 %collective-permute-start.13 = (bf16[1408,256]{1,0:T(8,128)(2,1)S(1)}, bf16[1408,256]{1,0:T(8,128)(2,1)S(1)}, u32[]{:S(2)}, u32[]{:S(2)}) collective-permute-start(bf16[1408,256]{1,0:T(8,128)(2,1)S(1)} %collective-permute-done.11.refs_12_), channel_id=1, source_target_pairs={{0,3},{1,0},{2,1},{3,2},{4,7},{5,4},{6,5},{7,6},{8,11},{9,8},{10,9... | collective-permute-start | bytes 2162696 | tf_op jit(solution)/shard_map/ppermute | solution.py:61
  177.6 24.0 %collective-permute-done.14.refs_15_ = bf16[640,256]{1,0:T(8,128)(2,1)S(1)} collective-permute-done((bf16[640,256]{1,0:T(8,128)(2,1)S(1)}, bf16[640,256]{1,0:T(8,128)(2,1)S(1)}, u32[]{:S(2)}, u32[]{:S(2)}) %collective-permute-start.14) | collective-permute-done | bytes 327712 | tf_op jit(solution)/shard_map/ppermute | solution.py:61
  201.6 3.0 collective-permute-start.7
  207.0 10.0 %collective-permute-done.13.refs_14_ = bf16[1408,256]{1,0:T(8,128)(2,1)S(1)} collective-permute-done((bf16[1408,256]{1,0:T(8,128)(2,1)S(1)}, bf16[1408,256]{1,0:T(8,128)(2,1)S(1)}, u32[]{:S(2)}, u32[]{:S(2)}) %collective-permute-start.13) | collective-permute-done | bytes 720928 | tf_op jit(solution)/shard_map/ppermute | solution.py:61
  217.0 2.4 collective-permute-done.7.refs_8_
  219.4 6.5 %collective-permute-done.8.refs_9_ = bf16[128,2048]{1,0:T(8,128)(2,1)S(1)} collective-permute-done((bf16[128,2048]{1,0:T(8,128)(2,1)S(1)}, bf16[128,2048]{1,0:T(8,128)(2,1)S(1)}, u32[]{:S(2)}, u32[]{:S(2)}) %collective-permute-start.8) | collective-permute-done | bytes 524320 | tf_op jit(solution)/shard_map/ppermute | solution.py:61
  226.8 10.8 %expert.1 = bf16[256,1792]{1,0:T(8,128)(2,1)} custom-call(bf16[256,1792]{1,0:T(8,128)(2,1)S(1)} %bitcast.15, bf16[2048,256]{1,0:T(8,128)(2,1)S(1)} %get-tuple-element.14.refs_0_, bf16[2048,256]{1,0:T(8,128)(2,1)S(1)} %get-tuple-element.15.refs_1_, bf16[256,2048]{1,0:T(8,128)(2,1)} %bitcast.20, bf16[2048,256]{1,0:T(8,128)(2,1)} %copy-done.4, ...), custom_call_target="tpu_custom_call" | custom-call | tf_op jit(solution)/shard_map/expert/pallas_call | solution.py:634
  237.7 13.7 %all-to-all-start.3 = ((bf16[32,8,1792]{2,1,0:T(8,128)(2,1)}), bf16[32,8,1792]{2,1,0:T(8,128)(2,1)S(1)}, u32[]{:S(2)}, u32[]{:S(2)}) async-start(bf16[32,8,1792]{2,1,0:T(8,128)(2,1)} %bitcast.18), calls=%async_computation.3 | async-start | bytes 1835008 | tf_op jit(solution)/shard_map/all_to_all | solution.py:647
  252.7 48.4 %all-to-all-done.3 = bf16[32,8,1792]{2,1,0:T(8,128)(2,1)S(1)} async-done(((bf16[32,8,1792]{2,1,0:T(8,128)(2,1)}), bf16[32,8,1792]{2,1,0:T(8,128)(2,1)S(1)}, u32[]{:S(2)}, u32[]{:S(2)}) %all-to-all-start.3) | async-done | bytes 917536 | tf_op jit(solution)/shard_map/all_to_all | solution.py:647
  301.1 2.0 combine.1
  (70 shorter events, 13.9 us)
Async XLA Ops:
  36.9 45.3 %collective-permute-start.1 = (bf16[4,376,512]{2,1,0:T(8,128)(2,1)S(1)}, bf16[4,376,512]{2,1,0:T(8,128)(2,1)S(1)}, u32[]{:S(2)}, u32[]{:S(2)}) collective-permute-start(bf16[4,376,512]{2,1,0:T(8,128)(2,1)S(1)} %all_to_all.20.shares_ref), channel_id=1, source_target_pairs={{0,4},{4,0},{1,5},{5,1},{2,6},{6,2},{3,7},{7,3},{8,12},{12,8},{9,1... | collective-permute-start | bytes 4620296 | tf_op jit(solution)/shard_map/ppermute | solution.py:61
  79.8 2.3 collective-permute-start
  91.6 11.9 %all-to-all-start.1 = ((bf16[4,40,1152]{2,1,0:T(8,128)(2,1)}), bf16[4,40,1152]{2,1,0:T(8,128)(2,1)S(1)}, u32[]{:S(2)}, u32[]{:S(2)}) async-start(bf16[4,40,1152]{2,1,0:T(8,128)(2,1)} %attend.1), calls=%async_computation.1 | async-start | bytes 737280 | tf_op jit(solution)/shard_map/all_to_all | solution.py:570
  108.6 118.2 %all-to-all-start.2 = ((bf16[32,8,1792]{2,1,0:T(8,128)(2,1)}), bf16[32,8,1792]{2,1,0:T(8,128)(2,1)S(1)}, u32[]{:S(2)}, u32[]{:S(2)}) async-start(bf16[32,8,1792]{2,1,0:T(8,128)(2,1)} %bitcast.25), calls=%async_computation.2 | async-start | bytes 1835008 | tf_op jit(solution)/shard_map/all_to_all | solution.py:602
  113.6 54.9 %copy-start.6 = (bf16[1,2048,256]{2,1,0:T(8,128)(2,1)S(1)}, bf16[1,2048,256]{2,1,0:T(8,128)(2,1)}, u32[]{:S(2)}) copy-start(bf16[1,2048,256]{2,1,0:T(8,128)(2,1)} %param.27) | copy-start | bytes 3145732
  113.6 57.3 %collective-permute-start.2 = (bf16[2048,256]{1,0:T(8,128)(2,1)}, bf16[2048,256]{1,0:T(8,128)(2,1)S(1)}, u32[]{:S(2)}, u32[]{:S(2)}) collective-permute-start(bf16[2048,256]{1,0:T(8,128)(2,1)} %bitcast.22), channel_id=1, source_target_pairs={{0,1},{1,2},{2,3},{3,0},{4,5},{5,6},{6,7},{7,4},{8,9},{9,10},{10,1... | collective-permute-start | bytes 3145736 | tf_op jit(solution)/shard_map/ppermute | solution.py:61
  113.9 57.0 %collective-permute-start.3 = (bf16[256,2048]{1,0:T(8,128)(2,1)}, bf16[256,2048]{1,0:T(8,128)(2,1)S(1)}, u32[]{:S(2)}, u32[]{:S(2)}) collective-permute-start(bf16[256,2048]{1,0:T(8,128)(2,1)} %bitcast.19), channel_id=1, source_target_pairs={{0,1},{1,2},{2,3},{3,0},{4,5},{5,6},{6,7},{7,4},{8,9},{9,10},{10,1... | collective-permute-start | bytes 3145736 | tf_op jit(solution)/shard_map/ppermute | solution.py:61
  115.9 10.8 %collective-permute-start.12 = (bf16[640,256]{1,0:T(8,128)(2,1)S(1)}, bf16[640,256]{1,0:T(8,128)(2,1)S(1)}, u32[]{:S(2)}, u32[]{:S(2)}) collective-permute-start(bf16[640,256]{1,0:T(8,128)(2,1)S(1)} %slice_bitcast_fusion.1), channel_id=1, source_target_pairs={{0,3},{1,0},{2,1},{3,2},{4,7},{5,4},{6,5},{7,6},{8,11},{9,8},{10,9... | collective-permute-start | bytes 983048 | tf_op jit(solution)/shard_map/ppermute | solution.py:61
  116.2 52.2 %collective-permute-start.11 = (bf16[1408,256]{1,0:T(8,128)(2,1)S(1)}, bf16[1408,256]{1,0:T(8,128)(2,1)S(1)}, u32[]{:S(2)}, u32[]{:S(2)}) collective-permute-start(bf16[1408,256]{1,0:T(8,128)(2,1)S(1)} %slice_bitcast_fusion), channel_id=1, source_target_pairs={{0,3},{1,0},{2,1},{3,2},{4,7},{5,4},{6,5},{7,6},{8,11},{9,8},{10,9... | collective-permute-start | bytes 2162696 | tf_op jit(solution)/shard_map/ppermute | solution.py:61
  119.4 54.8 %collective-permute-start.5 = (bf16[256,2048]{1,0:T(8,128)(2,1)S(1)}, bf16[256,2048]{1,0:T(8,128)(2,1)S(1)}, u32[]{:S(2)}, u32[]{:S(2)}) collective-permute-start(bf16[256,2048]{1,0:T(8,128)(2,1)S(1)} %bitcast.21), channel_id=1, source_target_pairs={{0,3},{1,0},{2,1},{3,2},{4,7},{5,4},{6,5},{7,6},{8,11},{9,8},{10,9... | collective-permute-start | bytes 3145736 | tf_op jit(solution)/shard_map/ppermute | solution.py:61
  126.7 100.1 %copy-start.12 = (bf16[640,256]{1,0:T(8,128)(2,1)}, bf16[640,256]{1,0:T(8,128)(2,1)S(1)}, u32[]{:S(2)}) copy-start(bf16[640,256]{1,0:T(8,128)(2,1)S(1)} %collective-permute-done.12.refs_13_) | copy-start | bytes 983044
  126.7 41.5 %collective-permute-start.10 = (bf16[640,256]{1,0:T(8,128)(2,1)S(1)}, bf16[640,256]{1,0:T(8,128)(2,1)S(1)}, u32[]{:S(2)}, u32[]{:S(2)}) collective-permute-start(bf16[640,256]{1,0:T(8,128)(2,1)S(1)} %slice_bitcast_fusion.1), channel_id=1, source_target_pairs={{0,1},{1,2},{2,3},{3,0},{4,5},{5,6},{6,7},{7,4},{8,9},{9,10},{10,1... | collective-permute-start | bytes 983048 | tf_op jit(solution)/shard_map/ppermute | solution.py:61
  168.1 36.5 %collective-permute-start.9 = (bf16[1408,256]{1,0:T(8,128)(2,1)S(1)}, bf16[1408,256]{1,0:T(8,128)(2,1)S(1)}, u32[]{:S(2)}, u32[]{:S(2)}) collective-permute-start(bf16[1408,256]{1,0:T(8,128)(2,1)S(1)} %slice_bitcast_fusion), channel_id=1, source_target_pairs={{0,1},{1,2},{2,3},{3,0},{4,5},{5,6},{6,7},{7,4},{8,9},{9,10},{10,1... | collective-permute-start | bytes 2162696 | tf_op jit(solution)/shard_map/ppermute | solution.py:61
  168.4 57.5 %copy-start.7 = (bf16[1408,256]{1,0:T(8,128)(2,1)}, bf16[1408,256]{1,0:T(8,128)(2,1)S(1)}, u32[]{:S(2)}) copy-start(bf16[1408,256]{1,0:T(8,128)(2,1)S(1)} %collective-permute-done.11.refs_12_) | copy-start | bytes 2162692
  168.4 38.6 %collective-permute-start.4 = (bf16[2048,256]{1,0:T(8,128)(2,1)S(1)}, bf16[2048,256]{1,0:T(8,128)(2,1)S(1)}, u32[]{:S(2)}, u32[]{:S(2)}) collective-permute-start(bf16[2048,256]{1,0:T(8,128)(2,1)S(1)} %bitcast.24), channel_id=1, source_target_pairs={{0,3},{1,0},{2,1},{3,2},{4,7},{5,4},{6,5},{7,6},{8,11},{9,8},{10,9... | collective-permute-start | bytes 3145736 | tf_op jit(solution)/shard_map/ppermute | solution.py:61
  170.9 55.0 %copy-start.4 = (bf16[2048,256]{1,0:T(8,128)(2,1)}, bf16[2048,256]{1,0:T(8,128)(2,1)S(1)}, u32[]{:S(2)}) copy-start(bf16[2048,256]{1,0:T(8,128)(2,1)S(1)} %collective-permute-done.2.refs_3_) | copy-start | bytes 3145732
  170.9 55.8 %collective-permute-start.6 = (bf16[2048,256]{1,0:T(8,128)(2,1)S(1)}, bf16[2048,256]{1,0:T(8,128)(2,1)}, u32[]{:S(2)}, u32[]{:S(2)}) collective-permute-start(bf16[2048,256]{1,0:T(8,128)(2,1)S(1)} %collective-permute-done.2.refs_3_), channel_id=1, source_target_pairs={{0,1},{1,2},{2,3},{3,0},{4,5},{5,6},{6,7},{7,4},{8,9},{9,10},{10,1... | collective-permute-start | bytes 3145736 | tf_op jit(solution)/shard_map/ppermute | solution.py:61
  170.9 34.1 %copy-start.1 = (bf16[256,2048]{1,0:T(8,128)(2,1)}, bf16[256,2048]{1,0:T(8,128)(2,1)S(1)}, u32[]{:S(2)}) copy-start(bf16[256,2048]{1,0:T(8,128)(2,1)S(1)} %collective-permute-done.3.refs_4_) | copy-start | bytes 3145732
  171.0 30.6 %collective-permute-start.14 = (bf16[640,256]{1,0:T(8,128)(2,1)S(1)}, bf16[640,256]{1,0:T(8,128)(2,1)S(1)}, u32[]{:S(2)}, u32[]{:S(2)}) collective-permute-start(bf16[640,256]{1,0:T(8,128)(2,1)S(1)} %collective-permute-done.12.refs_13_), channel_id=1, source_target_pairs={{0,3},{1,0},{2,1},{3,2},{4,7},{5,4},{6,5},{7,6},{8,11},{9,8},{10,9... | collective-permute-start | bytes 983048 | tf_op jit(solution)/shard_map/ppermute | solution.py:61
  174.3 30.8 %copy-start.2 = (bf16[256,2048]{1,0:T(8,128)(2,1)}, bf16[256,2048]{1,0:T(8,128)(2,1)S(1)}, u32[]{:S(2)}) copy-start(bf16[256,2048]{1,0:T(8,128)(2,1)S(1)} %collective-permute-done.5.refs_6_) | copy-start | bytes 3145732
  174.3 42.8 %collective-permute-start.13 = (bf16[1408,256]{1,0:T(8,128)(2,1)S(1)}, bf16[1408,256]{1,0:T(8,128)(2,1)S(1)}, u32[]{:S(2)}, u32[]{:S(2)}) collective-permute-start(bf16[1408,256]{1,0:T(8,128)(2,1)S(1)} %collective-permute-done.11.refs_12_), channel_id=1, source_target_pairs={{0,3},{1,0},{2,1},{3,2},{4,7},{5,4},{6,5},{7,6},{8,11},{9,8},{10,9... | collective-permute-start | bytes 2162696 | tf_op jit(solution)/shard_map/ppermute | solution.py:61
  201.6 17.8 %collective-permute-start.7 = (bf16[128,2048]{1,0:T(8,128)(2,1)S(1)}, bf16[128,2048]{1,0:T(8,128)(2,1)S(1)}, u32[]{:S(2)}, u32[]{:S(2)}) collective-permute-start(bf16[128,2048]{1,0:T(8,128)(2,1)S(1)} %slice.24), channel_id=1, source_target_pairs={{0,1},{1,2},{2,3},{3,0},{4,5},{5,6},{6,7},{7,4},{8,9},{9,10},{10,1... | collective-permute-start | bytes 1572872 | tf_op jit(solution)/shard_map/ppermute | solution.py:61
  204.6 21.4 %collective-permute-start.8 = (bf16[128,2048]{1,0:T(8,128)(2,1)S(1)}, bf16[128,2048]{1,0:T(8,128)(2,1)S(1)}, u32[]{:S(2)}, u32[]{:S(2)}) collective-permute-start(bf16[128,2048]{1,0:T(8,128)(2,1)S(1)} %slice.25), channel_id=1, source_target_pairs={{0,3},{1,0},{2,1},{3,2},{4,7},{5,4},{6,5},{7,6},{8,11},{9,8},{10,9... | collective-permute-start | bytes 1572872 | tf_op jit(solution)/shard_map/ppermute | solution.py:61
  237.7 63.4 %all-to-all-start.3 = ((bf16[32,8,1792]{2,1,0:T(8,128)(2,1)}), bf16[32,8,1792]{2,1,0:T(8,128)(2,1)S(1)}, u32[]{:S(2)}, u32[]{:S(2)}) async-start(bf16[32,8,1792]{2,1,0:T(8,128)(2,1)} %bitcast.18), calls=%async_computation.3 | async-start | bytes 1835008 | tf_op jit(solution)/shard_map/all_to_all | solution.py:647
  (11 other events, 92.0 us)

commit v7 on v5

--- a/solution.py
+++ b/solution.py
@@ -282,25 +282,50 @@
         ).astype(jnp.bfloat16)
 
 
-def expert_body(arrived_ref, *refs):
-    count = (len(refs) - 5) // 3
-    weights_hbm = refs[: 3 * count + 1]
-    out_ref, thin_ref, down_ref, sems = refs[3 * count + 1 :]
-    gate_up = weights_hbm[0].shape
-    cut = weights_hbm[-1].shape[0]
-    loads = []
-    for i, source in enumerate(weights_hbm):
-        q, m = divmod(i, 3) if i < 3 * count else (count - 1, 3)
-        if m < 2:
-            dst = thin_ref.at[q, m]
-        elif q < count - 1:
-            dst = down_ref.at[q]
-        else:
-            dst = down_ref.at[q, pl.ds((m - 2) * cut, cut)]
-        loads.append(pltpu.make_async_copy(source, dst, sems.at[i]))
-        loads[-1].start()
+def expert_body(parity_ref, arrived_ref, *refs):
+    out_ref, gate_up_ref, down_ref, sems = refs[-4:]
+    sources = refs[:-4]
+    count = down_ref.shape[0]
+    far = count - 1
+    long = sources[4].shape[0]
+    short = sources[5].shape[0]
+    cut = sources[13].shape[0]
+    part = sources[15].shape[0]
+    parity = parity_ref[0]
+    targets = [
+        ("gate", 0, gate_up_ref.at[0, 0]),
+        ("up", 0, gate_up_ref.at[0, 1]),
+        ("down", 0, down_ref.at[0]),
+    ]
+    for q in range(1, far):
+        targets += [
+            ("gate", q, gate_up_ref.at[q, 0]),
+            ("up", q, gate_up_ref.at[q, 1, pl.ds(0, long)]),
+            ("up", q, gate_up_ref.at[q, 1, pl.ds(long, short)]),
+            ("down", q, down_ref.at[q]),
+        ]
+    targets += [
+        ("gate", far, gate_up_ref.at[far, 0, pl.ds(long, short)]),
+        ("up", far, gate_up_ref.at[far, 1, pl.ds(long, short)]),
+        ("down", far, down_ref.at[far, pl.ds(0, cut)]),
+        ("down", far, down_ref.at[far, pl.ds(cut, cut)]),
+        ("gate", far, gate_up_ref.at[far, parity, pl.ds(0, part)]),
+        ("gate", far, gate_up_ref.at[far, parity, pl.ds(part, part)]),
+        ("gate", far, gate_up_ref.at[far, 1 - parity, pl.ds(0, part)]),
+        ("gate", far, gate_up_ref.at[far, 1 - parity, pl.ds(part, part)]),
+    ]
+    loads = {}
+    for i, (source, (kind, q, target)) in enumerate(zip(sources, targets, strict=True)):
+        load = pltpu.make_async_copy(source, target, sems.at[i])
+        load.start()
+        loads.setdefault((kind, q), []).append(load)
+
+    def ready(kind, q):
+        for load in loads.pop((kind, q), ()):
+            load.wait()
+
     rows, main = arrived_ref.shape
-    model_width = gate_up[0]
+    model_width = gate_up_ref.shape[2]
     tail = model_width - main
     line = lax.broadcasted_iota(jnp.int32, (rows, rows), 0)
     column = lax.broadcasted_iota(jnp.int32, (rows, rows), 1)
@@ -315,14 +340,15 @@
     ends = ends.astype(jnp.bfloat16)
     actives = []
     for q in range(count):
-        loads[3 * q].wait()
+        gate_ref, up_ref = gate_up_ref.at[q, 0], gate_up_ref.at[q, 1]
+        ready("gate", q)
         gate_pre = jnp.dot(
-            arrived_ref[...], thin_ref[q, 0, :main, :], preferred_element_type=jnp.float32
-        ) + jnp.dot(ends, thin_ref[q, 0, main:, :], preferred_element_type=jnp.float32)
-        loads[3 * q + 1].wait()
+            arrived_ref[...], gate_ref[:main, :], preferred_element_type=jnp.float32
+        ) + jnp.dot(ends, gate_ref[main:, :], preferred_element_type=jnp.float32)
+        ready("up", q)
         up_pre = jnp.dot(
-            arrived_ref[...], thin_ref[q, 1, :main, :], preferred_element_type=jnp.float32
-        ) + jnp.dot(ends, thin_ref[q, 1, main:, :], preferred_element_type=jnp.float32)
+            arrived_ref[...], up_ref[:main, :], preferred_element_type=jnp.float32
+        ) + jnp.dot(ends, up_ref[main:, :], preferred_element_type=jnp.float32)
         gate_pre = jnp.minimum(gate_pre, limit)
         actives.append(
             (
@@ -330,8 +356,7 @@
             ).astype(jnp.bfloat16)
         )
     for q in range(count):
-        loads[3 * q + 2].wait()
-    loads[-1].wait()
+        ready("down", q)
 
     def result_of(piece):
         total = jnp.zeros((rows, tail), jnp.float32)
@@ -538,33 +563,48 @@
         outgoing.reshape(experts_all, GROUP, main), SP, 0, 0, tiled=True
     )
 
-    own = (gate_weight[0], up_weight[0], down_weight[0])
-    left, right = [], []
-    for w in own:
-        left.append(shifted(w, "tp", 1))
-        right.append(shifted(w, "tp", -1))
-    cut = own[2].shape[0] // 2
-    far_gate = shifted(left[0], "tp", 1)
-    far_up = shifted(right[1], "tp", -1)
-    far_down_l = shifted(left[2][:cut], "tp", 1)
-    far_down_r = shifted(right[2][cut:], "tp", -1)
-
-    weights = []
-    for gate_w, up_w, down_w in (own, left, right):
-        weights += [gate_w, up_w, down_w]
-    weights += [far_gate, far_up, far_down_l, far_down_r]
+    gate_own, up_own, down_own = gate_weight[0], up_weight[0], down_weight[0]
+    long = model_width * 11 // 16
+    names = ("gate", "up", "more", "down")
+    left, right = {}, {}
+    for name, w in zip(names, (gate_own, up_own[:long], up_own[long:], down_own)):
+        left[name] = shifted(w, "tp", 1)
+        right[name] = shifted(w, "tp", -1)
+    cut = down_own.shape[0] // 2
+    part = long // 2
+    parity = lax.axis_index("grp") % 2
+    even = parity == 0
+    relay_l = jnp.where(even, left["gate"][:part], left["up"][:part])
+    relay_r = jnp.where(even, right["gate"][part:long], right["up"][part:])
+    far_l = shifted(relay_l, "tp", 1)
+    far_r = shifted(relay_r, "tp", -1)
+    pairs = [(i, i ^ 1) for i in range(lax.axis_size("grp"))]
+    pair_l = lax.ppermute(far_l, "grp", pairs)
+    pair_r = lax.ppermute(far_r, "grp", pairs)
+    far_gate = shifted(left["gate"][long:], "tp", 1)
+    far_more = shifted(right["more"], "tp", -1)
+    far_down_l = shifted(left["down"][:cut], "tp", 1)
+    far_down_r = shifted(right["down"][cut:], "tp", -1)
+    weights = [gate_own, up_own, down_own]
+    for side in (left, right):
+        weights += [side["gate"], side["up"], side["more"], side["down"]]
+    weights += [far_gate, far_more, far_down_l, far_down_r, far_l, far_r, pair_l, pair_r]
     result_rows = pl.pallas_call(
         expert_body,
         out_shape=pltpu.HBM((experts_all * GROUP, main), jnp.bfloat16),
-        in_specs=[vmem] + [hbm] * len(weights),
+        in_specs=[pl.BlockSpec(memory_space=pltpu.SMEM), vmem] + [hbm] * len(weights),
         scratch_shapes=[
-            pltpu.VMEM((group, 2) + own[0].shape, jnp.bfloat16),
-            pltpu.VMEM((group,) + own[2].shape, jnp.bfloat16),
+            pltpu.VMEM((group, 2) + gate_own.shape, jnp.bfloat16),
+            pltpu.VMEM((group,) + down_own.shape, jnp.bfloat16),
             pltpu.SemaphoreType.DMA((len(weights),)),
         ],
         compiler_params=pltpu.CompilerParams(vmem_limit_bytes=40 << 20),
         name="expert",
-    )(arrived.reshape(experts_all * GROUP, main), *map(in_hbm, weights))
+    )(
+        parity.reshape(1),
+        arrived.reshape(experts_all * GROUP, main),
+        *map(in_hbm, weights),
+    )
     returned = lax.all_to_all(
         result_rows.reshape(experts_all, GROUP, main), SP, 0, 0, tiled=True
     )

time: 298 us -> 292 us (0.980)
  waiting for transfers between devices: 140 us -> 119 us
  starting transfers between devices: 32.7 us -> 43.8 us
    ppermute x12 -> x16, waiting for transfers between devices: 91.7 us -> 70.2 us  [shifted(): lax.ppermute(array, axis, [(i, (i + step) % count) for i in range(count)])]
    ppermute x12 -> x16, starting transfers between devices: 14.9 us -> 20.9 us  [shifted(): lax.ppermute(array, axis, [(i, (i + step) % count) for i in range(count)])]
    ppermute x0 -> x2, starting transfers between devices: none -> 4.23 us  [the longest x1 2.12 us: on_device(): pair_l = lax.ppermute(far_l, 'grp', pairs)]
    slice x2 -> x5, local copies, waits for them, and re-layouts: 0.08 us -> 3.1 us  [the longest x1 1.08 us: on_device(): far_down_r = shifted(right['down'][cut:], 'tp', -1)]
  transfers between devices with their start and end apart: 14 -> 20, of which waited for: 7 -> 9; matrix products, arithmetic and copies ran while one was open for 1% -> 3% of each run, Pallas kernels for 0% -> 0%
where the time goes in v7:
time: 292 us; the launch traced here: 290 us
  waiting for transfers between devices  119 us (41%)
  blocking collectives  88.7 us (30%)
  starting transfers between devices  43.8 us (15%)
  Pallas kernels  29.1 us (10%)
  local copies, waits for them, and re-layouts  5.38 us (2%)
  other arithmetic  4.12 us (1%)
    ppermute x16, waiting for transfers between devices, shifted(): lax.ppermute(array, axis, [(i, (i + step) % count) for i in range(count)])  70.2 us
    all_to_all x1, waiting for transfers between devices, on_device(): lax.all_to_all(result_rows.reshape(experts_all, GROUP, main), SP, 0, 0, t...  48.4 us
    all_gather x1, blocking collectives, on_device(): near = lax.all_gather(sent, 'sp_0', axis=0, tiled=True)  43 us
    all_to_all x1, blocking collectives, on_device(): shares = lax.all_to_all(shares, 'tp', 0, 0, tiled=True)  33.9 us
    ppermute x16, starting transfers between devices, shifted(): lax.ppermute(array, axis, [(i, (i + step) % count) for i in range(count)])  20.9 us
    all_to_all x1, starting transfers between devices, on_device(): lax.all_to_all(result_rows.reshape(experts_all, GROUP, main), SP, 0, 0, t...  13.7 us
    all_to_all x1, blocking collectives, on_device(): gathered = lax.all_to_all(parts, 'tp', 0, 0, tiled=True)  11.9 us
    pallas_call x1, Pallas kernels, on_device(): pl.pallas_call(expert_body, out_shape=pltpu.HBM((experts_all * GROUP, mai...  9.91 us
  transfers between devices with their start and end apart: 20, of which 9 were waited for; matrix products, arithmetic and copies ran while one was open for 3% of the time, Pallas kernels for 0%

profile of v7, /device:TPU:34, one launch (start us, length us, event | category | flops | bytes accessed | tf_op | source)
XLA Modules:
  0.0 289.9 jit_solution(14197643902049958505)
XLA Ops:
  0.9 2.0 prepare.1
  2.9 33.9 %all_to_all.20.shares_ref = bf16[4,376,512]{2,1,0:T(8,128)(2,1)S(1)} all-to-all(bf16[4,376,512]{2,1,0:T(8,128)(2,1)S(1)} %get-tuple-element.10), channel_id=1, replica_groups=mesh['grp'=2,'sp_0'=16,'sp_1'=2,'tp'=4] {'tp'}, dimensions={0} | all-to-all | bytes 3080192 | tf_op jit(solution)/shard_map/all_to_all | solution.py:505
  36.9 43.0 %all_gather.3.near_ref = bf16[640,640]{1,0:T(8,128)(2,1)S(1)} all-gather(bf16[40,640]{1,0:T(8,128)(2,1)S(1)} %get-tuple-element.9), channel_id=1, replica_groups=mesh['grp'=2,'sp_0'=16,'sp_1'=2,'tp'=4] {'sp_0'}, dimensions={0}, use_global_device_ids=true | all-gather | bytes 870400 | tf_op jit(solution)/shard_map/all_gather | solution.py:507
  82.2 9.4 %attend.1 = bf16[4,40,1152]{2,1,0:T(8,128)(2,1)} custom-call(s32[1]{0:T(128)} %bitcast.1.core_ref, bf16[640,640]{1,0:T(8,128)(2,1)S(1)} %all_gather.3.near_ref, bf16[640,640]{1,0:T(8,128)(2,1)S(1)} %collective-permute-done.other_ref, bf16[4,376,512]{2,1,0:T(8,128)(2,1)S(1)} %all_to_all.20.shares_ref, ...), custom_call_target="tpu_custom_call" | custom-call | tf_op jit(solution)/shard_map/attend/pallas_call | solution.py:510
  91.6 11.9 %all_to_all.21.parts_ref = bf16[4,40,1152]{2,1,0:T(8,128)(2,1)S(1)} all-to-all(bf16[4,40,1152]{2,1,0:T(8,128)(2,1)} %attend.1), channel_id=1, replica_groups=mesh['grp'=2,'sp_0'=16,'sp_1'=2,'tp'=4] {'tp'}, dimensions={0} | all-to-all | bytes 737280 | tf_op jit(solution)/shard_map/all_to_all | solution.py:533
  103.4 5.7 %mix.1 = (bf16[40,2048]{1,0:T(8,128)(2,1)S(1)}, bf16[256,1792]{1,0:T(8,128)(2,1)}) custom-call(bf16[4,40,1152]{2,1,0:T(8,128)(2,1)S(1)} %all_to_all.21.parts_ref, bf16[1024,2048]{1,0:T(8,128)(2,1)} %weight_hbm.1, bf16[40,2048]{1,0:T(8,128)(2,1)} %residual_ref.1, bf16[2048]{0:T(1024)(128)(2,1)} %gain_ref.3, s32[4,40]{1,0:T(4,128)} %bitcast.28), custom_call_target="tpu_custom_call" | custom-call | tf_op jit(solution)/shard_map/mix/pallas_call | solution.py:542
  109.1 5.0 %all-to-all-start.2 = ((bf16[32,8,1792]{2,1,0:T(8,128)(2,1)}), bf16[32,8,1792]{2,1,0:T(8,128)(2,1)S(1)}, u32[]{:S(2)}, u32[]{:S(2)}) async-start(bf16[32,8,1792]{2,1,0:T(8,128)(2,1)} %bitcast.26), calls=%async_computation.2 | async-start | bytes 1835008 | tf_op jit(solution)/shard_map/all_to_all | solution.py:562
  117.3 1.8 collective-permute-start.5
  120.3 14.1 %collective-permute-done.3.refs_4_ = bf16[1408,256]{1,0:T(8,128)(2,1)} collective-permute-done((bf16[1408,256]{1,0:T(8,128)(2,1)}, bf16[1408,256]{1,0:T(8,128)(2,1)}, u32[]{:S(2)}, u32[]{:S(2)}) %collective-permute-start.3) | collective-permute-done | bytes 720928 | tf_op jit(solution)/shard_map/ppermute | solution.py:61
  134.4 2.7 collective-permute-start.9
  137.0 19.7 %collective-permute-done.2.refs_3_ = bf16[2048,256]{1,0:T(8,128)(2,1)S(1)} collective-permute-done((bf16[2048,256]{1,0:T(8,128)(2,1)}, bf16[2048,256]{1,0:T(8,128)(2,1)S(1)}, u32[]{:S(2)}, u32[]{:S(2)}) %collective-permute-start.2) | collective-permute-done | bytes 1048608 | tf_op jit(solution)/shard_map/ppermute | solution.py:61
  156.7 2.7 collective-permute-start.8
  160.9 1.8 collective-permute-start.14
  163.8 22.7 %collective-permute-done.8.refs_9_ = bf16[640,256]{1,0:T(8,128)(2,1)S(1)} collective-permute-done((bf16[640,256]{1,0:T(8,128)(2,1)S(1)}, bf16[640,256]{1,0:T(8,128)(2,1)S(1)}, u32[]{:S(2)}, u32[]{:S(2)}) %collective-permute-start.8) | collective-permute-done | bytes 327712 | tf_op jit(solution)/shard_map/ppermute | solution.py:61
  187.0 3.7 %collective-permute-start.11 = (bf16[640,256]{1,0:T(8,128)(2,1)S(1)}, bf16[640,256]{1,0:T(8,128)(2,1)S(1)}, u32[]{:S(2)}, u32[]{:S(2)}) collective-permute-start(bf16[640,256]{1,0:T(8,128)(2,1)S(1)} %collective-permute-done.8.refs_9_), channel_id=1, source_target_pairs={{0,3},{1,0},{2,1},{3,2},{4,7},{5,4},{6,5},{7,6},{8,11},{9,8},{10,9... | collective-permute-start | bytes 983048 | tf_op jit(solution)/shard_map/ppermute | solution.py:61
  193.0 2.1 collective-permute-start.13
  195.1 2.1 collective-permute-start.16
  197.8 2.1 collective-permute-start.17
  200.0 4.9 %collective-permute-done.11.refs_12_ = bf16[640,256]{1,0:T(8,128)(2,1)S(1)} collective-permute-done((bf16[640,256]{1,0:T(8,128)(2,1)S(1)}, bf16[640,256]{1,0:T(8,128)(2,1)S(1)}, u32[]{:S(2)}, u32[]{:S(2)}) %collective-permute-start.11) | collective-permute-done | bytes 327712 | tf_op jit(solution)/shard_map/ppermute | solution.py:61
  206.6 5.4 %collective-permute-done.10.refs_11_ = bf16[640,256]{1,0:T(8,128)(2,1)S(1)} collective-permute-done((bf16[640,256]{1,0:T(8,128)(2,1)S(1)}, bf16[640,256]{1,0:T(8,128)(2,1)S(1)}, u32[]{:S(2)}, u32[]{:S(2)}) %collective-permute-start.10) | collective-permute-done | bytes 327712 | tf_op jit(solution)/shard_map/ppermute | solution.py:61
  214.5 9.9 %expert.1 = bf16[256,1792]{1,0:T(8,128)(2,1)} custom-call(s32[1]{0:T(128)} %bitcast.parity_ref, bf16[256,1792]{1,0:T(8,128)(2,1)S(1)} %bitcast.16, bf16[2048,256]{1,0:T(8,128)(2,1)} %bitcast.22, bf16[2048,256]{1,0:T(8,128)(2,1)} %bitcast.18, bf16[256,2048]{1,0:T(8,128)(2,1)} %bitcast.25, bf16[2048,256]{1,0:T(8,128)(2,1)} %copy-done.1, ...), custom_call_target="tpu_custom_call" | custom-call | tf_op jit(solution)/shard_map/expert/pallas_call | solution.py:592
  224.4 13.7 %all-to-all-start.3 = ((bf16[32,8,1792]{2,1,0:T(8,128)(2,1)}), bf16[32,8,1792]{2,1,0:T(8,128)(2,1)S(1)}, u32[]{:S(2)}, u32[]{:S(2)}) async-start(bf16[32,8,1792]{2,1,0:T(8,128)(2,1)} %bitcast.19), calls=%async_computation.3 | async-start | bytes 1835008 | tf_op jit(solution)/shard_map/all_to_all | solution.py:608
  239.5 48.4 %all-to-all-done.3 = bf16[32,8,1792]{2,1,0:T(8,128)(2,1)S(1)} async-done(((bf16[32,8,1792]{2,1,0:T(8,128)(2,1)}), bf16[32,8,1792]{2,1,0:T(8,128)(2,1)S(1)}, u32[]{:S(2)}, u32[]{:S(2)}) %all-to-all-start.3) | async-done | bytes 917536 | tf_op jit(solution)/shard_map/all_to_all | solution.py:608
  287.9 2.0 combine.1
  (66 shorter events, 19.2 us)
Async XLA Ops:
  36.9 45.3 %collective-permute-start.1 = (bf16[4,376,512]{2,1,0:T(8,128)(2,1)S(1)}, bf16[4,376,512]{2,1,0:T(8,128)(2,1)S(1)}, u32[]{:S(2)}, u32[]{:S(2)}) collective-permute-start(bf16[4,376,512]{2,1,0:T(8,128)(2,1)S(1)} %all_to_all.20.shares_ref), channel_id=1, source_target_pairs={{0,4},{4,0},{1,5},{5,1},{2,6},{6,2},{3,7},{7,3},{8,12},{12,8},{9,1... | collective-permute-start | bytes 4620296 | tf_op jit(solution)/shard_map/ppermute | solution.py:61
  79.8 2.3 collective-permute-start
  109.1 105.3 %all-to-all-start.2 = ((bf16[32,8,1792]{2,1,0:T(8,128)(2,1)}), bf16[32,8,1792]{2,1,0:T(8,128)(2,1)S(1)}, u32[]{:S(2)}, u32[]{:S(2)}) async-start(bf16[32,8,1792]{2,1,0:T(8,128)(2,1)} %bitcast.26), calls=%async_computation.2 | async-start | bytes 1835008 | tf_op jit(solution)/shard_map/all_to_all | solution.py:562
  115.0 19.3 %collective-permute-start.3 = (bf16[1408,256]{1,0:T(8,128)(2,1)}, bf16[1408,256]{1,0:T(8,128)(2,1)}, u32[]{:S(2)}, u32[]{:S(2)}) collective-permute-start(bf16[1408,256]{1,0:T(8,128)(2,1)} %slice_bitcast_fusion), channel_id=1, source_target_pairs={{0,1},{1,2},{2,3},{3,0},{4,5},{5,6},{6,7},{7,4},{8,9},{9,10},{10,1... | collective-permute-start | bytes 2162696 | tf_op jit(solution)/shard_map/ppermute | solution.py:61
  115.3 41.4 %collective-permute-start.2 = (bf16[2048,256]{1,0:T(8,128)(2,1)}, bf16[2048,256]{1,0:T(8,128)(2,1)S(1)}, u32[]{:S(2)}, u32[]{:S(2)}) collective-permute-start(bf16[2048,256]{1,0:T(8,128)(2,1)} %bitcast.20), channel_id=1, source_target_pairs={{0,1},{1,2},{2,3},{3,0},{4,5},{5,6},{6,7},{7,4},{8,9},{9,10},{10,1... | collective-permute-start | bytes 3145736 | tf_op jit(solution)/shard_map/ppermute | solution.py:61
  117.0 43.9 %collective-permute-start.6 = (bf16[2048,256]{1,0:T(8,128)(2,1)}, bf16[2048,256]{1,0:T(8,128)(2,1)}, u32[]{:S(2)}, u32[]{:S(2)}) collective-permute-start(bf16[2048,256]{1,0:T(8,128)(2,1)} %bitcast.21), channel_id=1, source_target_pairs={{0,3},{1,0},{2,1},{3,2},{4,7},{5,4},{6,5},{7,6},{8,11},{9,8},{10,9... | collective-permute-start | bytes 3145736 | tf_op jit(solution)/shard_map/ppermute | solution.py:61
  117.3 69.6 %collective-permute-start.5 = (bf16[256,2048]{1,0:T(8,128)(2,1)}, bf16[256,2048]{1,0:T(8,128)(2,1)}, u32[]{:S(2)}, u32[]{:S(2)}) collective-permute-start(bf16[256,2048]{1,0:T(8,128)(2,1)} %bitcast.23), channel_id=1, source_target_pairs={{0,1},{1,2},{2,3},{3,0},{4,5},{5,6},{6,7},{7,4},{8,9},{9,10},{10,1... | collective-permute-start | bytes 3145736 | tf_op jit(solution)/shard_map/ppermute | solution.py:61
  119.1 41.3 %collective-permute-start.7 = (bf16[1408,256]{1,0:T(8,128)(2,1)}, bf16[1408,256]{1,0:T(8,128)(2,1)}, u32[]{:S(2)}, u32[]{:S(2)}) collective-permute-start(bf16[1408,256]{1,0:T(8,128)(2,1)} %slice_bitcast_fusion), channel_id=1, source_target_pairs={{0,3},{1,0},{2,1},{3,2},{4,7},{5,4},{6,5},{7,6},{8,11},{9,8},{10,9... | collective-permute-start | bytes 2162696 | tf_op jit(solution)/shard_map/ppermute | solution.py:61
  134.4 57.4 %collective-permute-start.9 = (bf16[256,2048]{1,0:T(8,128)(2,1)}, bf16[256,2048]{1,0:T(8,128)(2,1)}, u32[]{:S(2)}, u32[]{:S(2)}) collective-permute-start(bf16[256,2048]{1,0:T(8,128)(2,1)} %bitcast.24), channel_id=1, source_target_pairs={{0,3},{1,0},{2,1},{3,2},{4,7},{5,4},{6,5},{7,6},{8,11},{9,8},{10,9... | collective-permute-start | bytes 3145736 | tf_op jit(solution)/shard_map/ppermute | solution.py:61
  156.7 43.2 %copy-start.1 = (bf16[2048,256]{1,0:T(8,128)(2,1)}, bf16[2048,256]{1,0:T(8,128)(2,1)S(1)}, u32[]{:S(2)}) copy-start(bf16[2048,256]{1,0:T(8,128)(2,1)S(1)} %collective-permute-done.2.refs_3_) | copy-start | bytes 3145732
  156.7 29.8 %collective-permute-start.8 = (bf16[640,256]{1,0:T(8,128)(2,1)S(1)}, bf16[640,256]{1,0:T(8,128)(2,1)S(1)}, u32[]{:S(2)}, u32[]{:S(2)}) collective-permute-start(bf16[640,256]{1,0:T(8,128)(2,1)S(1)} %slice_bitcast_fusion.1), channel_id=1, source_target_pairs={{0,3},{1,0},{2,1},{3,2},{4,7},{5,4},{6,5},{7,6},{8,11},{9,8},{10,9... | collective-permute-start | bytes 983048 | tf_op jit(solution)/shard_map/ppermute | solution.py:61
  160.4 32.5 %collective-permute-start.4 = (bf16[640,256]{1,0:T(8,128)(2,1)S(1)}, bf16[640,256]{1,0:T(8,128)(2,1)}, u32[]{:S(2)}, u32[]{:S(2)}) collective-permute-start(bf16[640,256]{1,0:T(8,128)(2,1)S(1)} %slice_bitcast_fusion.1), channel_id=1, source_target_pairs={{0,1},{1,2},{2,3},{3,0},{4,5},{5,6},{6,7},{7,4},{8,9},{9,10},{10,1... | collective-permute-start | bytes 983048 | tf_op jit(solution)/shard_map/ppermute | solution.py:61
  160.9 34.2 %collective-permute-start.14 = (bf16[704,256]{1,0:T(8,128)(2,1)S(1)}, bf16[704,256]{1,0:T(8,128)(2,1)S(1)}, u32[]{:S(2)}, u32[]{:S(2)}) collective-permute-start(bf16[704,256]{1,0:T(8,128)(2,1)S(1)} %slice_select_fusion.1), channel_id=1, source_target_pairs={{0,1},{1,2},{2,3},{3,0},{4,5},{5,6},{6,7},{7,4},{8,9},{9,10},{10,1... | collective-permute-start | bytes 1081352 | tf_op jit(solution)/shard_map/ppermute | solution.py:61
  186.5 27.0 %copy-start.7 = (bf16[640,256]{1,0:T(8,128)(2,1)}, bf16[640,256]{1,0:T(8,128)(2,1)S(1)}, u32[]{:S(2)}) copy-start(bf16[640,256]{1,0:T(8,128)(2,1)S(1)} %collective-permute-done.8.refs_9_) | copy-start | bytes 983044
  186.5 11.3 %collective-permute-start.15 = (bf16[704,256]{1,0:T(8,128)(2,1)S(1)}, bf16[704,256]{1,0:T(8,128)(2,1)S(1)}, u32[]{:S(2)}, u32[]{:S(2)}) collective-permute-start(bf16[704,256]{1,0:T(8,128)(2,1)S(1)} %slice_select_fusion), channel_id=1, source_target_pairs={{0,3},{1,0},{2,1},{3,2},{4,7},{5,4},{6,5},{7,6},{8,11},{9,8},{10,9... | collective-permute-start | bytes 1081352 | tf_op jit(solution)/shard_map/ppermute | solution.py:61
  187.0 17.9 %collective-permute-start.11 = (bf16[640,256]{1,0:T(8,128)(2,1)S(1)}, bf16[640,256]{1,0:T(8,128)(2,1)S(1)}, u32[]{:S(2)}, u32[]{:S(2)}) collective-permute-start(bf16[640,256]{1,0:T(8,128)(2,1)S(1)} %collective-permute-done.8.refs_9_), channel_id=1, source_target_pairs={{0,3},{1,0},{2,1},{3,2},{4,7},{5,4},{6,5},{7,6},{8,11},{9,8},{10,9... | collective-permute-start | bytes 983048 | tf_op jit(solution)/shard_map/ppermute | solution.py:61
  191.7 20.2 %collective-permute-start.12 = (bf16[128,2048]{1,0:T(8,128)(2,1)S(1)}, bf16[128,2048]{1,0:T(8,128)(2,1)S(1)}, u32[]{:S(2)}, u32[]{:S(2)}) collective-permute-start(bf16[128,2048]{1,0:T(8,128)(2,1)S(1)} %slice.45), channel_id=1, source_target_pairs={{0,1},{1,2},{2,3},{3,0},{4,5},{5,6},{6,7},{7,4},{8,9},{9,10},{10,1... | collective-permute-start | bytes 1572872 | tf_op jit(solution)/shard_map/ppermute | solution.py:61
  193.0 20.6 %collective-permute-start.13 = (bf16[128,2048]{1,0:T(8,128)(2,1)S(1)}, bf16[128,2048]{1,0:T(8,128)(2,1)S(1)}, u32[]{:S(2)}, u32[]{:S(2)}) collective-permute-start(bf16[128,2048]{1,0:T(8,128)(2,1)S(1)} %slice.46), channel_id=1, source_target_pairs={{0,3},{1,0},{2,1},{3,2},{4,7},{5,4},{6,5},{7,6},{8,11},{9,8},{10,9... | collective-permute-start | bytes 1572872 | tf_op jit(solution)/shard_map/ppermute | solution.py:61
  195.1 19.3 %copy-start.4 = (bf16[704,256]{1,0:T(8,128)(2,1)}, bf16[704,256]{1,0:T(8,128)(2,1)S(1)}, u32[]{:S(2)}) copy-start(bf16[704,256]{1,0:T(8,128)(2,1)S(1)} %collective-permute-done.14.refs_15_) | copy-start | bytes 1081348
  195.1 18.5 %collective-permute-start.16 = (bf16[704,256]{1,0:T(8,128)(2,1)S(1)}, bf16[704,256]{1,0:T(8,128)(2,1)S(1)}, u32[]{:S(2)}, u32[]{:S(2)}) collective-permute-start(bf16[704,256]{1,0:T(8,128)(2,1)S(1)} %collective-permute-done.14.refs_15_), channel_id=1, source_target_pairs={{0,128},{128,0},{1,129},{129,1},{2,130},{130,2},{3,131},{131,3},{4... | collective-permute-start | bytes 1081352 | tf_op jit(solution)/shard_map/ppermute | solution.py:582
  197.8 15.8 %copy-start.5 = (bf16[704,256]{1,0:T(8,128)(2,1)}, bf16[704,256]{1,0:T(8,128)(2,1)S(1)}, u32[]{:S(2)}) copy-start(bf16[704,256]{1,0:T(8,128)(2,1)S(1)} %collective-permute-done.15.refs_16_) | copy-start | bytes 1081348
  197.8 16.6 %collective-permute-start.17 = (bf16[704,256]{1,0:T(8,128)(2,1)S(1)}, bf16[704,256]{1,0:T(8,128)(2,1)}, u32[]{:S(2)}, u32[]{:S(2)}) collective-permute-start(bf16[704,256]{1,0:T(8,128)(2,1)S(1)} %collective-permute-done.15.refs_16_), channel_id=1, source_target_pairs={{0,128},{128,0},{1,129},{129,1},{2,130},{130,2},{3,131},{131,3},{4... | collective-permute-start | bytes 1081352 | tf_op jit(solution)/shard_map/ppermute | solution.py:583
  204.9 7.1 %collective-permute-start.10 = (bf16[640,256]{1,0:T(8,128)(2,1)S(1)}, bf16[640,256]{1,0:T(8,128)(2,1)S(1)}, u32[]{:S(2)}, u32[]{:S(2)}) collective-permute-start(bf16[640,256]{1,0:T(8,128)(2,1)S(1)} %slice.44), channel_id=1, source_target_pairs={{0,1},{1,2},{2,3},{3,0},{4,5},{5,6},{6,7},{7,4},{8,9},{9,10},{10,1... | collective-permute-start | bytes 983048 | tf_op jit(solution)/shard_map/ppermute | solution.py:61
  224.4 63.4 %all-to-all-start.3 = ((bf16[32,8,1792]{2,1,0:T(8,128)(2,1)}), bf16[32,8,1792]{2,1,0:T(8,128)(2,1)S(1)}, u32[]{:S(2)}, u32[]{:S(2)}) async-start(bf16[32,8,1792]{2,1,0:T(8,128)(2,1)} %bitcast.19), calls=%async_computation.3 | async-start | bytes 1835008 | tf_op jit(solution)/shard_map/all_to_all | solution.py:608
  (8 other events, 48.6 us)

commit v8 on v6

--- a/solution.py
+++ b/solution.py
@@ -21,6 +21,7 @@
 limit = 7.0
 slope = 1.702
 STAT_LANES = 128
+LOG2_E = 1.4426950408889634
 
 
 def turn_tables(place, heads):
@@ -54,6 +55,10 @@
 
 def in_hbm(array):
     return pltpu.with_memory_space_constraint(array, pltpu.HBM)
+
+
+def in_vmem(array):
+    return pltpu.with_memory_space_constraint(array, pltpu.VMEM)
 
 
 def shifted(array, axis, step):
@@ -210,21 +215,25 @@
         turned = (raw.astype(jnp.float32) * cos_ref[...] + swapped * sin_ref[...]).astype(
             jnp.bfloat16
         )
+        all_weights, peaks, totals = [], [], []
         for h in range(heads):
-            lo = h * PLAIN_HEAD_WIDTH
             query_rot = turned[:, lanes_of(h, QK_ROPE)]
             query = jnp.concatenate(
-                (plain[:, lo : lo + PLAIN_HEAD_WIDTH], query_rot, jnp.zeros_like(query_rot)), axis=1
+                (plain[:, lanes_of(h, PLAIN_HEAD_WIDTH)], query_rot, jnp.zeros_like(query_rot)),
+                axis=1,
             )
             scores = lax.dot_general(query, keys_ref[h], last, preferred_element_type=jnp.float32)
             peak = jnp.max(scores, axis=1, keepdims=True)
-            weights = jnp.exp((scores - peak) * scale)
-            total = jnp.sum(weights, axis=1, keepdims=True)
-            summed = jnp.dot(
-                weights.astype(jnp.bfloat16),
-                values_ref[:, lanes_of(h, VALUE_WIDTH)],
-                preferred_element_type=jnp.float32,
-            )
+            weights = jnp.exp2((scores - peak) * (scale * LOG2_E))
+            peaks.append(peak)
+            totals.append(jnp.sum(weights, axis=1, keepdims=True))
+            all_weights.append(weights.astype(jnp.bfloat16))
+        crossed = jnp.dot(
+            jnp.concatenate(all_weights, axis=0), values_ref[...], preferred_element_type=jnp.float32
+        )
+        for h in range(heads):
+            peak, total = peaks[h], totals[h]
+            summed = crossed[h * tokens : (h + 1) * tokens, lanes_of(h, VALUE_WIDTH)]
             result = (summed / total).astype(jnp.bfloat16)
             head = j * heads + h
             for i in range(shards):
@@ -327,42 +336,60 @@
         ).astype(jnp.bfloat16)
 
 
-def expert_body(arrived_ref, *refs):
-    out_ref, gates_ref, ups_ref, down_ref, sems = refs[-5:]
-    own_gate_ref, own_up_ref, *sources = refs[:-5]
+def begin_loads(sources, targets, sems):
+    loads = {}
+    for i, (source, (name, target)) in enumerate(zip(sources, targets, strict=True)):
+        load = pltpu.make_async_copy(source, target, sems.at[i])
+        load.start()
+        loads.setdefault(name, []).append(load)
+
+    def ready(name):
+        for load in loads.pop(name):
+            load.wait()
+
+    return ready
+
+
+def activation(gate_pre, up_pre):
+    gate_pre = jnp.minimum(gate_pre, limit)
+    return (
+        (jnp.clip(up_pre, -limit, limit) + 1.0) * gate_pre * jax.nn.sigmoid(slope * gate_pre)
+    ).astype(jnp.bfloat16)
+
+
+def active_units(rows_ref, ends, gate_ref, up_ref, ready, q):
+    main = rows_ref.shape[1]
+    ready(("gate", q))
+    gate_pre = jnp.dot(
+        rows_ref[...], gate_ref[:main, :], preferred_element_type=jnp.float32
+    ) + jnp.dot(ends, gate_ref[main:, :], preferred_element_type=jnp.float32)
+    ready(("up", q))
+    up_pre = jnp.dot(
+        rows_ref[...], up_ref[:main, :], preferred_element_type=jnp.float32
+    ) + jnp.dot(ends, up_ref[main:, :], preferred_element_type=jnp.float32)
+    return activation(gate_pre, up_pre)
+
+
+def near_body(arrived_ref, *refs):
+    total_ref, ends_ref, gate_up_ref, down_ref, sems = refs[-5:]
+    sources = refs[:-5]
     count = down_ref.shape[0]
-    wanted = []
-    for q in range(count):
-        wanted.append((gates_ref.at[q - 1], ups_ref.at[q - 1], down_ref.at[q]))
-    cut = sources[7].shape[0]
-    long = sources[8].shape[0]
-    short = sources[9].shape[0]
+    long, short = sources[4].shape[0], sources[5].shape[0]
     targets = [
-        ("down", 0, wanted[0][2]),
-        ("gate", 1, wanted[1][0]),
-        ("down", 1, wanted[1][2]),
-        ("gate", 2, wanted[2][0]),
-        ("down", 2, wanted[2][2]),
-        ("gate", 3, wanted[3][0]),
-        ("down", 3, down_ref.at[3, pl.ds(0, cut)]),
-        ("down", 3, down_ref.at[3, pl.ds(cut, cut)]),
+        (("gate", 0), gate_up_ref.at[0, 0]),
+        (("up", 0), gate_up_ref.at[0, 1]),
+        (("down", 0), down_ref.at[0]),
     ]
     for q in range(1, count):
-        targets.append(("up", q, ups_ref.at[q - 1, pl.ds(0, long)]))
-        targets.append(("up", q, ups_ref.at[q - 1, pl.ds(long, short)]))
-    loads = {}
-    for i, (source, (kind, q, target)) in enumerate(zip(sources, targets, strict=True)):
-        load = pltpu.make_async_copy(source, target, sems.at[i])
-        load.start()
-        loads.setdefault((kind, q), []).append(load)
-
-    def ready(kind, q):
-        for load in loads.pop((kind, q), ()):
-            load.wait()
-
+        targets += [
+            (("gate", q), gate_up_ref.at[q, 0]),
+            (("up", q), gate_up_ref.at[q, 1, pl.ds(0, long)]),
+            (("up", q), gate_up_ref.at[q, 1, pl.ds(long, short)]),
+            (("down", q), down_ref.at[q]),
+        ]
+    ready = begin_loads(sources, targets, sems)
     rows, main = arrived_ref.shape
-    model_width = own_gate_ref.shape[0]
-    tail = model_width - main
+    tail = total_ref.shape[1] - main
     line = lax.broadcasted_iota(jnp.int32, (rows, rows), 0)
     column = lax.broadcasted_iota(jnp.int32, (rows, rows), 1)
     ends = jnp.zeros((rows, tail), jnp.float32)
@@ -374,35 +401,66 @@
             pick, arrived_ref[:, lanes_of(s, tail)], preferred_element_type=jnp.float32
         )
     ends = ends.astype(jnp.bfloat16)
-    actives = []
+    ends_ref[...] = ends
+    actives = [
+        active_units(arrived_ref, ends, gate_up_ref.at[q, 0], gate_up_ref.at[q, 1], ready, q)
+        for q in range(count)
+    ]
     for q in range(count):
-        gate_ref = gates_ref.at[q - 1] if q else own_gate_ref
-        up_ref = ups_ref.at[q - 1] if q else own_up_ref
-        ready("gate", q)
-        gate_pre = jnp.dot(
-            arrived_ref[...], gate_ref[:main, :], preferred_element_type=jnp.float32
-        ) + jnp.dot(ends, gate_ref[main:, :], preferred_element_type=jnp.float32)
-        ready("up", q)
-        up_pre = jnp.dot(
-            arrived_ref[...], up_ref[:main, :], preferred_element_type=jnp.float32
-        ) + jnp.dot(ends, up_ref[main:, :], preferred_element_type=jnp.float32)
-        gate_pre = jnp.minimum(gate_pre, limit)
-        actives.append(
-            (
-                (jnp.clip(up_pre, -limit, limit) + 1.0) * gate_pre * jax.nn.sigmoid(slope * gate_pre)
-            ).astype(jnp.bfloat16)
-        )
-    for q in range(count):
-        ready("down", q)
-
-    def result_of(piece):
+        ready(("down", q))
+    for piece in range(GROUP):
+        at = lanes_of(piece, tail)
         total = jnp.zeros((rows, tail), jnp.float32)
         for q in range(count):
-            product = jnp.dot(
-                actives[q], down_ref[q, :, lanes_of(piece, tail)], preferred_element_type=jnp.float32
-            )
+            product = jnp.dot(actives[q], down_ref[q, :, at], preferred_element_type=jnp.float32)
             total = total + product.astype(jnp.bfloat16).astype(jnp.float32)
-        return total
+        total_ref[:, at] = total
+
+
+def far_body(
+    arrived_ref,
+    ends_ref,
+    total_ref,
+    gate_ref,
+    up_ref,
+    down_l_ref,
+    more_hbm,
+    down_r_hbm,
+    out_ref,
+    more_ref,
+    down_r_ref,
+    sems,
+):
+    ready = begin_loads(
+        (more_hbm, down_r_hbm), (("more", more_ref), ("down", down_r_ref)), sems
+    )
+    rows, main = out_ref.shape
+    tail = ends_ref.shape[1]
+    line = lax.broadcasted_iota(jnp.int32, (rows, rows), 0)
+    column = lax.broadcasted_iota(jnp.int32, (rows, rows), 1)
+    long = up_ref.shape[0]
+    rest = main - long
+    ends = ends_ref[...]
+    gate_pre = jnp.dot(
+        arrived_ref[...], gate_ref[:main, :], preferred_element_type=jnp.float32
+    ) + jnp.dot(ends, gate_ref[main:, :], preferred_element_type=jnp.float32)
+    up_pre = jnp.dot(arrived_ref[:, :long], up_ref[...], preferred_element_type=jnp.float32)
+    ready("more")
+    up_pre = (
+        up_pre
+        + jnp.dot(arrived_ref[:, long:], more_ref[:rest, :], preferred_element_type=jnp.float32)
+        + jnp.dot(ends, more_ref[rest:, :], preferred_element_type=jnp.float32)
+    )
+    active = activation(gate_pre, up_pre)
+    ready("down")
+    cut = down_l_ref.shape[0]
+
+    def result_of(piece):
+        at = lanes_of(piece, tail)
+        product = jnp.dot(
+            active[:, :cut], down_l_ref[:, at], preferred_element_type=jnp.float32
+        ) + jnp.dot(active[:, cut:], down_r_ref[:, at], preferred_element_type=jnp.float32)
+        return total_ref[:, at] + product.astype(jnp.bfloat16).astype(jnp.float32)
 
     last = result_of(GROUP - 1).astype(jnp.bfloat16)
     group_end = lax.broadcasted_iota(jnp.int32, (rows, tail), 0) % GROUP == GROUP - 1
@@ -602,7 +660,6 @@
     arrived = lax.all_to_all(outgoing.reshape(experts_all, GROUP, main), SP, 0, 0, tiled=True)
 
     gate_own, up_own, down_own = gate_weight[0], up_weight[0], down_weight[0]
-    own_near = staged((gate_own, up_own), model_width)
     long = model_width * 11 // 16
     names = ("gate", "up", "more", "down")
     left, right = {}, {}
@@ -615,35 +672,44 @@
     far_more = shifted(right["more"], "tp", -1)
     far_down_l = shifted(left["down"][:cut], "tp", 1)
     far_down_r = shifted(right["down"][cut:], "tp", -1)
-    weights = (
-        down_own,
-        left["gate"],
-        left["down"],
-        right["gate"],
-        right["down"],
-        far_gate,
-        far_down_l,
-        far_down_r,
-        left["up"],
-        left["more"],
-        right["up"],
-        right["more"],
-        far_up,
-        far_more,
-    )
+    arrived_rows = arrived.reshape(experts_all * GROUP, main)
+    near_weights = [gate_own, up_own, down_own]
+    for side in (left, right):
+        near_weights += [side["gate"], side["up"], side["more"], side["down"]]
+    total, ends = pl.pallas_call(
+        near_body,
+        out_shape=(
+            pltpu.VMEM((experts_all * GROUP, model_width), jnp.float32),
+            pltpu.VMEM((experts_all * GROUP, model_width - main), jnp.bfloat16),
+        ),
+        in_specs=[vmem] + [hbm] * len(near_weights),
+        out_specs=(vmem, vmem),
+        scratch_shapes=[
+            pltpu.VMEM((group - 1, 2) + gate_own.shape, jnp.bfloat16),
+            pltpu.VMEM((group - 1,) + down_own.shape, jnp.bfloat16),
+            pltpu.SemaphoreType.DMA((len(near_weights),)),
+        ],
+        compiler_params=pltpu.CompilerParams(vmem_limit_bytes=32 << 20),
+        name="near_quarters",
+    )(arrived_rows, *map(in_hbm, near_weights))
     result_rows = pl.pallas_call(
-        expert_body,
+        far_body,
         out_shape=pltpu.HBM((experts_all * GROUP, main), jnp.bfloat16),
-        in_specs=[vmem] * 3 + [hbm] * len(weights),
+        in_specs=[vmem] * 6 + [hbm] * 2,
         scratch_shapes=[
-            pltpu.VMEM((group - 1,) + gate_own.shape, jnp.bfloat16),
-            pltpu.VMEM((group - 1,) + gate_own.shape, jnp.bfloat16),
-            pltpu.VMEM((group,) + down_own.shape, jnp.bfloat16),
-            pltpu.SemaphoreType.DMA((len(weights),)),
+            pltpu.VMEM(far_more.shape, jnp.bfloat16),
+            pltpu.VMEM(far_down_r.shape, jnp.bfloat16),
+            pltpu.SemaphoreType.DMA((2,)),
         ],
-        compiler_params=pltpu.CompilerParams(vmem_limit_bytes=40 << 20),
-        name="expert",
-    )(arrived.reshape(experts_all * GROUP, main), *own_near, *map(in_hbm, weights))
+        compiler_params=pltpu.CompilerParams(vmem_limit_bytes=24 << 20),
+        name="far_quarter",
+    )(
+        arrived_rows,
+        ends,
+        total,
+        *map(in_vmem, (far_gate, far_up, far_down_l)),
+        *map(in_hbm, (far_more, far_down_r)),
+    )
     returned = lax.all_to_all(result_rows.reshape(experts_all, GROUP, main), SP, 0, 0, tiled=True)
     return pl.pallas_call(
         combine_body,

time: 307 us -> 303 us (0.987)
  waiting for transfers between devices: 143 us -> 139 us
    ppermute x15, waiting for transfers between devices: 89.4 us -> 84.9 us  [shifted(): lax.ppermute(array, axis, [(i, (i + step) % count) for i in range(count)])]
    pallas_call x1 -> x2, Pallas kernels: 10.8 us -> 10.9 us  [the longest x1 6.68 us: on_device(): pl.pallas_call(near_body, out_shape=(pltpu.VMEM((experts_all * GROUP, mod...]
  transfers between devices with their start and end apart: 18 -> 18, of which waited for: 9 -> 6; matrix products, arithmetic and copies ran while one was open for 1% -> 1% of each run, Pallas kernels for 1% -> 3%
where the time goes in v8:
time: 303 us; the launch traced here: 299 us
  waiting for transfers between devices  139 us (46%)
  blocking collectives  76.9 us (25%)
  starting transfers between devices  47 us (16%)
  Pallas kernels  30.1 us (10%)
  local copies, waits for them, and re-layouts  4.18 us (1%)
    ppermute x15, waiting for transfers between devices, shifted(): lax.ppermute(array, axis, [(i, (i + step) % count) for i in range(count)])  84.9 us
    all_to_all x1, waiting for transfers between devices, on_device(): lax.all_to_all(result_rows.reshape(experts_all, GROUP, main), SP, 0, 0, t...  48.4 us
    all_gather x1, blocking collectives, on_device(): near = lax.all_gather(sent, 'sp_0', axis=0, tiled=True)  43 us
    all_to_all x1, blocking collectives, on_device(): shares = lax.all_to_all(shares, 'tp', 0, 0, tiled=True)  33.9 us
    ppermute x15, starting transfers between devices, shifted(): lax.ppermute(array, axis, [(i, (i + step) % count) for i in range(count)])  22.8 us
    all_to_all x1, starting transfers between devices, on_device(): lax.all_to_all(result_rows.reshape(experts_all, GROUP, main), SP, 0, 0, t...  14.3 us
    pallas_call x1, Pallas kernels, on_device(): pl.pallas_call(attend_body, out_shape=pltpu.HBM((group, rows_dev, group *...  8.52 us
    pallas_call x1, Pallas kernels, on_device(): pl.pallas_call(near_body, out_shape=(pltpu.VMEM((experts_all * GROUP, mod...  6.68 us
  transfers between devices with their start and end apart: 18, of which 6 were waited for; matrix products, arithmetic and copies ran while one was open for 1% of the time, Pallas kernels for 3%

profile of v8, /device:TPU:34, one launch (start us, length us, event | category | flops | bytes accessed | tf_op | source)
XLA Modules:
  0.0 299.1 jit_solution(2095798458604913908)
XLA Ops:
  0.9 2.0 prepare.1
  2.9 33.9 %all_to_all.20.shares_ref = bf16[4,376,512]{2,1,0:T(8,128)(2,1)S(1)} all-to-all(bf16[4,376,512]{2,1,0:T(8,128)(2,1)S(1)} %get-tuple-element.12), channel_id=1, replica_groups=mesh['grp'=2,'sp_0'=16,'sp_1'=2,'tp'=4] {'tp'}, dimensions={0} | all-to-all | bytes 3080192 | tf_op jit(solution)/shard_map/all_to_all | solution.py:600
  36.9 43.0 %all_gather.3.near_ref = bf16[640,640]{1,0:T(8,128)(2,1)S(1)} all-gather(bf16[40,640]{1,0:T(8,128)(2,1)S(1)} %get-tuple-element.11), channel_id=1, replica_groups=mesh['grp'=2,'sp_0'=16,'sp_1'=2,'tp'=4] {'sp_0'}, dimensions={0}, use_global_device_ids=true | all-gather | bytes 870400 | tf_op jit(solution)/shard_map/all_gather | solution.py:602
  82.2 8.5 %attend.1 = bf16[4,40,1152]{2,1,0:T(8,128)(2,1)} custom-call(s32[1]{0:T(128)} %bitcast.core_ref, bf16[640,640]{1,0:T(8,128)(2,1)S(1)} %all_gather.3.near_ref, bf16[640,640]{1,0:T(8,128)(2,1)S(1)} %collective-permute-done.other_ref, bf16[4,376,512]{2,1,0:T(8,128)(2,1)S(1)} %all_to_all.20.shares_ref, ...), custom_call_target="tpu_custom_call" | custom-call | tf_op jit(solution)/shard_map/attend/pallas_call | solution.py:605
  90.7 4.9 %all-to-all-start.1 = ((bf16[4,40,1152]{2,1,0:T(8,128)(2,1)}), bf16[4,40,1152]{2,1,0:T(8,128)(2,1)S(1)}, u32[]{:S(2)}, u32[]{:S(2)}) async-start(bf16[4,40,1152]{2,1,0:T(8,128)(2,1)} %attend.1), calls=%async_computation.1 | async-start | bytes 737280 | tf_op jit(solution)/shard_map/all_to_all | solution.py:628
  97.1 5.4 %all-to-all-done.1.parts_ref = bf16[4,40,1152]{2,1,0:T(8,128)(2,1)S(1)} async-done(((bf16[4,40,1152]{2,1,0:T(8,128)(2,1)}), bf16[4,40,1152]{2,1,0:T(8,128)(2,1)S(1)}, u32[]{:S(2)}, u32[]{:S(2)}) %all-to-all-start.1) | async-done | bytes 368672 | tf_op jit(solution)/shard_map/all_to_all | solution.py:628
  102.5 5.1 %mix.1 = (bf16[40,2048]{1,0:T(8,128)(2,1)S(1)}, bf16[256,1792]{1,0:T(8,128)(2,1)}) custom-call(bf16[4,40,1152]{2,1,0:T(8,128)(2,1)S(1)} %all-to-all-done.1.parts_ref, bf16[512,2048]{1,0:T(8,128)(2,1)S(1)} %shard_map.163.near_ref, bf16[1024,2048]{1,0:T(8,128)(2,1)} %weight_hbm.1, bf16[40,2048]{1,0:T(8,128)(2,1)} %residual_ref.1, bf16[2048]{0:T(1024)(128)(2,1)} %gain_ref.3, ...), custom_call_target="tpu_custom_call" | custom-call | tf_op jit(solution)/shard_map/mix/pallas_call | solution.py:639
  107.7 5.0 %all-to-all-start.2 = ((bf16[32,8,1792]{2,1,0:T(8,128)(2,1)}), bf16[32,8,1792]{2,1,0:T(8,128)(2,1)S(1)}, u32[]{:S(2)}, u32[]{:S(2)}) async-start(bf16[32,8,1792]{2,1,0:T(8,128)(2,1)} %bitcast.23), calls=%async_computation.2 | async-start | bytes 1835008 | tf_op jit(solution)/shard_map/all_to_all | solution.py:660
  113.1 2.1 collective-permute-start.7
  115.3 2.5 collective-permute-start.9
  117.9 3.3 %collective-permute-start.8 = (bf16[640,256]{1,0:T(8,128)(2,1)S(1)}, bf16[640,256]{1,0:T(8,128)(2,1)}, u32[]{:S(2)}, u32[]{:S(2)}) collective-permute-start(bf16[640,256]{1,0:T(8,128)(2,1)S(1)} %slice_bitcast_fusion.1), channel_id=1, source_target_pairs={{0,3},{1,0},{2,1},{3,2},{4,7},{5,4},{6,5},{7,6},{8,11},{9,8},{10,9... | collective-permute-start | bytes 983048 | tf_op jit(solution)/shard_map/ppermute | solution.py:66
  121.2 39.1 %collective-permute-done.8.refs_9_ = bf16[640,256]{1,0:T(8,128)(2,1)} collective-permute-done((bf16[640,256]{1,0:T(8,128)(2,1)S(1)}, bf16[640,256]{1,0:T(8,128)(2,1)}, u32[]{:S(2)}, u32[]{:S(2)}) %collective-permute-start.8) | collective-permute-done | bytes 327712 | tf_op jit(solution)/shard_map/ppermute | solution.py:66
  160.3 1.8 collective-permute-start.6
  162.4 2.9 collective-permute-start.10
  165.3 3.2 %collective-permute-start.4 = (bf16[640,256]{1,0:T(8,128)(2,1)S(1)}, bf16[640,256]{1,0:T(8,128)(2,1)S(1)}, u32[]{:S(2)}, u32[]{:S(2)}) collective-permute-start(bf16[640,256]{1,0:T(8,128)(2,1)S(1)} %slice_bitcast_fusion.1), channel_id=1, source_target_pairs={{0,1},{1,2},{2,3},{3,0},{4,5},{5,6},{6,7},{7,4},{8,9},{9,10},{10,1... | collective-permute-start | bytes 983048 | tf_op jit(solution)/shard_map/ppermute | solution.py:66
  170.3 39.5 %collective-permute-done.4.refs_5_ = bf16[640,256]{1,0:T(8,128)(2,1)S(1)} collective-permute-done((bf16[640,256]{1,0:T(8,128)(2,1)S(1)}, bf16[640,256]{1,0:T(8,128)(2,1)S(1)}, u32[]{:S(2)}, u32[]{:S(2)}) %collective-permute-start.4) | collective-permute-done | bytes 327712 | tf_op jit(solution)/shard_map/ppermute | solution.py:66
  209.8 3.1 %collective-permute-start.14 = (bf16[128,2048]{1,0:T(8,128)(2,1)}, bf16[128,2048]{1,0:T(8,128)(2,1)}, u32[]{:S(2)}, u32[]{:S(2)}) collective-permute-start(bf16[128,2048]{1,0:T(8,128)(2,1)} %slice.25), channel_id=1, source_target_pairs={{0,3},{1,0},{2,1},{3,2},{4,7},{5,4},{6,5},{7,6},{8,11},{9,8},{10,9... | collective-permute-start | bytes 1572872 | tf_op jit(solution)/shard_map/ppermute | solution.py:66
  213.8 3.1 %collective-permute-start.13 = (bf16[640,256]{1,0:T(8,128)(2,1)}, bf16[640,256]{1,0:T(8,128)(2,1)}, u32[]{:S(2)}, u32[]{:S(2)}) collective-permute-start(bf16[640,256]{1,0:T(8,128)(2,1)} %collective-permute-done.8.refs_9_), channel_id=1, source_target_pairs={{0,3},{1,0},{2,1},{3,2},{4,7},{5,4},{6,5},{7,6},{8,11},{9,8},{10,9... | collective-permute-start | bytes 983048 | tf_op jit(solution)/shard_map/ppermute | solution.py:66
  217.0 6.7 %near_quarters.1 = (f32[256,2048]{1,0:T(8,128)S(1)}, bf16[256,256]{1,0:T(8,128)(2,1)S(1)}) custom-call(bf16[256,1792]{1,0:T(8,128)(2,1)S(1)} %bitcast.15, bf16[2048,256]{1,0:T(8,128)(2,1)} %bitcast.6.refs_0_, bf16[2048,256]{1,0:T(8,128)(2,1)} %bitcast.18, bf16[256,2048]{1,0:T(8,128)(2,1)} %bitcast.20, bf16[2048,256]{1,0:T(8,128)(2,1)} %collective-permute-done.2.refs_3_, ...), custom_call_target="tpu_custom_call" | custom-call | tf_op jit(solution)/shard_map/near_quarters/pallas_call | solution.py:679
  223.7 5.1 %collective-permute-done.13.more_hbm = bf16[640,256]{1,0:T(8,128)(2,1)} collective-permute-done((bf16[640,256]{1,0:T(8,128)(2,1)}, bf16[640,256]{1,0:T(8,128)(2,1)}, u32[]{:S(2)}, u32[]{:S(2)}) %collective-permute-start.13) | collective-permute-done | bytes 327712 | tf_op jit(solution)/shard_map/ppermute | solution.py:66
  228.8 4.2 %far_quarter.1 = bf16[256,1792]{1,0:T(8,128)(2,1)} custom-call(bf16[256,1792]{1,0:T(8,128)(2,1)S(1)} %bitcast.16, bf16[256,256]{1,0:T(8,128)(2,1)S(1)} %get-tuple-element.14.ends_ref, f32[256,2048]{1,0:T(8,128)S(1)} %get-tuple-element.15.total_ref, bf16[2048,256]{1,0:T(8,128)(2,1)S(1)} %collective-permute-done.10.gate_ref, ...), custom_call_target="tpu_custom_call" | custom-call | tf_op jit(solution)/shard_map/far_quarter/pallas_call | solution.py:695
  233.0 14.3 %all-to-all-start.3 = ((bf16[32,8,1792]{2,1,0:T(8,128)(2,1)}), bf16[32,8,1792]{2,1,0:T(8,128)(2,1)S(1)}, u32[]{:S(2)}, u32[]{:S(2)}) async-start(bf16[32,8,1792]{2,1,0:T(8,128)(2,1)} %bitcast.19), calls=%async_computation.3 | async-start | bytes 1835008 | tf_op jit(solution)/shard_map/all_to_all | solution.py:713
  248.7 48.4 %all-to-all-done.3 = bf16[32,8,1792]{2,1,0:T(8,128)(2,1)S(1)} async-done(((bf16[32,8,1792]{2,1,0:T(8,128)(2,1)}), bf16[32,8,1792]{2,1,0:T(8,128)(2,1)S(1)}, u32[]{:S(2)}, u32[]{:S(2)}) %all-to-all-start.3) | async-done | bytes 917536 | tf_op jit(solution)/shard_map/all_to_all | solution.py:713
  297.1 2.0 combine.1
  (54 shorter events, 9.7 us)
Async XLA Ops:
  36.9 45.3 %collective-permute-start.1 = (bf16[4,376,512]{2,1,0:T(8,128)(2,1)S(1)}, bf16[4,376,512]{2,1,0:T(8,128)(2,1)S(1)}, u32[]{:S(2)}, u32[]{:S(2)}) collective-permute-start(bf16[4,376,512]{2,1,0:T(8,128)(2,1)S(1)} %all_to_all.20.shares_ref), channel_id=1, source_target_pairs={{0,4},{4,0},{1,5},{5,1},{2,6},{6,2},{3,7},{7,3},{8,12},{12,8},{9,1... | collective-permute-start | bytes 4620296 | tf_op jit(solution)/shard_map/ppermute | solution.py:66
  79.8 2.3 collective-permute-start
  90.7 11.9 %all-to-all-start.1 = ((bf16[4,40,1152]{2,1,0:T(8,128)(2,1)}), bf16[4,40,1152]{2,1,0:T(8,128)(2,1)S(1)}, u32[]{:S(2)}, u32[]{:S(2)}) async-start(bf16[4,40,1152]{2,1,0:T(8,128)(2,1)} %attend.1), calls=%async_computation.1 | async-start | bytes 737280 | tf_op jit(solution)/shard_map/all_to_all | solution.py:628
  107.7 5.3 %copy-start = (bf16[1,2048,256]{2,1,0:T(8,128)(2,1)S(1)}, bf16[1,2048,256]{2,1,0:T(8,128)(2,1)}, u32[]{:S(2)}) copy-start(bf16[1,2048,256]{2,1,0:T(8,128)(2,1)} %param.28) | copy-start | bytes 3145732
  107.7 7.5 %copy-start.3 = (bf16[1,256,2048]{2,1,0:T(8,128)(2,1)S(1)}, bf16[1,256,2048]{2,1,0:T(8,128)(2,1)}, u32[]{:S(2)}) copy-start(bf16[1,256,2048]{2,1,0:T(8,128)(2,1)} %param.29) | copy-start | bytes 3145732
  107.7 109.3 %all-to-all-start.2 = ((bf16[32,8,1792]{2,1,0:T(8,128)(2,1)}), bf16[32,8,1792]{2,1,0:T(8,128)(2,1)S(1)}, u32[]{:S(2)}, u32[]{:S(2)}) async-start(bf16[32,8,1792]{2,1,0:T(8,128)(2,1)} %bitcast.23), calls=%async_computation.2 | async-start | bytes 1835008 | tf_op jit(solution)/shard_map/all_to_all | solution.py:660
  112.7 49.7 %collective-permute-start.2 = (bf16[2048,256]{1,0:T(8,128)(2,1)}, bf16[2048,256]{1,0:T(8,128)(2,1)}, u32[]{:S(2)}, u32[]{:S(2)}) collective-permute-start(bf16[2048,256]{1,0:T(8,128)(2,1)} %bitcast.6.refs_0_), channel_id=1, source_target_pairs={{0,1},{1,2},{2,3},{3,0},{4,5},{5,6},{6,7},{7,4},{8,9},{9,10},{10,1... | collective-permute-start | bytes 3145736 | tf_op jit(solution)/shard_map/ppermute | solution.py:66
  113.1 49.0 %collective-permute-start.7 = (bf16[1408,256]{1,0:T(8,128)(2,1)S(1)}, bf16[1408,256]{1,0:T(8,128)(2,1)}, u32[]{:S(2)}, u32[]{:S(2)}) collective-permute-start(bf16[1408,256]{1,0:T(8,128)(2,1)S(1)} %slice_bitcast_fusion), channel_id=1, source_target_pairs={{0,3},{1,0},{2,1},{3,2},{4,7},{5,4},{6,5},{7,6},{8,11},{9,8},{10,9... | collective-permute-start | bytes 2162696 | tf_op jit(solution)/shard_map/ppermute | solution.py:66
  115.2 50.1 %collective-permute-start.5 = (bf16[256,2048]{1,0:T(8,128)(2,1)S(1)}, bf16[256,2048]{1,0:T(8,128)(2,1)S(1)}, u32[]{:S(2)}, u32[]{:S(2)}) collective-permute-start(bf16[256,2048]{1,0:T(8,128)(2,1)S(1)} %bitcast.21), channel_id=1, source_target_pairs={{0,1},{1,2},{2,3},{3,0},{4,5},{5,6},{6,7},{7,4},{8,9},{9,10},{10,1... | collective-permute-start | bytes 3145736 | tf_op jit(solution)/shard_map/ppermute | solution.py:66
  115.3 53.2 %collective-permute-start.9 = (bf16[256,2048]{1,0:T(8,128)(2,1)S(1)}, bf16[256,2048]{1,0:T(8,128)(2,1)S(1)}, u32[]{:S(2)}, u32[]{:S(2)}) collective-permute-start(bf16[256,2048]{1,0:T(8,128)(2,1)S(1)} %bitcast.22), channel_id=1, source_target_pairs={{0,3},{1,0},{2,1},{3,2},{4,7},{5,4},{6,5},{7,6},{8,11},{9,8},{10,9... | collective-permute-start | bytes 3145736 | tf_op jit(solution)/shard_map/ppermute | solution.py:66
  117.9 42.5 %collective-permute-start.8 = (bf16[640,256]{1,0:T(8,128)(2,1)S(1)}, bf16[640,256]{1,0:T(8,128)(2,1)}, u32[]{:S(2)}, u32[]{:S(2)}) collective-permute-start(bf16[640,256]{1,0:T(8,128)(2,1)S(1)} %slice_bitcast_fusion.1), channel_id=1, source_target_pairs={{0,3},{1,0},{2,1},{3,2},{4,7},{5,4},{6,5},{7,6},{8,11},{9,8},{10,9... | collective-permute-start | bytes 983048 | tf_op jit(solution)/shard_map/ppermute | solution.py:66
  160.3 52.5 %collective-permute-start.6 = (bf16[2048,256]{1,0:T(8,128)(2,1)}, bf16[2048,256]{1,0:T(8,128)(2,1)S(1)}, u32[]{:S(2)}, u32[]{:S(2)}) collective-permute-start(bf16[2048,256]{1,0:T(8,128)(2,1)} %bitcast.6.refs_0_), channel_id=1, source_target_pairs={{0,3},{1,0},{2,1},{3,2},{4,7},{5,4},{6,5},{7,6},{8,11},{9,8},{10,9... | collective-permute-start | bytes 3145736 | tf_op jit(solution)/shard_map/ppermute | solution.py:66
  162.1 47.7 %collective-permute-start.3 = (bf16[1408,256]{1,0:T(8,128)(2,1)S(1)}, bf16[1408,256]{1,0:T(8,128)(2,1)S(1)}, u32[]{:S(2)}, u32[]{:S(2)}) collective-permute-start(bf16[1408,256]{1,0:T(8,128)(2,1)S(1)} %slice_bitcast_fusion), channel_id=1, source_target_pairs={{0,1},{1,2},{2,3},{3,0},{4,5},{5,6},{6,7},{7,4},{8,9},{9,10},{10,1... | collective-permute-start | bytes 2162696 | tf_op jit(solution)/shard_map/ppermute | solution.py:66
  162.4 66.4 %collective-permute-start.10 = (bf16[2048,256]{1,0:T(8,128)(2,1)}, bf16[2048,256]{1,0:T(8,128)(2,1)S(1)}, u32[]{:S(2)}, u32[]{:S(2)}) collective-permute-start(bf16[2048,256]{1,0:T(8,128)(2,1)} %collective-permute-done.2.refs_3_), channel_id=1, source_target_pairs={{0,1},{1,2},{2,3},{3,0},{4,5},{5,6},{6,7},{7,4},{8,9},{9,10},{10,1... | collective-permute-start | bytes 3145736 | tf_op jit(solution)/shard_map/ppermute | solution.py:66
  165.3 47.5 %copy-start.1 = (bf16[256,2048]{1,0:T(8,128)(2,1)}, bf16[256,2048]{1,0:T(8,128)(2,1)S(1)}, u32[]{:S(2)}) copy-start(bf16[256,2048]{1,0:T(8,128)(2,1)S(1)} %collective-permute-done.5.refs_6_) | copy-start | bytes 3145732
  165.3 44.4 %collective-permute-start.4 = (bf16[640,256]{1,0:T(8,128)(2,1)S(1)}, bf16[640,256]{1,0:T(8,128)(2,1)S(1)}, u32[]{:S(2)}, u32[]{:S(2)}) collective-permute-start(bf16[640,256]{1,0:T(8,128)(2,1)S(1)} %slice_bitcast_fusion.1), channel_id=1, source_target_pairs={{0,1},{1,2},{2,3},{3,0},{4,5},{5,6},{6,7},{7,4},{8,9},{9,10},{10,1... | collective-permute-start | bytes 983048 | tf_op jit(solution)/shard_map/ppermute | solution.py:66
  168.5 44.3 %copy-start.2 = (bf16[256,2048]{1,0:T(8,128)(2,1)}, bf16[256,2048]{1,0:T(8,128)(2,1)S(1)}, u32[]{:S(2)}) copy-start(bf16[256,2048]{1,0:T(8,128)(2,1)S(1)} %collective-permute-done.9.refs_10_) | copy-start | bytes 3145732
  168.5 60.2 %collective-permute-start.11 = (bf16[1408,256]{1,0:T(8,128)(2,1)}, bf16[1408,256]{1,0:T(8,128)(2,1)S(1)}, u32[]{:S(2)}, u32[]{:S(2)}) collective-permute-start(bf16[1408,256]{1,0:T(8,128)(2,1)} %collective-permute-done.7.refs_8_), channel_id=1, source_target_pairs={{0,3},{1,0},{2,1},{3,2},{4,7},{5,4},{6,5},{7,6},{8,11},{9,8},{10,9... | collective-permute-start | bytes 2162696 | tf_op jit(solution)/shard_map/ppermute | solution.py:66
  209.8 19.0 %collective-permute-start.12 = (bf16[128,2048]{1,0:T(8,128)(2,1)}, bf16[128,2048]{1,0:T(8,128)(2,1)S(1)}, u32[]{:S(2)}, u32[]{:S(2)}) collective-permute-start(bf16[128,2048]{1,0:T(8,128)(2,1)} %slice.24), channel_id=1, source_target_pairs={{0,1},{1,2},{2,3},{3,0},{4,5},{5,6},{6,7},{7,4},{8,9},{9,10},{10,1... | collective-permute-start | bytes 1572872 | tf_op jit(solution)/shard_map/ppermute | solution.py:66
  209.8 19.0 %collective-permute-start.14 = (bf16[128,2048]{1,0:T(8,128)(2,1)}, bf16[128,2048]{1,0:T(8,128)(2,1)}, u32[]{:S(2)}, u32[]{:S(2)}) collective-permute-start(bf16[128,2048]{1,0:T(8,128)(2,1)} %slice.25), channel_id=1, source_target_pairs={{0,3},{1,0},{2,1},{3,2},{4,7},{5,4},{6,5},{7,6},{8,11},{9,8},{10,9... | collective-permute-start | bytes 1572872 | tf_op jit(solution)/shard_map/ppermute | solution.py:66
  213.8 14.9 %collective-permute-start.13 = (bf16[640,256]{1,0:T(8,128)(2,1)}, bf16[640,256]{1,0:T(8,128)(2,1)}, u32[]{:S(2)}, u32[]{:S(2)}) collective-permute-start(bf16[640,256]{1,0:T(8,128)(2,1)} %collective-permute-done.8.refs_9_), channel_id=1, source_target_pairs={{0,3},{1,0},{2,1},{3,2},{4,7},{5,4},{6,5},{7,6},{8,11},{9,8},{10,9... | collective-permute-start | bytes 983048 | tf_op jit(solution)/shard_map/ppermute | solution.py:66
  228.8 18.6 %copy-start.7 = (s32[40,4]{0,1:T(4,128)S(1)}, s32[40,4]{0,1:T(4,128)}, u32[]{:S(2)}) copy-start(s32[40,4]{0,1:T(4,128)} %param.30) | copy-start | bytes 1924
  228.8 19.2 %copy-start.8 = (f32[40,4]{0,1:T(4,128)S(1)}, f32[40,4]{0,1:T(4,128)}, u32[]{:S(2)}) copy-start(f32[40,4]{0,1:T(4,128)} %param.31) | copy-start | bytes 1924
  233.0 64.1 %all-to-all-start.3 = ((bf16[32,8,1792]{2,1,0:T(8,128)(2,1)}), bf16[32,8,1792]{2,1,0:T(8,128)(2,1)S(1)}, u32[]{:S(2)}, u32[]{:S(2)}) async-start(bf16[32,8,1792]{2,1,0:T(8,128)(2,1)} %bitcast.19), calls=%async_computation.3 | async-start | bytes 1835008 | tf_op jit(solution)/shard_map/all_to_all | solution.py:713
  (3 other events, 7.2 us)
